TPU v7x, 32 devices: a whole 2x2x4 slice. The times are simulated.
32 devices in a mesh: sp: 16 (over z, y, core), tp: 2 (over x).
Axes of the slice: x: 2, y: 2, z: 4, core: 2. Of those that a mesh axis runs over, the one named last changes fastest.
Arguments:
- tokens: bfloat16 [6144, 2048], P('sp', 'tp'), may hold values from -60 to 60
- pre_gain: bfloat16 [2048], P('tp'), may hold values from 0.099609375 to 1.8984375
- w_query: bfloat16 [2048, 1024], P('sp', 'tp'), may hold values from -1 to 1
- w_key: bfloat16 [2048, 1024], P('sp', 'tp'), may hold values from -1 to 1
- w_value: bfloat16 [2048, 1024], P('sp', 'tp'), may hold values from -0.125 to 0.125
- w_pool: bfloat16 [2048, 1024], P('sp', 'tp'), may hold values from -0.125 to 0.125
- lambdas: float32 [8], P('tp'), may hold values from 0.3 to 0.8
- sub_gain: float32 [128], replicated, may hold values from 0.1 to 1.9
- group_weight: bfloat16 [8, 128, 128], P('tp'), may hold values from -0.5 to 0.5
- pool_scale: float32 [1024], P('tp'), may hold values from 0.1 to 1.9
- w_out: bfloat16 [2048, 2048], P('tp', 'sp'), may hold values from -0.125 to 0.125
Outputs:
- mixed_out: bfloat16 [6144, 2048], P(('sp', 'tp'))
All inputs are finite; a program needn't handle non-finite values.
Results may differ from a plain program's by a relative error of at most 0.015.
Values may be sent and summed in bfloat16 or wider, within the bound.
A program may use at most 128 MiB of HBM per device.

v0:
```python
import functools
import math

import jax
import jax.numpy as jnp
from jax import lax
from jax.experimental import pallas as pl
from jax.experimental.pallas import tpu as pltpu
from jax.sharding import PartitionSpec as P

EPSILON = 1e-06
NEG_LARGE = -1e30
WINDOWS = (2, 4, 8, 16)
RIM_ROWS = 15


def passed_along(block, axis, distance):
    devices = range(lax.axis_size(axis))
    route = [(i - distance, i) for i in devices if i - distance in devices]
    return lax.ppermute(block, axis, route)


def attend(inner, vdim, hdim, member_ref, lam_ref, q_ref, kv_ref, gain_ref, out_ref, acc_ref, max_ref):
    rows = q_ref.shape[1]
    block = pl.program_id(0)
    last = block * inner + member_ref[0]
    scale = 1.0 / math.sqrt(hdim)
    queries = (q_ref[0].astype(jnp.float32) * scale).astype(jnp.bfloat16)
    maps = (queries[:, :hdim], queries[:, hdim:])
    ones = jnp.ones((rows, vdim), jnp.bfloat16)
    acc_ref[...] = jnp.zeros_like(acc_ref)
    max_ref[...] = jnp.full_like(max_ref, NEG_LARGE)

    def step(g, masked):
        keys_values = kv_ref[lax.rem(g, inner), lax.div(g, inner)]
        values = jnp.concatenate([keys_values[:, 2 * hdim :], ones], axis=1)
        for m in range(2):
            keys = keys_values[:, m * hdim : (m + 1) * hdim]
            scores = lax.dot_general(
                maps[m], keys, (((1,), (1,)), ((), ())), preferred_element_type=jnp.float32
            )
            if masked:
                row = lax.broadcasted_iota(jnp.int32, scores.shape, 0)
                col = lax.broadcasted_iota(jnp.int32, scores.shape, 1)
                scores = jnp.where(col <= row, scores, NEG_LARGE)
            old_max = max_ref[m]
            new_max = jnp.maximum(old_max, jnp.max(scores, axis=1, keepdims=True))
            factor = jnp.exp(old_max - new_max)
            expo = jnp.exp(scores - new_max[:, :1])
            acc_ref[m] = acc_ref[m] * factor[:, :1] + jnp.dot(
                expo.astype(jnp.bfloat16), values, preferred_element_type=jnp.float32
            )
            max_ref[m] = new_max

    def body(g, carry):
        step(g, False)
        return carry

    lax.fori_loop(0, last, body, 0)
    step(last, True)
    first = acc_ref[0]
    second = acc_ref[1]
    mix = first[:, :vdim] / first[:, vdim:] - lam_ref[0] * (second[:, :vdim] / second[:, vdim:])
    mean_sq = jnp.mean(mix * mix, axis=1, keepdims=True)
    out_ref[0] = (mix * lax.rsqrt(mean_sq + EPSILON) * gain_ref[...]).astype(jnp.bfloat16)


def flash(q, kv, member, lam, sub_gain):
    inner, outer, rows, width = kv.shape
    qdim = q.shape[-1]
    vdim = width - qdim
    smem = pl.BlockSpec(memory_space=pltpu.SMEM)
    work = outer * rows * outer * rows * inner
    return pl.pallas_call(
        functools.partial(attend, inner, vdim, qdim // 2),
        grid=(outer,),
        out_shape=jax.ShapeDtypeStruct((outer, rows, vdim), jnp.bfloat16),
        in_specs=[
            smem,
            smem,
            pl.BlockSpec((1, rows, qdim), lambda b: (b, 0, 0)),
            pl.BlockSpec(memory_space=pltpu.VMEM),
            pl.BlockSpec(memory_space=pltpu.VMEM),
        ],
        out_specs=pl.BlockSpec((1, rows, vdim), lambda b: (b, 0, 0)),
        scratch_shapes=[
            pltpu.VMEM((2, rows, 2 * vdim), jnp.float32),
            pltpu.VMEM((2, rows, 128), jnp.float32),
        ],
        compiler_params=pltpu.CompilerParams(vmem_limit_bytes=56 * 2**20),
        cost_estimate=pl.CostEstimate(
            flops=4 * work * vdim, bytes_accessed=kv.size * 2, transcendentals=work
        ),
    )(member, lam, q, kv, sub_gain.reshape(1, -1))


def attend_members(hdim, lam_ref, q_ref, own_ref, gain_ref, out_ref, held, acc_ref, max_ref, send, recv):
    outer, rows, _ = q_ref.shape
    vdim = own_ref.shape[2] - 2 * hdim
    sp = lax.axis_index("sp")
    member = lax.rem(sp, 4)
    y = lax.div(member, 2)
    c = lax.rem(member, 2)
    y_peer = sp + 2 - 4 * y
    c_peer = sp + 1 - 2 * c
    barrier = pltpu.get_barrier_semaphore()
    for peer in (y_peer, c_peer):
        pl.semaphore_signal(
            barrier, 1, device_id={"sp": peer}, device_id_type=pl.DeviceIdType.MESH
        )
    pl.semaphore_wait(barrier, 2)

    def remote(src, index, peer):
        return pltpu.make_async_remote_copy(
            src_ref=src,
            dst_ref=held.at[index],
            send_sem=send.at[index],
            recv_sem=recv.at[index],
            device_id={"sp": peer},
            device_id_type=pl.DeviceIdType.MESH,
        )

    across = remote(own_ref, 1, y_peer)
    beside = remote(own_ref, 0, c_peer)
    onward = remote(held.at[1], 2, c_peer)
    across.start()
    beside.start()
    acc_ref[...] = jnp.zeros_like(acc_ref)
    max_ref[...] = jnp.full_like(max_ref, NEG_LARGE)
    scale = 1.0 / math.sqrt(hdim)

    def visit(ref, other):
        shift = (member - other) * rows
        for block in range(outer):
            queries = (q_ref[block].astype(jnp.float32) * scale).astype(jnp.bfloat16)
            length = (block + 1) * rows
            keys_values = ref[: block + 1].reshape(length, 2 * hdim + vdim)
            values = jnp.concatenate(
                [keys_values[:, 2 * hdim :], jnp.ones((length, vdim), jnp.bfloat16)], axis=1
            )
            for m in range(2):
                scores = lax.dot_general(
                    queries[:, m * hdim : (m + 1) * hdim],
                    keys_values[:, m * hdim : (m + 1) * hdim],
                    (((1,), (1,)), ((), ())),
                    preferred_element_type=jnp.float32,
                )
                edge = scores[:, block * rows :]
                row = lax.broadcasted_iota(jnp.int32, edge.shape, 0)
                col = lax.broadcasted_iota(jnp.int32, edge.shape, 1)
                edge = jnp.where(col <= row + shift, edge, NEG_LARGE)
                if block > 0:
                    scores = jnp.concatenate([scores[:, : block * rows], edge], axis=1)
                else:
                    scores = edge
                old_max = max_ref[block, m]
                new_max = jnp.maximum(old_max, jnp.max(scores, axis=1, keepdims=True))
                factor = jnp.exp(old_max - new_max)
                expo = jnp.exp(scores - new_max[:, :1])
                acc_ref[block, m] = acc_ref[block, m] * factor[:, :1] + jnp.dot(
                    expo.astype(jnp.bfloat16), values, preferred_element_type=jnp.float32
                )
                max_ref[block, m] = new_max

    visit(own_ref, member)

    def arrived(j, carry):
        @pl.when(j == 0)
        def _():
            beside.wait_recv()

        @pl.when(j == 1)
        def _():
            across.wait_recv()
            onward.start()

        @pl.when(j == 2)
        def _():
            onward.wait_recv()

        other_y = jnp.where(j >= 1, 1 - y, y)
        other_c = jnp.where(j == 1, c, 1 - c)
        visit(held.at[j], 2 * other_y + other_c)
        return carry

    lax.fori_loop(0, 3, arrived, 0)
    for copy in (across, beside, onward):
        copy.wait_send()
    for block in range(outer):
        first = acc_ref[block, 0]
        second = acc_ref[block, 1]
        mix = first[:, :vdim] / first[:, vdim:]
        mix = mix - lam_ref[0] * (second[:, :vdim] / second[:, vdim:])
        mean_sq = jnp.mean(mix * mix, axis=1, keepdims=True)
        normed = mix * lax.rsqrt(mean_sq + EPSILON) * gain_ref[...]
        out_ref[block] = normed.astype(jnp.bfloat16)


def flash_members(q, kv, lam, sub_gain):
    outer, rows, width = kv.shape
    qdim = q.shape[-1]
    vdim = width - qdim
    vmem = pl.BlockSpec(memory_space=pltpu.VMEM)
    work = 4 * outer * rows * outer * rows
    return pl.pallas_call(
        functools.partial(attend_members, qdim // 2),
        out_shape=jax.ShapeDtypeStruct((outer, rows, vdim), jnp.bfloat16),
        in_specs=[pl.BlockSpec(memory_space=pltpu.SMEM), vmem, vmem, vmem],
        out_specs=vmem,
        scratch_shapes=[
            pltpu.VMEM((3, outer, rows, width), jnp.bfloat16),
            pltpu.VMEM((outer, 2, rows, 2 * vdim), jnp.float32),
            pltpu.VMEM((outer, 2, rows, 128), jnp.float32),
            pltpu.SemaphoreType.DMA((3,)),
            pltpu.SemaphoreType.DMA((3,)),
        ],
        compiler_params=pltpu.CompilerParams(
            vmem_limit_bytes=56 * 2**20, collective_id=1, has_side_effects=True
        ),
        cost_estimate=pl.CostEstimate(
            flops=4 * work * vdim, bytes_accessed=4 * kv.size * 2, transcendentals=work
        ),
    )(lam, q, kv, sub_gain.reshape(1, -1))


def spread(n_sp, count, with_swap, *refs):
    weights, refs = refs[:count], refs[count:]
    mine, refs = refs[0], refs[1:]
    fulls, refs = refs[:count], refs[count:]
    theirs, refs = refs[0], refs[1:]
    up_send, up_recv, down_send, down_recv, y_send, y_recv, c_send, c_recv, own_sem, swap_sem = refs
    depth = n_sp // 4
    rows = weights[0].shape[0]
    sp = lax.axis_index("sp")
    z = lax.div(sp, 4)
    y = lax.rem(lax.div(sp, 2), 2)
    c = lax.rem(sp, 2)
    y_peer = z * 4 + (1 - y) * 2 + c
    c_peer = z * 4 + y * 2 + (1 - c)
    barrier = pltpu.get_barrier_semaphore()

    def greet(device):
        pl.semaphore_signal(barrier, 1, device_id=device, device_id_type=pl.DeviceIdType.MESH)

    greet({"sp": y_peer})
    greet({"sp": c_peer})
    greeted = 2
    if with_swap:
        greet({"tp": 1 - lax.axis_index("tp")})
        greeted = 3

    @pl.when(z > 0)
    def _():
        greet({"sp": sp - 4})

    @pl.when(z < depth - 1)
    def _():
        greet({"sp": sp + 4})

    in_line = jnp.where(z > 0, 1, 0) + jnp.where(z < depth - 1, 1, 0)
    pl.semaphore_wait(barrier, greeted + in_line)

    def slot(a, zz, yy, cc):
        start = pl.multiple_of((zz * 4 + yy * 2 + cc) * rows, rows)
        return fulls[a].at[pl.ds(start, rows), :]

    def remote(src, dst, send, recv, device):
        return pltpu.make_async_remote_copy(
            src_ref=src,
            dst_ref=dst,
            send_sem=send,
            recv_sem=recv,
            device_id=device,
            device_id_type=pl.DeviceIdType.MESH,
        )

    def line_copy(side, k, a, src):
        sends, recvs = (up_send, up_recv) if side > 0 else (down_send, down_recv)
        there = slot(a, z - side * k, y, c)
        return remote(
            there if src is None else src,
            there,
            sends.at[k, a],
            recvs.at[k + 1, a],
            {"sp": sp + 4 * side},
        )

    def y_copy(zz, yy, a, src):
        there = slot(a, zz, yy, c)
        src = there if src is None else src
        return remote(src, there, y_send.at[zz, a], y_recv.at[zz, a], {"sp": y_peer})

    def c_copy(zz, yy, cc, a, src):
        there = slot(a, zz, yy, cc)
        src = there if src is None else src
        return remote(src, there, c_send.at[zz, yy, a], c_recv.at[zz, yy, a], {"sp": c_peer})

    def can_go(side):
        return z < depth - 1 if side > 0 else z > 0

    def came(side, k):
        return z >= k if side > 0 else z + k <= depth - 1

    if with_swap:
        swap = remote(
            mine, theirs, swap_sem.at[0], swap_sem.at[1], {"tp": 1 - lax.axis_index("tp")}
        )
        swap.start()
    for a in range(count):
        for side in (1, -1):

            @pl.when(can_go(side))
            def _():
                line_copy(side, 0, a, weights[a]).start()

        y_copy(z, y, a, weights[a]).start()
    for a in range(count):
        c_copy(z, y, c, a, weights[a]).start()
        pltpu.make_async_copy(weights[a], slot(a, z, y, c), own_sem.at[a]).start()

    def from_pair(zz):
        for a in range(count):
            y_copy(zz, 1 - y, a, None).wait_recv()
            c_copy(zz, 1 - y, c, a, None).start()

    def relay(k, carry):
        for side in (1, -1):
            recvs = up_recv if side > 0 else down_recv

            @pl.when(came(side, k))
            def _():
                zz = z - side * k
                for a in range(count):
                    there = slot(a, zz, y, c)
                    remote(there, there, up_send.at[0, a], recvs.at[k, a], {"sp": y_peer}).wait_recv()

                    @pl.when(can_go(side))
                    def _():
                        line_copy(side, k, a, None).start()

                    y_copy(zz, y, a, None).start()
                    c_copy(zz, y, c, a, None).start()

        @pl.when(k == 1)
        def _():
            from_pair(z)

        for side in (1, -1):

            @pl.when((k > 1) & came(side, k - 1))
            def _():
                from_pair(z - side * (k - 1))

        return carry

    lax.fori_loop(1, depth, relay, 0)
    if depth == 1:
        from_pair(z)
    for side in (1, -1):
        if depth > 1:

            @pl.when(came(side, depth - 1))
            def _():
                from_pair(z - side * (depth - 1))

    def drain(zz, carry):
        for a in range(count):
            y_copy(zz, y, a, None).wait_send()
            for yy in range(2):
                c_copy(zz, yy, 1 - c, a, None).wait_recv()
                c_copy(zz, yy, c, a, None).wait_send()
        return carry

    lax.fori_loop(0, depth, drain, 0)

    def drain_line(k, carry):
        for side in (1, -1):

            @pl.when(came(side, k) & can_go(side))
            def _():
                for a in range(count):
                    line_copy(side, k, a, None).wait_send()

        return carry

    lax.fori_loop(0, depth, drain_line, 0)
    for a in range(count):
        pltpu.make_async_copy(weights[a], slot(a, z, y, c), own_sem.at[a]).wait()
    if with_swap:
        swap.wait()


def gather_weights(weights, mine, with_swap):
    n_sp = lax.axis_size("sp")
    count = len(weights)
    depth = n_sp // 4
    sems = pltpu.SemaphoreType.DMA
    any_spec = pl.BlockSpec(memory_space=pl.ANY)
    vmem_spec = pl.BlockSpec(memory_space=pltpu.VMEM)
    shapes = [jax.ShapeDtypeStruct((n_sp * w.shape[0], w.shape[1]), w.dtype) for w in weights]
    shapes.append(jax.ShapeDtypeStruct(mine.shape, mine.dtype))
    moved = sum(w.size for w in weights) * 2 * n_sp
    return pl.pallas_call(
        functools.partial(spread, n_sp, count, with_swap),
        out_shape=shapes,
        in_specs=[vmem_spec] * (count + 1),
        out_specs=[any_spec] * (count + 1),
        scratch_shapes=[
            sems((depth + 1, count)),
            sems((depth + 1, count)),
            sems((depth + 1, count)),
            sems((depth + 1, count)),
            sems((depth, count)),
            sems((depth, count)),
            sems((depth, 2, count)),
            sems((depth, 2, count)),
            sems((count,)),
            sems((2,)),
        ],
        compiler_params=pltpu.CompilerParams(collective_id=0, has_side_effects=True),
        cost_estimate=pl.CostEstimate(flops=10**10, bytes_accessed=moved, transcendentals=0),
    )(*weights, mine)


def trailing(x, window_ids, group_dim):
    column_window = jnp.repeat(window_ids, group_dim)[None, :]
    running = x
    picked = jnp.zeros_like(x)
    for slot, span in enumerate(WINDOWS):
        half = span // 2
        running = running + jnp.pad(running[:-half], ((half, 0), (0, 0)))
        picked = jnp.where(column_window == slot, running, picked)
    return picked


def local(
    tokens,
    pre_gain,
    w_query,
    w_key,
    w_value,
    w_pool,
    lambdas,
    sub_gain,
    group_weight,
    pool_scale,
    w_out,
):
    n_tp = lax.axis_size("tp")
    n_sp = lax.axis_size("sp")
    tp = lax.axis_index("tp")
    sp = lax.axis_index("sp")
    tok_rows = tokens.shape[0]
    model_width = tokens.shape[1] * n_tp
    heads = lambdas.shape[0]
    qdim = w_query.shape[1] // heads
    vdim = w_value.shape[1] // heads
    groups = group_weight.shape[0]
    group_dim = group_weight.shape[1]
    head_width = 2 * qdim + vdim
    outer = math.gcd(n_sp, heads)
    inner = n_sp // outer
    per_device = heads // outer

    features = tokens.astype(jnp.float32)
    mine = (features * pre_gain.astype(jnp.float32)[None, :]).astype(jnp.bfloat16)
    squares = jnp.sum(features * features, axis=1, keepdims=True)
    swap = [(0, 1), (1, 0)]
    weights = [w_query, w_key, w_value, w_pool]
    if n_sp % 4 == 0:
        *weights, theirs = gather_weights(weights, mine, n_tp == 2)
    else:
        weights = [lax.all_gather(w, "sp", axis=0, tiled=True) for w in weights]
        theirs = lax.ppermute(mine, "tp", swap) if n_tp == 2 else mine
    w_sorted = w_out.reshape(heads, 2, vdim, -1).swapaxes(0, 1).reshape(w_out.shape)
    w_sorted, weights = lax.optimization_barrier((w_sorted, weights))
    w_out_rows = lax.all_gather(w_sorted, "sp", axis=1, tiled=True)
    if n_tp == 2:
        squares = squares + lax.ppermute(squares, "tp", swap)
        scaled = jnp.concatenate(
            [jnp.where(tp == 0, mine, theirs), jnp.where(tp == 0, theirs, mine)], axis=1
        )
    else:
        scaled = lax.all_gather(mine, "tp", axis=1, tiled=True)
        squares = lax.psum(squares, "tp")
    inverse = lax.rsqrt(squares / model_width + EPSILON)
    queries, key_rows, values, pool_in = [
        (jnp.dot(scaled, w, preferred_element_type=jnp.float32) * inverse).astype(jnp.bfloat16)
        for w in weights
    ]
    by_head = jnp.concatenate(
        [
            x.reshape(tok_rows, heads, -1).swapaxes(0, 1)
            for x in (queries, key_rows, values)
        ],
        axis=2,
    )
    across = [[o * inner + i for o in range(outer)] for i in range(inner)]
    within = [[o * inner + i for i in range(inner)] for o in range(outer)]
    by_head = by_head.reshape(outer, per_device, tok_rows, head_width)
    if outer > 1:
        by_head = lax.all_to_all(by_head, "sp", 0, 0, axis_index_groups=across)
    first_head = lax.div(sp, inner) * per_device
    attended = []
    if inner == 4 and per_device == 1:
        lam = lax.dynamic_slice_in_dim(lambdas, first_head, 1)
        attended.append(
            flash_members(by_head[:, 0, :, :qdim], by_head[:, 0, :, qdim:], lam, sub_gain)
        )
    else:
        kv = lax.all_gather(by_head[..., qdim:], "sp", axis=0, axis_index_groups=within)
        member = lax.rem(sp, inner).reshape(1)
        for p in range(per_device):
            lam = lax.dynamic_slice_in_dim(lambdas, first_head + p, 1)
            attended.append(flash(by_head[:, p, :, :qdim], kv[:, :, p], member, lam, sub_gain))
    attended = jnp.stack(attended, axis=1)
    if outer > 1:
        attended = lax.all_to_all(attended, "sp", 0, 0, axis_index_groups=across)
    attended = attended.reshape(heads, tok_rows, vdim)

    halo = passed_along(pool_in[tok_rows - RIM_ROWS - 1 :], "sp", 1)
    extended = jnp.concatenate([halo, pool_in], axis=0).astype(jnp.float32)
    window_ids = (tp * groups + jnp.arange(groups, dtype=jnp.int32)) % len(WINDOWS)
    sums = trailing(extended, window_ids, group_dim)[RIM_ROWS + 1 :]
    spans = jnp.repeat(jnp.left_shift(2, window_ids), group_dim)
    positions = sp * tok_rows + jnp.arange(tok_rows, dtype=jnp.int32)
    count = jnp.minimum(positions[:, None] + 1, spans[None, :]).astype(jnp.float32)
    differ = (sums / count - pool_in.astype(jnp.float32)).astype(jnp.bfloat16)
    pooled = jnp.einsum(
        "tgc,gcd->tgd",
        differ.reshape(tok_rows, groups, group_dim),
        group_weight,
        preferred_element_type=jnp.float32,
    )
    pooled = (pooled * pool_scale.reshape(groups, group_dim)).astype(jnp.bfloat16)
    branch = jnp.concatenate(
        [attended.swapaxes(0, 1).reshape(tok_rows, -1), pooled.reshape(tok_rows, -1)], axis=1
    )
    if n_tp == 2:
        half = tok_rows // 2
        send = lax.dynamic_slice_in_dim(branch, (1 - tp) * half, half, 0)
        send = jnp.dot(send, w_out_rows, preferred_element_type=jnp.float32).astype(jnp.bfloat16)
        got = lax.ppermute(send, "tp", swap)
        keep = lax.dynamic_slice_in_dim(branch, tp * half, half, 0)
        keep = jnp.dot(keep, w_out_rows, preferred_element_type=jnp.float32)
        return (keep + got.astype(jnp.float32)).astype(jnp.bfloat16)
    partial = jnp.dot(branch, w_out_rows, preferred_element_type=jnp.float32)
    return lax.psum_scatter(partial.astype(jnp.bfloat16), "tp", scatter_dimension=0, tiled=True)


def solution(mesh):
    placed = (
        P("sp", "tp"),
        P("tp"),
        P("sp", "tp"),
        P("sp", "tp"),
        P("sp", "tp"),
        P("sp", "tp"),
        P("tp"),
        P(),
        P("tp", None, None),
        P("tp"),
        P("tp", "sp"),
    )
    return jax.shard_map(
        local, mesh=mesh, in_specs=placed, out_specs=P(("sp", "tp"), None), check_vma=False
    )
```

profile of v0, /device:TPU:0, one launch (start us, length us, event | category | flops | bytes accessed | tf_op | source)
XLA Modules:
  0.0 214.9 jit_solution(7316979511020602199)
XLA Ops:
  6.5 0.7 convert_element_type.57
  7.3 1.7 copy.33
  8.9 2.2 %fusion.1 = (f32[384]{0:T(512)S(1)}, bf16[384,1024]{1,0:T(8,128)(2,1)}) fusion(bf16[384,1024]{1,0:T(8,128)(2,1)} %param.11, f32[1024]{0:T(1024)S(1)} %convert_element_type.57), kind=kLoop, calls=%fused_computation.4 | loop fusion | flops 1965696 | bytes 1578496 | tf_op jit(solution)/shard_map/reduce_sum | solution.py:467
  11.2 54.5 %shard_map.109 = (bf16[2048,512]{1,0:T(8,128)(2,1)}, bf16[2048,512]{1,0:T(8,128)(2,1)}, bf16[2048,512]{1,0:T(8,128)(2,1)}, bf16[2048,512]{1,0:T(8,128)(2,1)}, bf16[384,1024]{1,0:T(8,128)(2,1)}) custom-call(bf16[128,512]{1,0:T(8,128)(2,1)} %refs_0_.1, bf16[128,512]{1,0:T(8,128)(2,1)} %refs_1_.1, bf16[128,512]{1,0:T(8,128)(2,1)} %refs_2_.1, ...), custom_call_target="tpu_custom_call" | custom-call | flops 10000000000 | bytes 8388608 | tf_op jit(solution)/shard_map/pallas_call | solution.py:403
  65.6 0.0 all-gather.2.cloned.1.call-update
  65.7 1.6 collective-permute-start
  67.2 0.1 broadcast_bitcast_fusion.1
  67.3 1.4 broadcast_select_fusion.1
  68.7 0.0 copy-start.2
  68.7 0.6 collective-permute-done
  69.3 0.0 copy-done.7
  69.3 1.0 fusion.2
  70.3 0.2 copy.34
  70.6 2.6 %fusion.3 = bf16[384,512]{1,0:T(8,128)(2,1)S(1)} fusion(bf16[2048,512]{1,0:T(8,128)(2,1)} %get-tuple-element.21, f32[384]{0:T(512)S(1)} %rsqrt_reduce_fusion, bf16[384,1024]{1,0:T(8,128)(2,1)S(1)} %get-tuple-element.26, bf16[384,1024]{1,0:T(8,128)(2,1)S(1)} %get-tuple-element.25), kind=kOutput, calls=%fused_computation.13 | convolution fusion | flops 808845312 | bytes 4064768 | tf_op jit(solution)/shard_map/dot_general | solution.py:488
  73.1 0.2 copy.35
  73.4 2.6 %fusion.4 = bf16[384,512]{1,0:T(8,128)(2,1)S(1)} fusion(bf16[2048,512]{1,0:T(8,128)(2,1)} %get-tuple-element.22, f32[384]{0:T(512)S(1)} %rsqrt_reduce_fusion, bf16[384,1024]{1,0:T(8,128)(2,1)S(1)} %get-tuple-element.26, bf16[384,1024]{1,0:T(8,128)(2,1)S(1)} %get-tuple-element.25), kind=kOutput, calls=%fused_computation.14 | convolution fusion | flops 808845312 | bytes 4064768 | tf_op jit(solution)/shard_map/dot_general | solution.py:488
  76.0 0.2 copy.36
  76.2 0.1 maximum_bitcast_fusion
  76.3 1.5 copy.37
  77.8 5.1 %all-to-all-start = ((bf16[4,1,384,384]{3,2,1,0:T(8,128)(2,1)}), bf16[4,1,384,384]{3,2,1,0:T(8,128)(2,1)S(1)}, u32[]{:S(2)}, u32[]{:S(2)}) async-start(bf16[4,1,384,384]{3,2,1,0:T(8,128)(2,1)} %copy.37), calls=%async_computation | async-start | bytes 2359296 | tf_op jit(solution)/shard_map/all_to_all | solution.py:502
  82.9 0.1 broadcast_bitcast_fusion.2
  83.0 0.1 broadcast_bitcast_fusion.3
  83.0 0.1 broadcast_bitcast_fusion.4
  83.1 0.1 broadcast_bitcast_fusion
  83.2 2.6 %fusion.5 = bf16[384,512]{1,0:T(8,128)(2,1)S(1)} fusion(bf16[2048,512]{1,0:T(8,128)(2,1)} %get-tuple-element.23, f32[384]{0:T(512)S(1)} %rsqrt_reduce_fusion, bf16[384,1024]{1,0:T(8,128)(2,1)S(1)} %get-tuple-element.26, bf16[384,1024]{1,0:T(8,128)(2,1)S(1)} %copy-done.3), kind=kOutput, calls=%fused_computation.15 | convolution fusion | flops 808845312 | bytes 4064768 | tf_op jit(solution)/shard_map/dot_general | solution.py:488
  85.8 1.3 collective-permute-start.1
  87.1 0.7 dynamic_slice.9.lam_ref
  87.8 0.1 collective-permute-done.1
  87.9 0.1 maximum_convert_fusion
  88.0 0.1 pad_add_fusion.2
  88.1 0.2 pad_add_fusion.1
  88.3 40.3 %all-to-all-done = bf16[4,1,384,384]{3,2,1,0:T(8,128)(2,1)S(1)} async-done(((bf16[4,1,384,384]{3,2,1,0:T(8,128)(2,1)}), bf16[4,1,384,384]{3,2,1,0:T(8,128)(2,1)S(1)}, u32[]{:S(2)}, u32[]{:S(2)}) %all-to-all-start) | async-done | bytes 1179680 | tf_op jit(solution)/shard_map/all_to_all | solution.py:502
  128.6 0.8 slice_bitcast_fusion.1.q_ref
  129.5 0.9 slice_bitcast_fusion.own_ref
  130.4 35.5 %shard_map.110 = bf16[4,384,128]{2,1,0:T(8,128)(2,1)} custom-call(f32[1]{0:T(128)} %dynamic_slice.9.lam_ref, bf16[4,384,128]{2,1,0:T(8,128)(2,1)} %slice_bitcast_fusion.1.q_ref, bf16[4,384,256]{2,1,0:T(8,128)(2,1)} %slice_bitcast_fusion.own_ref, f32[1,128]{1,0:T(1,128)} %bitcast.75), custom_call_target="tpu_custom_call" | custom-call | flops 4831838208 | bytes 3145728 | tf_op jit(solution)/shard_map/pallas_call | solution.py:205
  165.9 3.5 %all-to-all-start.1 = ((bf16[4,1,384,128]{3,2,1,0:T(8,128)(2,1)}), bf16[4,1,384,128]{3,2,1,0:T(8,128)(2,1)S(1)}, u32[]{:S(2)}, u32[]{:S(2)}) async-start(bf16[4,1,384,128]{3,2,1,0:T(8,128)(2,1)} %bitcast.72), calls=%async_computation.1 | async-start | bytes 786432 | tf_op jit(solution)/shard_map/all_to_all | solution.py:518
  169.4 0.0 copy-start.4
  169.4 0.2 pad_add_fusion
  169.6 0.1 slice.38
  169.7 0.4 copy-done.4
  170.1 0.7 fusion.6
  170.8 10.2 %all-to-all-done.1 = bf16[4,1,384,128]{3,2,1,0:T(8,128)(2,1)S(1)} async-done(((bf16[4,1,384,128]{3,2,1,0:T(8,128)(2,1)}), bf16[4,1,384,128]{3,2,1,0:T(8,128)(2,1)S(1)}, u32[]{:S(2)}, u32[]{:S(2)}) %all-to-all-start.1) | async-done | bytes 393248 | tf_op jit(solution)/shard_map/all_to_all | solution.py:518
  181.0 0.2 copy.41
  181.3 0.0 all-gather.2.cloned.1.call-done
  181.3 3.6 %convolution_convert_fusion = bf16[192,2048]{1,0:T(8,128)(2,1)S(1)} fusion(bf16[1024,2048]{1,0:T(8,128)(2,1)} %all-gather.2.cloned.1.call-done, s32[]{:T(128)S(6)} %select_n.51, bf16[384,512]{0,1:T(8,128)(2,1)S(1)} %bitcast.70, bf16[384,512]{0,1:T(8,128)(2,1)S(1)} %bitcast.76), kind=kOutput, calls=%fused_computation | convolution fusion | flops 806486016 | bytes 5767172 | tf_op jit(solution)/shard_map/dot_general | solution.py:542
  184.9 1.9 collective-permute-start.2
  186.8 16.8 %collective-permute-done.2 = bf16[192,2048]{1,0:T(8,128)(2,1)S(1)} collective-permute-done((bf16[192,2048]{1,0:T(8,128)(2,1)S(1)}, bf16[192,2048]{1,0:T(8,128)(2,1)S(1)}, u32[]{:S(2)}, u32[]{:S(2)}) %collective-permute-start.2) | collective-permute-done | bytes 786464 | tf_op jit(solution)/shard_map/ppermute | solution.py:543
  203.6 4.4 %add_convert_fusion = bf16[192,2048]{1,0:T(8,128)(2,1)} fusion(bf16[192,2048]{1,0:T(8,128)(2,1)S(1)} %collective-permute-done.2, bf16[1024,2048]{1,0:T(8,128)(2,1)} %all-gather.2.cloned.1.call-done, s32[]{:T(128)S(6)} %select_n.50, bf16[384,512]{0,1:T(8,128)(2,1)S(1)} %bitcast.71, bf16[384,512]{0,1:T(8,128)(2,1)} %bitcast.77), kind=kOutput, calls=%fused_computation.6 | convolution fusion | flops 807272448 | bytes 6553604 | tf_op jit(solution)/shard_map/dot_general | solution.py:545
  (20 shorter events, 0.1 us)
Async XLA Ops:
  6.5 163.1 %copy-start = (bf16[4,128,128]{2,1,0:T(8,128)(2,1)S(1)}, bf16[4,128,128]{2,1,0:T(8,128)(2,1)}, u32[]{:S(2)}) copy-start(bf16[4,128,128]{2,1,0:T(8,128)(2,1)} %param.19) | copy-start | bytes 393220
  6.5 174.8 %all-gather.2.cloned.1.call-start = ((), (), s32[]{:S(2)}) async-start(), calls=%async_computation.2 | async-start | bytes 4456448 | tf_op jit(solution)/shard_map/all_gather | solution.py:477
  11.2 56.2 %copy-start.1 = (bf16[384,1024]{1,0:T(8,128)(2,1)S(1)}, bf16[384,1024]{1,0:T(8,128)(2,1)}, u32[]{:S(2)}) copy-start(bf16[384,1024]{1,0:T(8,128)(2,1)} %get-tuple-element.28.refs_4_) | copy-start | bytes 2359300
  65.7 3.6 %collective-permute-start = (f32[384,1]{0,1:T(1,128)S(1)}, f32[384,1]{0,1:T(1,128)S(1)}, u32[]{:S(2)}, u32[]{:S(2)}) collective-permute-start(f32[384,1]{0,1:T(1,128)S(1)} %broadcast_in_dim.43), channel_id=1, source_target_pairs={{0,1},{1,0},{2,3},{3,2},{4,5},{5,4},{6,7},{7,6},{8,9},{9,8},{10,11... | collective-permute-start | bytes 4616 | tf_op jit(solution)/shard_map/ppermute | solution.py:479
  67.2 2.1 copy-start.7
  68.7 4.7 %copy-start.2 = (bf16[384,1024]{1,0:T(8,128)(2,1)}, bf16[384,1024]{1,0:T(8,128)(2,1)S(1)}, u32[]{:S(2)}) copy-start(bf16[384,1024]{1,0:T(8,128)(2,1)S(1)} %get-tuple-element.25) | copy-start | bytes 2359300
  77.8 5.4 %copy-start.3 = (bf16[384,1024]{1,0:T(8,128)(2,1)S(1)}, bf16[384,1024]{1,0:T(8,128)(2,1)}, u32[]{:S(2)}) copy-start(bf16[384,1024]{1,0:T(8,128)(2,1)} %copy-done.2) | copy-start | bytes 2359300
  77.8 50.8 %all-to-all-start = ((bf16[4,1,384,384]{3,2,1,0:T(8,128)(2,1)}), bf16[4,1,384,384]{3,2,1,0:T(8,128)(2,1)S(1)}, u32[]{:S(2)}, u32[]{:S(2)}) async-start(bf16[4,1,384,384]{3,2,1,0:T(8,128)(2,1)} %copy.37), calls=%async_computation | async-start | bytes 2359296 | tf_op jit(solution)/shard_map/all_to_all | solution.py:502
  83.2 3.9 %copy-start.5 = (f32[4]{0:T(128)S(1)}, f32[4]{0:T(128)}, u32[]{:S(2)}) copy-start(f32[4]{0:T(128)} %param.17) | copy-start | bytes 52
  85.8 2.1 collective-permute-start.1
  165.9 15.1 %all-to-all-start.1 = ((bf16[4,1,384,128]{3,2,1,0:T(8,128)(2,1)}), bf16[4,1,384,128]{3,2,1,0:T(8,128)(2,1)S(1)}, u32[]{:S(2)}, u32[]{:S(2)}) async-start(bf16[4,1,384,128]{3,2,1,0:T(8,128)(2,1)} %bitcast.72), calls=%async_computation.1 | async-start | bytes 786432 | tf_op jit(solution)/shard_map/all_to_all | solution.py:518
  169.4 0.7 copy-start.4
  170.8 10.5 %copy-start.6 = (bf16[4,384,128]{1,2,0:T(8,128)(2,1)}, bf16[4,384,128]{1,2,0:T(8,128)(2,1)S(1)}, u32[]{:S(2)}) copy-start(bf16[4,384,128]{1,2,0:T(8,128)(2,1)S(1)} %fusion.6) | copy-start | bytes 1179652
  184.9 18.7 %collective-permute-start.2 = (bf16[192,2048]{1,0:T(8,128)(2,1)S(1)}, bf16[192,2048]{1,0:T(8,128)(2,1)S(1)}, u32[]{:S(2)}, u32[]{:S(2)}) collective-permute-start(bf16[192,2048]{1,0:T(8,128)(2,1)S(1)} %convolution_convert_fusion), channel_id=1, source_target_pairs={{0,1},{1,0},{2,3},{3,2},{4,5},{5,4},{6,7},{7,6},{8,9},{9,8},{10,11... | collective-permute-start | bytes 2359304 | tf_op jit(solution)/shard_map/ppermute | solution.py:543
Sparse Core Ops, SparseCore 0:
  65.8 67.5 all-gather.1
where the time goes:
time: 215 us
  Pallas kernels  90 us (42%)
  waiting for transfers between devices  68.1 us (32%)
  matrix products  17.5 us (8%)
  between operations  13.7 us (6%)
  starting transfers between devices  13.3 us (6%)
  local copies, waits for them, and re-layouts  7.27 us (3%)
  other arithmetic  5.08 us (2%)
    pallas_call x1, Pallas kernels, gather_weights(): pl.pallas_call(functools.partial(spread, n_sp, count, with_swap), out_sha...  54.5 us
    all_to_all x1, waiting for transfers between devices, local(): by_head = lax.all_to_all(by_head, 'sp', 0, 0, axis_index_groups=across)  40.3 us
    pallas_call x1, Pallas kernels, flash_members(): pl.pallas_call(functools.partial(attend_members, qdim // 2), out_shape=ja...  35.5 us
    ppermute x1, waiting for transfers between devices, local(): got = lax.ppermute(send, 'tp', swap)  16.8 us
    all_to_all x1, waiting for transfers between devices, local(): attended = lax.all_to_all(attended, 'sp', 0, 0, axis_index_groups=across)  10.2 us
    dot_general x4, matrix products, local(): jnp.dot(scaled, w, preferred_element_type=jnp.float32) * inverse  8.75 us
    all_to_all x1, starting transfers between devices, local(): by_head = lax.all_to_all(by_head, 'sp', 0, 0, axis_index_groups=across)  5.07 us
    dot_general x1, matrix products, local(): keep = jnp.dot(keep, w_out_rows, preferred_element_type=jnp.float32)  4.4 us
  transfers between devices with their start and end apart: 6, of which 5 were waited for; matrix products, arithmetic and copies ran while one was open for 8% of the time, Pallas kernels for 17%

commit v1 on v0

--- a/solution.py
+++ b/solution.py
@@ -422,6 +422,272 @@
     )(*weights, mine)
 
 
+def arrival(z, i):
+    half = z // 2
+    return (z, 1 + 4 * half - z, 2 - half, 3 - 3 * half)[i]
+
+
+def mix(hdim, lam_ref, q_ref, k_ref, v_ref, gain_ref, out_ref, q_in, k_all, v_all, acc, top, total, done, *sems):
+    (z_send, z_recv, in_send, in_recv, back_send, back_recv) = sems
+    planes, rows, _ = q_ref.shape
+    vdim = v_ref.shape[1]
+    members = k_all.shape[1]
+    sp = lax.axis_index("sp")
+    z = sp // members
+    m = sp % members
+    y_member = (m + 2) % members
+    c_member = m + 1 - 2 * (m % 2)
+    turned = members - 1 - m
+
+    def at(plane, member):
+        return {"sp": plane * members + member}
+
+    def holder(block, member):
+        return member + (block % 2) * (members - 1 - 2 * member)
+
+    barrier = pltpu.get_barrier_semaphore()
+
+    def greet(device):
+        pl.semaphore_signal(barrier, 1, device_id=device, device_id_type=pl.DeviceIdType.MESH)
+
+    order = [arrival(z, i) for i in range(planes)]
+    for plane in order[1:]:
+        greet(at(plane, m))
+        greet(at(plane, turned))
+    for member in (turned, y_member, c_member):
+        greet(at(z, member))
+    pl.semaphore_wait(barrier, 2 * planes + 1)
+
+    def remote(src, dst, send, recv, device):
+        return pltpu.make_async_remote_copy(
+            src_ref=src,
+            dst_ref=dst,
+            send_sem=send,
+            recv_sem=recv,
+            device_id=device,
+            device_id_type=pl.DeviceIdType.MESH,
+        )
+
+    def k_out(plane):
+        return remote(k_ref.at[plane], k_all.at[z, m], z_send.at[0, plane], z_recv.at[0, z], at(plane, m))
+
+    def v_out(plane):
+        return remote(v_ref.at[plane], v_all.at[z, m], z_send.at[1, plane], z_recv.at[1, z], at(plane, m))
+
+    def q_out(plane):
+        return remote(
+            q_ref.at[plane], q_in.at[z], z_send.at[2, plane], z_recv.at[2, z], at(plane, holder(z, m))
+        )
+
+    def came(kind, plane, dst):
+        remote(dst, dst, z_send.at[kind, plane], z_recv.at[kind, plane], at(z, c_member)).wait_recv()
+
+    def in_plane(plane, own):
+        copies = []
+        for t, (mine, everyone) in enumerate(((k_ref, k_all), (v_ref, v_all))):
+            src = mine.at[plane] if own else everyone.at[plane, m]
+            there = everyone.at[plane, m]
+            passed = everyone.at[plane, y_member]
+            copies.append(
+                [
+                    remote(src, there, in_send.at[plane, 0, t], in_recv.at[plane, 0, t], at(z, y_member)),
+                    remote(src, there, in_send.at[plane, 1, t], in_recv.at[plane, 1, t], at(z, c_member)),
+                    remote(passed, passed, in_send.at[plane, 2, t], in_recv.at[plane, 2, t], at(z, c_member)),
+                ]
+            )
+        return copies
+
+    def share(plane, own):
+        for copies in in_plane(plane, own):
+            copies[0].start()
+            copies[1].start()
+
+    def hand_on(plane, own):
+        for copies in in_plane(plane, own):
+            copies[0].wait_recv()
+            copies[2].start()
+
+    def shared(plane, own):
+        for copies in in_plane(plane, own):
+            copies[1].wait_recv()
+            copies[2].wait_recv()
+
+    share(z, True)
+
+    @pl.when(z % 2 == 1)
+    def _():
+        q_out(z).start()
+
+    for plane in order[1:]:
+        k_out(plane).start()
+        v_out(plane).start()
+        q_out(plane).start()
+    k_all[z, m] = k_ref[z]
+    v_all[z, m] = v_ref[z]
+
+    @pl.when(z % 2 == 0)
+    def _():
+        q_in[z] = q_ref[z]
+
+    acc[...] = jnp.zeros_like(acc)
+    total[...] = jnp.zeros_like(total)
+    top[...] = jnp.full_like(top, NEG_LARGE)
+
+    def visit(block, plane, first, count, masked):
+        query = q_in[block]
+        lane = lax.broadcasted_iota(jnp.int32, query.shape, 1)
+        none = jnp.zeros_like(query)
+        both = jnp.concatenate(
+            [jnp.where(lane < hdim, query, none), jnp.where(lane < hdim, none, query)], axis=0
+        )
+        keys = k_all[plane, pl.ds(first, count)].reshape(count * rows, 2 * hdim)
+        values = jnp.concatenate([v_all[plane, first + i] for i in range(count)], axis=1)
+        scores = lax.dot_general(
+            keys, both, (((1,), (1,)), ((), ())), preferred_element_type=jnp.float32
+        )
+        if masked:
+            shift = (first - holder(block, m)) * rows
+            key = lax.broadcasted_iota(jnp.int32, scores.shape, 0)
+            col = lax.broadcasted_iota(jnp.int32, scores.shape, 1)
+            col = jnp.where(col < rows, col, col - rows)
+            scores = jnp.where(key + shift <= col, scores, NEG_LARGE)
+        old = top[block]
+        new = jnp.maximum(old, jnp.max(scores, axis=0, keepdims=True))
+        factor = jnp.exp(old - new)
+        expo = jnp.exp(scores - new)
+        acc[block] = acc[block] * factor + jnp.dot(
+            values, expo.astype(jnp.bfloat16), preferred_element_type=jnp.float32
+        )
+        partial = jnp.sum(expo.reshape(count * rows // 8, 8, 2 * rows), axis=0)
+        total[block] = total[block] * factor + partial
+        top[block] = new
+
+    def diagonal(block):
+        pair = holder(block, m) // 2
+
+        @pl.when(pair > 0)
+        def _():
+            visit(block, block, 0, members // 2, False)
+
+        visit(block, block, pair * (members // 2), members // 2, True)
+
+    def across(a, b):
+        visit(jnp.maximum(a, b), jnp.minimum(a, b), 0, members, False)
+
+    def result_copy(block):
+        return remote(
+            done.at[block], out_ref.at[z], back_send.at[block], back_recv.at[z], at(block, holder(block, m))
+        )
+
+    def at_home(block):
+        return (block == z) & (z % 2 == 0)
+
+    def finish(block):
+        both = acc[block] / jnp.sum(total[block], axis=0, keepdims=True)
+        mixed = both[:, :rows] - lam_ref[z] * both[:, rows:]
+        mean_sq = jnp.mean(mixed * mixed, axis=0, keepdims=True)
+        normed = (mixed * lax.rsqrt(mean_sq + EPSILON)).T * gain_ref[...]
+        done[block] = normed.astype(jnp.bfloat16)
+
+        @pl.when(at_home(block))
+        def _():
+            out_ref[z] = done[block]
+
+        @pl.when(jnp.logical_not(at_home(block)))
+        def _():
+            result_copy(block).start()
+
+    def landed(i):
+        plane = order[i]
+        came(0, plane, k_all.at[plane, m])
+        came(1, plane, v_all.at[plane, m])
+        share(plane, False)
+
+    hand_on(z, True)
+    shared(z, True)
+
+    @pl.when(z % 2 == 1)
+    def _():
+        came(2, z, q_in.at[z])
+
+    for i in range(planes - 1):
+        landed(i + 1)
+        diagonal(order[i])
+        hand_on(order[i + 1], False)
+        for j in range(i):
+            across(order[i], order[j])
+        came(2, order[i + 1], q_in.at[order[i + 1]])
+        shared(order[i + 1], False)
+    late = order[planes - 1]
+    diagonal(late)
+    finish(0)
+    half = z // 2
+
+    def last(s, carry):
+        across(late, s - 1 + half)
+        finish(s)
+        return carry
+
+    lax.fori_loop(1, planes, last, 0)
+
+    for plane in order[1:]:
+        k_out(plane).wait_send()
+        v_out(plane).wait_send()
+        q_out(plane).wait_send()
+
+    @pl.when(z % 2 == 1)
+    def _():
+        q_out(z).wait_send()
+
+    for i in range(planes):
+        for copies in in_plane(order[i], i == 0):
+            for copy in copies:
+                copy.wait_send()
+    for block in range(planes):
+
+        @pl.when(jnp.logical_not(at_home(block)))
+        def _():
+            result_copy(block).wait_send()
+            here = out_ref.at[block]
+            remote(here, here, back_send.at[block], back_recv.at[block], at(z, c_member)).wait_recv()
+
+
+def attend_and_return(queries, keys, values, lambdas, sub_gain):
+    planes, rows, width = queries.shape
+    vdim = values.shape[1]
+    members = lax.axis_size("sp") // planes
+    vmem = pl.BlockSpec(memory_space=pltpu.VMEM)
+    dma = pltpu.SemaphoreType.DMA
+    work = planes * rows * members * planes * rows
+    return pl.pallas_call(
+        functools.partial(mix, width // 2),
+        out_shape=jax.ShapeDtypeStruct((planes, rows, vdim), jnp.bfloat16),
+        in_specs=[pl.BlockSpec(memory_space=pltpu.SMEM), vmem, vmem, vmem, vmem],
+        out_specs=vmem,
+        scratch_shapes=[
+            pltpu.VMEM((planes, rows, width), jnp.bfloat16),
+            pltpu.VMEM((planes, members, rows, width), jnp.bfloat16),
+            pltpu.VMEM((planes, members, vdim, rows), jnp.bfloat16),
+            pltpu.VMEM((planes, vdim, 2 * rows), jnp.float32),
+            pltpu.VMEM((planes, 1, 2 * rows), jnp.float32),
+            pltpu.VMEM((planes, 8, 2 * rows), jnp.float32),
+            pltpu.VMEM((planes, rows, vdim), jnp.bfloat16),
+            dma((3, planes)),
+            dma((3, planes)),
+            dma((planes, 3, 2)),
+            dma((planes, 3, 2)),
+            dma((planes,)),
+            dma((planes,)),
+        ],
+        compiler_params=pltpu.CompilerParams(
+            vmem_limit_bytes=56 * 2**20, collective_id=2, has_side_effects=True
+        ),
+        cost_estimate=pl.CostEstimate(
+            flops=4 * work * vdim, bytes_accessed=keys.size * 8, transcendentals=work
+        ),
+    )(lambdas, queries, keys, values, sub_gain.reshape(1, -1))
+
+
 def trailing(x, window_ids, group_dim):
     column_window = jnp.repeat(window_ids, group_dim)[None, :]
     running = x
@@ -431,6 +697,48 @@
         running = running + jnp.pad(running[:-half], ((half, 0), (0, 0)))
         picked = jnp.where(column_window == slot, running, picked)
     return picked
+
+
+def general_attention(queries, key_rows, values, lambdas, sub_gain):
+    n_sp = lax.axis_size("sp")
+    sp = lax.axis_index("sp")
+    tok_rows = queries.shape[0]
+    heads = lambdas.shape[0]
+    qdim = queries.shape[1] // heads
+    vdim = values.shape[1] // heads
+    head_width = 2 * qdim + vdim
+    outer = math.gcd(n_sp, heads)
+    inner = n_sp // outer
+    per_device = heads // outer
+    by_head = jnp.concatenate(
+        [
+            x.reshape(tok_rows, heads, -1).swapaxes(0, 1)
+            for x in (queries, key_rows, values)
+        ],
+        axis=2,
+    )
+    across = [[o * inner + i for o in range(outer)] for i in range(inner)]
+    within = [[o * inner + i for i in range(inner)] for o in range(outer)]
+    by_head = by_head.reshape(outer, per_device, tok_rows, head_width)
+    if outer > 1:
+        by_head = lax.all_to_all(by_head, "sp", 0, 0, axis_index_groups=across)
+    first_head = lax.div(sp, inner) * per_device
+    attended = []
+    if inner == 4 and per_device == 1:
+        lam = lax.dynamic_slice_in_dim(lambdas, first_head, 1)
+        attended.append(
+            flash_members(by_head[:, 0, :, :qdim], by_head[:, 0, :, qdim:], lam, sub_gain)
+        )
+    else:
+        kv = lax.all_gather(by_head[..., qdim:], "sp", axis=0, axis_index_groups=within)
+        member = lax.rem(sp, inner).reshape(1)
+        for p in range(per_device):
+            lam = lax.dynamic_slice_in_dim(lambdas, first_head + p, 1)
+            attended.append(flash(by_head[:, p, :, :qdim], kv[:, :, p], member, lam, sub_gain))
+    attended = jnp.stack(attended, axis=1)
+    if outer > 1:
+        attended = lax.all_to_all(attended, "sp", 0, 0, axis_index_groups=across)
+    return attended.reshape(heads, tok_rows, vdim)
 
 
 def local(
@@ -457,10 +765,6 @@
     vdim = w_value.shape[1] // heads
     groups = group_weight.shape[0]
     group_dim = group_weight.shape[1]
-    head_width = 2 * qdim + vdim
-    outer = math.gcd(n_sp, heads)
-    inner = n_sp // outer
-    per_device = heads // outer
 
     features = tokens.astype(jnp.float32)
     mine = (features * pre_gain.astype(jnp.float32)[None, :]).astype(jnp.bfloat16)
@@ -488,35 +792,19 @@
         (jnp.dot(scaled, w, preferred_element_type=jnp.float32) * inverse).astype(jnp.bfloat16)
         for w in weights
     ]
-    by_head = jnp.concatenate(
-        [
-            x.reshape(tok_rows, heads, -1).swapaxes(0, 1)
-            for x in (queries, key_rows, values)
-        ],
-        axis=2,
-    )
-    across = [[o * inner + i for o in range(outer)] for i in range(inner)]
-    within = [[o * inner + i for i in range(inner)] for o in range(outer)]
-    by_head = by_head.reshape(outer, per_device, tok_rows, head_width)
-    if outer > 1:
-        by_head = lax.all_to_all(by_head, "sp", 0, 0, axis_index_groups=across)
-    first_head = lax.div(sp, inner) * per_device
-    attended = []
-    if inner == 4 and per_device == 1:
-        lam = lax.dynamic_slice_in_dim(lambdas, first_head, 1)
-        attended.append(
-            flash_members(by_head[:, 0, :, :qdim], by_head[:, 0, :, qdim:], lam, sub_gain)
+    shaped_for_mix = n_tp == 2 and heads == 4 and n_sp == 4 * heads and qdim == vdim
+    if shaped_for_mix:
+        scale = 1.0 / math.sqrt(qdim // 2)
+        by_head = [x.reshape(tok_rows, heads, -1) for x in (queries * scale, key_rows, values)]
+        attended = attend_and_return(
+            by_head[0].swapaxes(0, 1),
+            by_head[1].swapaxes(0, 1),
+            by_head[2].transpose(1, 2, 0),
+            lambdas,
+            sub_gain,
         )
     else:
-        kv = lax.all_gather(by_head[..., qdim:], "sp", axis=0, axis_index_groups=within)
-        member = lax.rem(sp, inner).reshape(1)
-        for p in range(per_device):
-            lam = lax.dynamic_slice_in_dim(lambdas, first_head + p, 1)
-            attended.append(flash(by_head[:, p, :, :qdim], kv[:, :, p], member, lam, sub_gain))
-    attended = jnp.stack(attended, axis=1)
-    if outer > 1:
-        attended = lax.all_to_all(attended, "sp", 0, 0, axis_index_groups=across)
-    attended = attended.reshape(heads, tok_rows, vdim)
+        attended = general_attention(queries, key_rows, values, lambdas, sub_gain)
 
     halo = passed_along(pool_in[tok_rows - RIM_ROWS - 1 :], "sp", 1)
     extended = jnp.concatenate([halo, pool_in], axis=0).astype(jnp.float32)

time: 215 us -> 194 us (0.902)
  waiting for transfers between devices: 68.1 us -> 17.4 us
  Pallas kernels: 90 us -> 128 us
  starting transfers between devices: 13.3 us -> 4.36 us
    all_to_all x2 -> x0, waiting for transfers between devices: 50.6 us -> none  [the longest x1 40.3 us: local(): by_head = lax.all_to_all(by_head, 'sp', 0, 0, axis_index_groups=across)]
    pallas_call x1, Pallas kernels: 35.5 us -> 73.9 us  [attend_and_return(): pl.pallas_call(functools.partial(mix, width // 2), out_shape=jax.ShapeDty...]
    all_to_all x2 -> x0, starting transfers between devices: 8.54 us -> none  [the longest x1 5.07 us: local(): by_head = lax.all_to_all(by_head, 'sp', 0, 0, axis_index_groups=across)]
  transfers between devices with their start and end apart: 6 -> 4, of which waited for: 5 -> 2; matrix products, arithmetic and copies ran while one was open for 8% -> 8% of each run, Pallas kernels for 17% -> 38%
where the time goes in v1:
time: 194 us; the launch traced here: 193 us
  Pallas kernels  128 us (66%)
  matrix products  17.7 us (9%)
  waiting for transfers between devices  17.4 us (9%)
  between operations  13.6 us (7%)
  local copies, waits for them, and re-layouts  7 us (4%)
  other arithmetic  4.85 us (2%)
  starting transfers between devices  4.36 us (2%)
    pallas_call x1, Pallas kernels, attend_and_return(): pl.pallas_call(functools.partial(mix, width // 2), out_shape=jax.ShapeDty...  73.9 us
    pallas_call x1, Pallas kernels, gather_weights(): pl.pallas_call(functools.partial(spread, n_sp, count, with_swap), out_sha...  54.5 us
    ppermute x1, waiting for transfers between devices, local(): got = lax.ppermute(send, 'tp', swap)  17 us
    dot_general x4, matrix products, local(): jnp.dot(scaled, w, preferred_element_type=jnp.float32) * inverse  8.88 us
    dot_general x1, matrix products, local(): keep = jnp.dot(keep, w_out_rows, preferred_element_type=jnp.float32)  4.5 us
  transfers between devices with their start and end apart: 4, of which 2 were waited for; matrix products, arithmetic and copies ran while one was open for 8% of the time, Pallas kernels for 38%

profile of v1, /device:TPU:0, one launch (start us, length us, event | category | flops | bytes accessed | tf_op | source)
XLA Modules:
  0.0 193.3 jit_solution(15193486407343717151)
XLA Ops:
  6.5 0.0 copy-start
  6.5 0.0 all-gather.2.cloned.1.call-start
  6.5 0.7 convert_element_type.57
  7.3 1.7 copy.23
  8.9 2.2 %fusion.1 = (f32[384]{0:T(512)S(1)}, bf16[384,1024]{1,0:T(8,128)(2,1)}) fusion(bf16[384,1024]{1,0:T(8,128)(2,1)} %param.11, f32[1024]{0:T(1024)S(1)} %convert_element_type.57), kind=kLoop, calls=%fused_computation.4 | loop fusion | flops 1965696 | bytes 1578496 | tf_op jit(solution)/shard_map/reduce_sum | solution.py:771
  11.2 0.0 copy-start.1
  11.2 54.5 %shard_map.109 = (bf16[2048,512]{1,0:T(8,128)(2,1)}, bf16[2048,512]{1,0:T(8,128)(2,1)}, bf16[2048,512]{1,0:T(8,128)(2,1)}, bf16[2048,512]{1,0:T(8,128)(2,1)}, bf16[384,1024]{1,0:T(8,128)(2,1)}) custom-call(bf16[128,512]{1,0:T(8,128)(2,1)} %refs_0_.1, bf16[128,512]{1,0:T(8,128)(2,1)} %refs_1_.1, bf16[128,512]{1,0:T(8,128)(2,1)} %refs_2_.1, ...), custom_call_target="tpu_custom_call" | custom-call | flops 10000000000 | bytes 8388608 | tf_op jit(solution)/shard_map/pallas_call | solution.py:403
  65.6 0.0 all-gather.2.cloned.1.call-update
  65.7 1.6 collective-permute-start
  67.3 0.1 broadcast_bitcast_fusion.1
  67.3 0.1 broadcast_bitcast_fusion.2
  67.4 0.1 broadcast_bitcast_fusion.3
  67.5 0.1 broadcast_bitcast_fusion.4
  67.6 0.1 broadcast_bitcast_fusion
  67.6 0.0 copy-done.1
  67.6 1.2 broadcast_select_fusion.1
  68.9 0.4 collective-permute-done
  69.3 0.0 copy-start.3
  69.3 2.7 %fusion.5 = bf16[384,512]{1,0:T(8,128)(2,1)S(1)} fusion(bf16[2048,512]{1,0:T(8,128)(2,1)} %get-tuple-element.23, f32[384]{0:T(512)S(1)} %rsqrt_reduce_fusion, bf16[384,1024]{1,0:T(8,128)(2,1)S(1)} %get-tuple-element.26, bf16[384,1024]{1,0:T(8,128)(2,1)S(1)} %get-tuple-element.25), kind=kOutput, calls=%fused_computation.15 | convolution fusion | flops 808845312 | bytes 4064768 | tf_op jit(solution)/shard_map/dot_general | solution.py:792
  72.1 1.6 collective-permute-start.1
  73.7 0.0 copy-done.3
  73.7 1.0 fusion.4
  74.7 1.0 copy.28
  75.6 2.6 %fusion.3 = bf16[384,512]{1,0:T(8,128)(2,1)S(1)} fusion(bf16[2048,512]{1,0:T(8,128)(2,1)} %get-tuple-element.21, f32[384]{0:T(512)S(1)} %rsqrt_reduce_fusion, bf16[384,1024]{1,0:T(8,128)(2,1)S(1)} %get-tuple-element.26, bf16[384,1024]{1,0:T(8,128)(2,1)S(1)} %get-tuple-element.25), kind=kOutput, calls=%fused_computation.13 | convolution fusion | flops 808845312 | bytes 4064768 | tf_op jit(solution)/shard_map/dot_general | solution.py:792
  78.2 0.2 copy.26
  78.5 0.9 copy.27
  79.4 2.6 %fusion.7 = bf16[384,512]{1,0:T(8,128)(2,1)S(1)} fusion(bf16[2048,512]{1,0:T(8,128)(2,1)} %get-tuple-element.20, f32[384]{0:T(512)S(1)} %rsqrt_reduce_fusion, bf16[384,1024]{1,0:T(8,128)(2,1)S(1)} %get-tuple-element.26, bf16[384,1024]{1,0:T(8,128)(2,1)S(1)} %get-tuple-element.25), kind=kOutput, calls=%fused_computation.17 | convolution fusion | flops 809041920 | bytes 4064768 | tf_op jit(solution)/shard_map/dot_general | solution.py:792
  82.0 0.2 copy.24
  82.2 0.9 copy.25
  83.1 73.9 %shard_map.110 = bf16[4,384,128]{2,1,0:T(8,128)(2,1)} custom-call(f32[4]{0:T(128)} %lam_ref.1, bf16[4,384,128]{2,1,0:T(8,128)(2,1)} %bitcast.55, bf16[4,384,128]{2,1,0:T(8,128)(2,1)} %bitcast.54, bf16[4,128,384]{2,1,0:T(8,128)(2,1)} %bitcast.53, f32[1,128]{1,0:T(1,128)} %bitcast.59), custom_call_target="tpu_custom_call" | custom-call | flops 4831838208 | bytes 1572864 | tf_op jit(solution)/shard_map/pallas_call | solution.py:662
  157.1 1.2 copy.29
  158.3 0.0 collective-permute-done.1
  158.3 0.1 maximum_convert_fusion
  158.4 0.2 pad_add_fusion.2
  158.6 0.2 pad_add_fusion.1
  158.7 0.0 copy-start.2
  158.7 0.2 pad_add_fusion
  158.9 0.1 slice.28
  159.0 0.0 copy-done
  159.0 0.4 copy-done.2
  159.4 0.7 fusion.6
  160.1 0.0 all-gather.2.cloned.1.call-done
  160.2 3.6 %convolution_convert_fusion = bf16[192,2048]{1,0:T(8,128)(2,1)S(1)} fusion(bf16[1024,2048]{1,0:T(8,128)(2,1)} %all-gather.2.cloned.1.call-done, s32[]{:T(128)S(6)} %select_n.47, bf16[384,512]{0,1:T(8,128)(2,1)S(1)} %bitcast.51, bf16[384,512]{0,1:T(8,128)(2,1)S(1)} %bitcast.60), kind=kOutput, calls=%fused_computation | convolution fusion | flops 806486016 | bytes 5767172 | tf_op jit(solution)/shard_map/dot_general | solution.py:830
  163.8 1.2 collective-permute-start.2
  165.0 17.0 %collective-permute-done.2 = bf16[192,2048]{1,0:T(8,128)(2,1)S(1)} collective-permute-done((bf16[192,2048]{1,0:T(8,128)(2,1)S(1)}, bf16[192,2048]{1,0:T(8,128)(2,1)S(1)}, u32[]{:S(2)}, u32[]{:S(2)}) %collective-permute-start.2) | collective-permute-done | bytes 786464 | tf_op jit(solution)/shard_map/ppermute | solution.py:831
  182.0 4.5 %add_convert_fusion = bf16[192,2048]{1,0:T(8,128)(2,1)} fusion(bf16[192,2048]{1,0:T(8,128)(2,1)S(1)} %collective-permute-done.2, bf16[1024,2048]{1,0:T(8,128)(2,1)} %all-gather.2.cloned.1.call-done, s32[]{:T(128)S(6)} %select_n.46, bf16[384,512]{0,1:T(8,128)(2,1)S(1)} %bitcast.52, bf16[384,512]{0,1:T(8,128)(2,1)S(1)} %bitcast.61), kind=kOutput, calls=%fused_computation.6 | convolution fusion | flops 807272448 | bytes 6553604 | tf_op jit(solution)/shard_map/dot_general | solution.py:833
  (7 shorter events, 0.1 us)
Async XLA Ops:
  6.5 152.5 %copy-start = (bf16[4,128,128]{2,1,0:T(8,128)(2,1)S(1)}, bf16[4,128,128]{2,1,0:T(8,128)(2,1)}, u32[]{:S(2)}) copy-start(bf16[4,128,128]{2,1,0:T(8,128)(2,1)} %param.19) | copy-start | bytes 393220
  6.5 153.6 %all-gather.2.cloned.1.call-start = ((), (), s32[]{:S(2)}) async-start(), calls=%async_computation | async-start | bytes 4456448 | tf_op jit(solution)/shard_map/all_gather | solution.py:781
  11.2 56.5 %copy-start.1 = (bf16[384,1024]{1,0:T(8,128)(2,1)S(1)}, bf16[384,1024]{1,0:T(8,128)(2,1)}, u32[]{:S(2)}) copy-start(bf16[384,1024]{1,0:T(8,128)(2,1)} %get-tuple-element.28.refs_4_) | copy-start | bytes 2359300
  65.7 3.6 %collective-permute-start = (f32[384,1]{0,1:T(1,128)S(1)}, f32[384,1]{0,1:T(1,128)S(1)}, u32[]{:S(2)}, u32[]{:S(2)}) collective-permute-start(f32[384,1]{0,1:T(1,128)S(1)} %broadcast_in_dim.43), channel_id=1, source_target_pairs={{0,1},{1,0},{2,3},{3,2},{4,5},{5,4},{6,7},{7,6},{8,9},{9,8},{10,11... | collective-permute-start | bytes 4616 | tf_op jit(solution)/shard_map/ppermute | solution.py:783
  69.3 4.4 %copy-start.3 = (bf16[2048,512]{1,0:T(8,128)(2,1)S(1)}, bf16[2048,512]{1,0:T(8,128)(2,1)}, u32[]{:S(2)}) copy-start(bf16[2048,512]{1,0:T(8,128)(2,1)} %get-tuple-element.22) | copy-start | bytes 6291460
  72.1 86.2 %collective-permute-start.1 = (bf16[16,512]{1,0:T(8,128)(2,1)S(1)}, bf16[16,512]{1,0:T(8,128)(2,1)S(1)}, u32[]{:S(2)}, u32[]{:S(2)}) collective-permute-start(bf16[16,512]{1,0:T(8,128)(2,1)S(1)} %slice.24), channel_id=1, source_target_pairs={{0,2},{2,4},{4,6},{6,8},{8,10},{10,12},{12,14},{14,16},{16,18},{18... | collective-permute-start | bytes 49160 | tf_op jit(solution)/shard_map/ppermute | solution.py:20
  158.7 0.7 copy-start.2
  163.8 18.2 %collective-permute-start.2 = (bf16[192,2048]{1,0:T(8,128)(2,1)S(1)}, bf16[192,2048]{1,0:T(8,128)(2,1)S(1)}, u32[]{:S(2)}, u32[]{:S(2)}) collective-permute-start(bf16[192,2048]{1,0:T(8,128)(2,1)S(1)} %convolution_convert_fusion), channel_id=1, source_target_pairs={{0,1},{1,0},{2,3},{3,2},{4,5},{5,4},{6,7},{7,6},{8,9},{9,8},{10,11... | collective-permute-start | bytes 2359304 | tf_op jit(solution)/shard_map/ppermute | solution.py:831
Sparse Core Ops, SparseCore 0:
  65.8 69.9 all-gather.1

commit v2 on v1

--- a/solution.py
+++ b/solution.py
@@ -425,6 +425,281 @@
 def arrival(z, i):
     half = z // 2
     return (z, 1 + 4 * half - z, 2 - half, 3 - 3 * half)[i]
+
+
+def project(
+    hdim,
+    model_width,
+    tok_ref,
+    gain_ref,
+    wq_ref,
+    wk_ref,
+    wv_ref,
+    q_out,
+    k_out,
+    v_out,
+    scaled_out,
+    inverse_out,
+    full,
+    theirs,
+    their_gain,
+    pieces,
+    acc,
+    *sems,
+):
+    (line_send, line_recv, y_send, y_recv, c_send, c_recv, turn_send, turn_recv, swap_sem) = sems
+    weights = (wq_ref, wk_ref, wv_ref)
+    arrays = range(len(weights))
+    rows, columns = wq_ref.shape
+    tok_rows, half_width = tok_ref.shape
+    planes = q_out.shape[0]
+    members = lax.axis_size("sp") // planes
+    sp = lax.axis_index("sp")
+    tp = lax.axis_index("tp")
+    z = sp // members
+    y = (sp % members) // 2
+    c = sp % 2
+    y_peer = {"sp": sp + 2 - 4 * y}
+    c_peer = {"sp": sp + 1 - 2 * c}
+    x_peer = {"tp": 1 - tp}
+    order = [arrival(z, i) for i in range(planes)]
+    partner = {"sp": order[1] * members + sp % members}
+
+    barrier = pltpu.get_barrier_semaphore()
+
+    def greet(device):
+        pl.semaphore_signal(barrier, 1, device_id=device, device_id_type=pl.DeviceIdType.MESH)
+
+    for device in (y_peer, c_peer, x_peer):
+        greet(device)
+
+    @pl.when(z > 0)
+    def _():
+        greet({"sp": sp - members})
+
+    @pl.when(z < planes - 1)
+    def _():
+        greet({"sp": sp + members})
+
+    pl.semaphore_wait(barrier, 3 + jnp.where(z > 0, 1, 0) + jnp.where(z < planes - 1, 1, 0))
+
+    def remote(src, dst, send, recv, device):
+        return pltpu.make_async_remote_copy(
+            src_ref=src,
+            dst_ref=dst,
+            send_sem=send,
+            recv_sem=recv,
+            device_id=device,
+            device_id_type=pl.DeviceIdType.MESH,
+        )
+
+    def slot(a, zz, yy, cc, first=0, count=rows):
+        start = pl.multiple_of((zz * members + yy * 2 + cc) * rows + first, count)
+        return full.at[a, pl.ds(start, count), :]
+
+    def line(a, zz, up, own):
+        there = slot(a, zz, y, c)
+        side = 1 if up else 0
+        return remote(
+            weights[a] if own else there,
+            there,
+            line_send.at[zz, side, a],
+            line_recv.at[zz, a],
+            {"sp": sp + (members if up else -members)},
+        )
+
+    def y_copy(a, i, own):
+        if i == 1:
+            there = slot(a, order[i], y, c, rows // 2, rows // 2)
+            src = there
+        else:
+            there = slot(a, order[i], y, c)
+            src = weights[a] if own else there
+        return remote(src, there, y_send.at[order[i], a], y_recv.at[order[i], a], y_peer)
+
+    def y_came(a, i):
+        there = slot(a, order[i], 1 - y, c, *((rows // 2, rows // 2) if i == 1 else ()))
+        return remote(there, there, y_send.at[order[i], a], y_recv.at[order[i], a], y_peer)
+
+    def turn(a):
+        there = slot(a, z, 1 - y, c, 0, rows // 2)
+        return remote(there, there, turn_send.at[a], turn_recv.at[a], partner)
+
+    def turned(a):
+        there = slot(a, order[1], 1 - y, c, 0, rows // 2)
+        return remote(there, there, turn_send.at[a], turn_recv.at[a], partner)
+
+    def c_copy(a, zz, yy, own):
+        there = slot(a, zz, yy, c)
+        src = weights[a] if own else there
+        return remote(src, there, c_send.at[zz, yy, a], c_recv.at[zz, yy, a], c_peer)
+
+    def c_came(a, zz, yy):
+        there = slot(a, zz, yy, 1 - c)
+        return remote(there, there, c_send.at[zz, yy, a], c_recv.at[zz, yy, a], c_peer)
+
+    swaps = (
+        remote(tok_ref, theirs, swap_sem.at[0], swap_sem.at[1], x_peer),
+        remote(gain_ref, their_gain, swap_sem.at[2], swap_sem.at[3], x_peer),
+    )
+    for a in arrays:
+
+        @pl.when(z < planes - 1)
+        def _():
+            line(a, z, True, True).start()
+
+        @pl.when(z > 0)
+        def _():
+            line(a, z, False, True).start()
+
+        y_copy(a, 0, True).start()
+        if a == 0:
+            for swap in swaps:
+                swap.start()
+    for a in arrays:
+        c_copy(a, z, y, True).start()
+        full[a, pl.ds(pl.multiple_of(sp * rows, rows), rows), :] = weights[a][...]
+
+    def from_line(i):
+        zz = order[i]
+        for a in arrays:
+            there = slot(a, zz, y, c)
+            remote(there, there, line_send.at[zz, 0, a], line_recv.at[zz, a], c_peer).wait_recv()
+
+            @pl.when((zz < z) & (z < planes - 1))
+            def _():
+                line(a, zz, True, False).start()
+
+            @pl.when((zz > z) & (z > 0))
+            def _():
+                line(a, zz, False, False).start()
+
+            y_copy(a, i, False).start()
+            c_copy(a, zz, y, False).start()
+
+    def from_pair(i):
+        zz = order[i]
+        for a in arrays:
+            y_came(a, i).wait_recv()
+            if i == 0:
+                turn(a).start()
+            if i == 1:
+                turned(a).wait_recv()
+            c_copy(a, zz, 1 - y, False).start()
+
+    def multiply(zz, yy, first=False):
+        for a in arrays:
+            c_came(a, zz, yy).wait_recv()
+        piece = zz * 2 + yy
+        start = pl.multiple_of(piece * 2 * rows, 2 * rows)
+        for a in arrays:
+            part = jnp.dot(
+                pieces[piece], full[a, pl.ds(start, 2 * rows), :], preferred_element_type=jnp.float32
+            )
+            if first:
+                acc[a] = part
+            else:
+                acc[a] += part
+
+    from_line(1)
+    from_pair(0)
+    from_line(2)
+    for swap in swaps:
+        swap.wait()
+    squares = jnp.zeros((tok_rows, 1), jnp.float32)
+    per_half = half_width // (2 * rows)
+    for ref, gains, owner in ((tok_ref, gain_ref, tp), (theirs, their_gain, 1 - tp)):
+        for j in range(per_half):
+            chunk = pl.ds(j * 2 * rows, 2 * rows)
+            features = ref[:, chunk].astype(jnp.float32)
+            squares += jnp.sum(features * features, axis=1, keepdims=True)
+            scaled = (features * gains[:, chunk].astype(jnp.float32)).astype(jnp.bfloat16)
+            pieces[owner * per_half + j] = scaled
+    inverse = lax.rsqrt(squares / model_width + EPSILON)
+    inverse_out[...] = jnp.broadcast_to(inverse, inverse_out.shape)
+    multiply(order[0], y, True)
+    multiply(order[0], 1 - y)
+    from_line(3)
+    from_pair(1)
+    multiply(order[1], y)
+    from_pair(2)
+    multiply(order[1], 1 - y)
+    for j in range(2 * per_half):
+        scaled_out[:, j * 2 * rows : (j + 1) * 2 * rows] = pieces[j]
+    multiply(order[2], y)
+    multiply(order[2], 1 - y)
+    from_pair(3)
+    multiply(order[3], y)
+    multiply(order[3], 1 - y)
+    width = columns // planes
+    scale = 1.0 / math.sqrt(hdim)
+    for p in range(planes):
+        part = slice(p * width, (p + 1) * width)
+        q_out[p] = (acc[0, :, part] * inverse).astype(jnp.bfloat16) * scale
+        k_out[p] = (acc[1, :, part] * inverse).astype(jnp.bfloat16)
+        v_out[p] = (acc[2, :, part] * inverse).T.astype(jnp.bfloat16)
+
+    for a in arrays:
+        for i in range(planes):
+            zz = order[i]
+            y_copy(a, i, i == 0).wait_send()
+            c_copy(a, zz, y, i == 0).wait_send()
+            c_copy(a, zz, 1 - y, False).wait_send()
+
+            @pl.when((zz <= z) & (z < planes - 1))
+            def _():
+                line(a, zz, True, i == 0).wait_send()
+
+            @pl.when((zz >= z) & (z > 0))
+            def _():
+                line(a, zz, False, i == 0).wait_send()
+
+        turn(a).wait_send()
+
+
+def gather_and_project(tokens, pre_gain, w_query, w_key, w_value, heads):
+    tok_rows, half_width = tokens.shape
+    n_sp = lax.axis_size("sp")
+    rows, columns = w_query.shape
+    width = columns // heads
+    full_width = n_sp * rows
+    vmem = pl.BlockSpec(memory_space=pltpu.VMEM)
+    dma = pltpu.SemaphoreType.DMA
+    by_head = jax.ShapeDtypeStruct((heads, tok_rows, width), jnp.bfloat16)
+    return pl.pallas_call(
+        functools.partial(project, width // 2, full_width),
+        out_shape=[
+            by_head,
+            by_head,
+            jax.ShapeDtypeStruct((heads, width, tok_rows), jnp.bfloat16),
+            jax.ShapeDtypeStruct((tok_rows, full_width), jnp.bfloat16),
+            jax.ShapeDtypeStruct((tok_rows, 128), jnp.float32),
+        ],
+        in_specs=[vmem] * 5,
+        out_specs=[vmem] * 5,
+        scratch_shapes=[
+            pltpu.VMEM((3, full_width, columns), jnp.bfloat16),
+            pltpu.VMEM((tok_rows, half_width), jnp.bfloat16),
+            pltpu.VMEM((1, half_width), jnp.bfloat16),
+            pltpu.VMEM((full_width // (2 * rows), tok_rows, 2 * rows), jnp.bfloat16),
+            pltpu.VMEM((3, tok_rows, columns), jnp.float32),
+            dma((heads, 2, 3)),
+            dma((heads, 3)),
+            dma((heads, 3)),
+            dma((heads, 3)),
+            dma((heads, 2, 3)),
+            dma((heads, 2, 3)),
+            dma((3,)),
+            dma((3,)),
+            dma((4,)),
+        ],
+        compiler_params=pltpu.CompilerParams(
+            vmem_limit_bytes=56 * 2**20, collective_id=3, has_side_effects=True
+        ),
+        cost_estimate=pl.CostEstimate(
+            flops=6 * tok_rows * full_width * columns, bytes_accessed=2**23, transcendentals=0
+        ),
+    )(tokens, pre_gain.reshape(1, -1), w_query, w_key, w_value)
 
 
 def mix(hdim, lam_ref, q_ref, k_ref, v_ref, gain_ref, out_ref, q_in, k_all, v_all, acc, top, total, done, *sems):
@@ -766,44 +1041,43 @@
     groups = group_weight.shape[0]
     group_dim = group_weight.shape[1]
 
-    features = tokens.astype(jnp.float32)
-    mine = (features * pre_gain.astype(jnp.float32)[None, :]).astype(jnp.bfloat16)
-    squares = jnp.sum(features * features, axis=1, keepdims=True)
     swap = [(0, 1), (1, 0)]
-    weights = [w_query, w_key, w_value, w_pool]
-    if n_sp % 4 == 0:
-        *weights, theirs = gather_weights(weights, mine, n_tp == 2)
+    shaped_for_mix = n_tp == 2 and heads == 4 and n_sp == 4 * heads and qdim == vdim
+    w_sorted = w_out.reshape(heads, 2, vdim, -1).swapaxes(0, 1).reshape(w_out.shape)
+    if shaped_for_mix:
+        w_pool_rows = lax.all_gather(w_pool, "sp", axis=0, tiled=True)
+        w_out_rows = lax.all_gather(w_sorted, "sp", axis=1, tiled=True)
+        queries, key_rows, values, scaled, inverse = gather_and_project(
+            tokens, pre_gain, w_query, w_key, w_value, heads
+        )
+        attended = attend_and_return(queries, key_rows, values, lambdas, sub_gain)
+        pool_in = jnp.dot(scaled, w_pool_rows, preferred_element_type=jnp.float32)
+        pool_in = (pool_in * inverse[:, :1]).astype(jnp.bfloat16)
     else:
-        weights = [lax.all_gather(w, "sp", axis=0, tiled=True) for w in weights]
-        theirs = lax.ppermute(mine, "tp", swap) if n_tp == 2 else mine
-    w_sorted = w_out.reshape(heads, 2, vdim, -1).swapaxes(0, 1).reshape(w_out.shape)
-    w_sorted, weights = lax.optimization_barrier((w_sorted, weights))
-    w_out_rows = lax.all_gather(w_sorted, "sp", axis=1, tiled=True)
-    if n_tp == 2:
-        squares = squares + lax.ppermute(squares, "tp", swap)
-        scaled = jnp.concatenate(
-            [jnp.where(tp == 0, mine, theirs), jnp.where(tp == 0, theirs, mine)], axis=1
-        )
-    else:
-        scaled = lax.all_gather(mine, "tp", axis=1, tiled=True)
-        squares = lax.psum(squares, "tp")
-    inverse = lax.rsqrt(squares / model_width + EPSILON)
-    queries, key_rows, values, pool_in = [
-        (jnp.dot(scaled, w, preferred_element_type=jnp.float32) * inverse).astype(jnp.bfloat16)
-        for w in weights
-    ]
-    shaped_for_mix = n_tp == 2 and heads == 4 and n_sp == 4 * heads and qdim == vdim
-    if shaped_for_mix:
-        scale = 1.0 / math.sqrt(qdim // 2)
-        by_head = [x.reshape(tok_rows, heads, -1) for x in (queries * scale, key_rows, values)]
-        attended = attend_and_return(
-            by_head[0].swapaxes(0, 1),
-            by_head[1].swapaxes(0, 1),
-            by_head[2].transpose(1, 2, 0),
-            lambdas,
-            sub_gain,
-        )
-    else:
+        features = tokens.astype(jnp.float32)
+        mine = (features * pre_gain.astype(jnp.float32)[None, :]).astype(jnp.bfloat16)
+        squares = jnp.sum(features * features, axis=1, keepdims=True)
+        weights = [w_query, w_key, w_value, w_pool]
+        if n_sp % 4 == 0:
+            *weights, theirs = gather_weights(weights, mine, n_tp == 2)
+        else:
+            weights = [lax.all_gather(w, "sp", axis=0, tiled=True) for w in weights]
+            theirs = lax.ppermute(mine, "tp", swap) if n_tp == 2 else mine
+        w_sorted, weights = lax.optimization_barrier((w_sorted, weights))
+        w_out_rows = lax.all_gather(w_sorted, "sp", axis=1, tiled=True)
+        if n_tp == 2:
+            squares = squares + lax.ppermute(squares, "tp", swap)
+            scaled = jnp.concatenate(
+                [jnp.where(tp == 0, mine, theirs), jnp.where(tp == 0, theirs, mine)], axis=1
+            )
+        else:
+            scaled = lax.all_gather(mine, "tp", axis=1, tiled=True)
+            squares = lax.psum(squares, "tp")
+        inverse = lax.rsqrt(squares / model_width + EPSILON)
+        queries, key_rows, values, pool_in = [
+            (jnp.dot(scaled, w, preferred_element_type=jnp.float32) * inverse).astype(jnp.bfloat16)
+            for w in weights
+        ]
         attended = general_attention(queries, key_rows, values, lambdas, sub_gain)
 
     halo = passed_along(pool_in[tok_rows - RIM_ROWS - 1 :], "sp", 1)

time: 194 us -> 189 us (0.974)
  matrix products: 17.7 us -> 11.4 us
  Pallas kernels: 128 us -> 134 us
  other arithmetic: 4.85 us -> 0.63 us
  waiting for transfers between devices: 17.4 us -> 19.9 us
    dot_general x4 -> x1, matrix products: 8.88 us -> 2.61 us  [local(): pool_in = jnp.dot(scaled, w_pool_rows, preferred_element_type=jnp.float32)]
    pallas_call x1, Pallas kernels: 73.9 us -> 76.8 us  [attend_and_return(): pl.pallas_call(functools.partial(mix, width // 2), out_shape=jax.ShapeDty...]
    pallas_call x1, Pallas kernels: 54.5 us -> 57 us  [gather_and_project(): pl.pallas_call(functools.partial(project, width // 2, full_width), out_sh...]
    reduce_sum x1 -> x0, other arithmetic: 2.24 us -> none  [local(): squares = jnp.sum(features * features, axis=1, keepdims=True)]
  transfers between devices with their start and end apart: 4 -> 4, of which waited for: 2 -> 2; matrix products, arithmetic and copies ran while one was open for 8% -> 5% of each run, Pallas kernels for 38% -> 71%
where the time goes in v2:
time: 189 us; the launch traced here: 187 us
  Pallas kernels  134 us (71%)
  waiting for transfers between devices  19.9 us (11%)
  between operations  13.6 us (7%)
  matrix products  11.4 us (6%)
  local copies, waits for them, and re-layouts  5.09 us (3%)
  starting transfers between devices  3.1 us (2%)
    pallas_call x1, Pallas kernels, attend_and_return(): pl.pallas_call(functools.partial(mix, width // 2), out_shape=jax.ShapeDty...  76.8 us
    pallas_call x1, Pallas kernels, gather_and_project(): pl.pallas_call(functools.partial(project, width // 2, full_width), out_sh...  57 us
    ppermute x1, waiting for transfers between devices, local(): got = lax.ppermute(send, 'tp', swap)  18.8 us
    dot_general x1, matrix products, local(): keep = jnp.dot(keep, w_out_rows, preferred_element_type=jnp.float32)  4.51 us
  transfers between devices with their start and end apart: 4, of which 2 were waited for; matrix products, arithmetic and copies ran while one was open for 5% of the time, Pallas kernels for 71%

profile of v2, /device:TPU:0, one launch (start us, length us, event | category | flops | bytes accessed | tf_op | source)
XLA Modules:
  0.0 187.4 jit_solution(13299570342677887896)
XLA Ops:
  6.5 0.0 copy-start
  6.5 0.0 all-gather.3.cloned.1.call-start
  6.5 0.7 all-gather.3.cloned.1.call-update
  7.3 0.0 all-gather.5.cloned.1.call-start
  7.3 1.7 copy.20
  9.0 0.0 all-gather.5.cloned.1.call-update
  9.0 1.3 reshape.65.gain_ref
  10.3 57.0 %shard_map.109 = (bf16[4,384,128]{2,1,0:T(8,128)(2,1)}, bf16[4,384,128]{2,1,0:T(8,128)(2,1)}, bf16[4,128,384]{2,1,0:T(8,128)(2,1)}, bf16[384,2048]{1,0:T(8,128)(2,1)}, f32[384,128]{1,0:T(8,128)}) custom-call(bf16[384,1024]{1,0:T(8,128)(2,1)} %tok_ref.1, bf16[1,1024]{1,0:T(2,128)(2,1)} %reshape.65.gain_ref, bf16[128,512]{1,0:T(8,128)(2,1)} %wq_ref.1, ...), custom_call_target="tpu_custom_call" | custom-call | flops 2415919104 | bytes 8388608 | tf_op jit(solution)/shard_map/pallas_call | solution.py:669
  67.3 1.1 slice_reduce_fusion
  68.4 0.1 broadcast_bitcast_fusion.1
  68.4 0.1 broadcast_bitcast_fusion.2
  68.5 0.1 broadcast_bitcast_fusion.3
  68.6 0.1 broadcast_bitcast_fusion.4
  68.6 0.1 broadcast_bitcast_fusion
  68.7 0.0 copy-start.3
  68.7 76.8 %shard_map.110 = bf16[4,384,128]{2,1,0:T(8,128)(2,1)} custom-call(f32[4]{0:T(128)} %lam_ref.1, bf16[4,384,128]{2,1,0:T(8,128)(2,1)} %get-tuple-element.10.q_ref, bf16[4,384,128]{2,1,0:T(8,128)(2,1)} %get-tuple-element.11.k_ref, bf16[4,128,384]{2,1,0:T(8,128)(2,1)} %get-tuple-element.12.v_ref, f32[1,128]{1,0:T(1,128)} %bitcast.45), custom_call_target="tpu_custom_call" | custom-call | flops 4831838208 | bytes 1572864 | tf_op jit(solution)/shard_map/pallas_call | solution.py:937
  145.5 0.0 all-gather.3.cloned.1.call-done
  145.5 0.0 copy-done.3
  145.5 0.0 copy-start.1
  145.5 2.6 %fusion = bf16[384,512]{1,0:T(8,128)(2,1)S(1)} fusion(bf16[384,2048]{1,0:T(8,128)(2,1)S(1)} %copy-done.3, bf16[2048,512]{1,0:T(8,128)(2,1)} %all-gather.3.cloned.1.call-done, f32[384]{0:T(512)S(1)} %slice_reduce_fusion), kind=kOutput, calls=%fused_computation.4 | convolution fusion | flops 805699584 | bytes 4064768 | tf_op jit(solution)/shard_map/dot_general | solution.py:1054
  148.2 1.5 collective-permute-start
  149.7 0.0 copy-done.1
  149.7 0.2 copy.17
  149.9 0.3 collective-permute-done
  150.3 0.1 maximum_convert_fusion
  150.4 0.2 pad_add_fusion.2
  150.5 0.2 pad_add_fusion.1
  150.7 0.0 copy-start.2
  150.7 0.2 pad_add_fusion
  150.9 0.1 slice.32
  151.0 0.0 copy-done
  151.0 0.4 copy-done.2
  151.4 0.7 fusion.1
  152.1 0.0 all-gather.5.cloned.1.call-done
  152.2 3.6 %convolution_convert_fusion = bf16[192,2048]{1,0:T(8,128)(2,1)S(1)} fusion(bf16[1024,2048]{1,0:T(8,128)(2,1)} %all-gather.5.cloned.1.call-done, s32[]{:T(128)S(6)} %select_n.32, bf16[384,512]{0,1:T(8,128)(2,1)S(1)} %bitcast.40, bf16[384,512]{0,1:T(8,128)(2,1)S(1)} %bitcast.46), kind=kOutput, calls=%fused_computation | convolution fusion | flops 806486016 | bytes 5767172 | tf_op jit(solution)/shard_map/dot_general | solution.py:1104
  155.8 1.5 collective-permute-start.1
  157.3 18.8 %collective-permute-done.1 = bf16[192,2048]{1,0:T(8,128)(2,1)S(1)} collective-permute-done((bf16[192,2048]{1,0:T(8,128)(2,1)S(1)}, bf16[192,2048]{1,0:T(8,128)(2,1)S(1)}, u32[]{:S(2)}, u32[]{:S(2)}) %collective-permute-start.1) | collective-permute-done | bytes 786464 | tf_op jit(solution)/shard_map/ppermute | solution.py:1105
  176.1 4.5 %add_convert_fusion = bf16[192,2048]{1,0:T(8,128)(2,1)} fusion(bf16[192,2048]{1,0:T(8,128)(2,1)S(1)} %collective-permute-done.1, bf16[1024,2048]{1,0:T(8,128)(2,1)} %all-gather.5.cloned.1.call-done, s32[]{:T(128)S(6)} %select_n.31, bf16[384,512]{0,1:T(8,128)(2,1)S(1)} %bitcast.41, bf16[384,512]{0,1:T(8,128)(2,1)S(1)} %bitcast.47), kind=kOutput, calls=%fused_computation.1 | convolution fusion | flops 807272448 | bytes 6553604 | tf_op jit(solution)/shard_map/dot_general | solution.py:1107
  (5 shorter events, 0.0 us)
Async XLA Ops:
  6.5 144.4 %copy-start = (bf16[4,128,128]{2,1,0:T(8,128)(2,1)S(1)}, bf16[4,128,128]{2,1,0:T(8,128)(2,1)}, u32[]{:S(2)}) copy-start(bf16[4,128,128]{2,1,0:T(8,128)(2,1)} %param.19) | copy-start | bytes 393220
  6.5 139.0 %all-gather.3.cloned.1.call-start = ((), (), s32[]{:S(2)}) async-start(), calls=%async_computation | async-start | bytes 2228224 | tf_op jit(solution)/shard_map/all_gather | solution.py:1048
  7.3 144.9 %all-gather.5.cloned.1.call-start = ((), (), s32[]{:S(2)}) async-start(), calls=%async_computation.1 | async-start | bytes 4456448 | tf_op jit(solution)/shard_map/all_gather | solution.py:1049
  68.7 76.8 %copy-start.3 = (bf16[384,2048]{1,0:T(8,128)(2,1)S(1)}, bf16[384,2048]{1,0:T(8,128)(2,1)}, u32[]{:S(2)}) copy-start(bf16[384,2048]{1,0:T(8,128)(2,1)} %get-tuple-element.13) | copy-start | bytes 4718596
  145.5 4.2 %copy-start.1 = (bf16[4,384,128]{2,1,0:T(8,128)(2,1)S(1)}, bf16[4,384,128]{2,1,0:T(8,128)(2,1)}, u32[]{:S(2)}) copy-start(bf16[4,384,128]{2,1,0:T(8,128)(2,1)} %shard_map.110) | copy-start | bytes 1179652
  148.2 2.1 %collective-permute-start = (bf16[16,512]{1,0:T(8,128)(2,1)S(1)}, bf16[16,512]{1,0:T(8,128)(2,1)S(1)}, u32[]{:S(2)}, u32[]{:S(2)}) collective-permute-start(bf16[16,512]{1,0:T(8,128)(2,1)S(1)} %slice.28), channel_id=1, source_target_pairs={{0,2},{2,4},{4,6},{6,8},{8,10},{10,12},{12,14},{14,16},{16,18},{18... | collective-permute-start | bytes 49160 | tf_op jit(solution)/shard_map/ppermute | solution.py:20
  150.7 0.7 copy-start.2
  155.8 20.3 %collective-permute-start.1 = (bf16[192,2048]{1,0:T(8,128)(2,1)S(1)}, bf16[192,2048]{1,0:T(8,128)(2,1)S(1)}, u32[]{:S(2)}, u32[]{:S(2)}) collective-permute-start(bf16[192,2048]{1,0:T(8,128)(2,1)S(1)} %convolution_convert_fusion), channel_id=1, source_target_pairs={{0,1},{1,0},{2,3},{3,2},{4,5},{5,4},{6,7},{7,6},{8,9},{9,8},{10,11... | collective-permute-start | bytes 2359304 | tf_op jit(solution)/shard_map/ppermute | solution.py:1105
Sparse Core Ops, SparseCore 0:
  9.5 50.6 all-gather.2
  62.3 71.3 all-gather.4

commit v3 on v2

--- a/solution.py
+++ b/solution.py
@@ -12,6 +12,7 @@
 NEG_LARGE = -1e30
 WINDOWS = (2, 4, 8, 16)
 RIM_ROWS = 15
+LINE_STAGE = 2
 
 
 def passed_along(block, axis, distance):
@@ -424,7 +425,8 @@
 
 def arrival(z, i):
     half = z // 2
-    return (z, 1 + 4 * half - z, 2 - half, 3 - 3 * half)[i]
+    later = jnp.where(i == 2, 2 - half, 3 - 3 * half)
+    return jnp.where(i == 0, z, jnp.where(i == 1, 1 + 4 * half - z, later))
 
 
 def project(
@@ -435,11 +437,13 @@
     wq_ref,
     wk_ref,
     wv_ref,
+    wp_ref,
     q_out,
     k_out,
     v_out,
     scaled_out,
     inverse_out,
+    pool_out,
     full,
     theirs,
     their_gain,
@@ -447,7 +451,7 @@
     acc,
     *sems,
 ):
-    (line_send, line_recv, y_send, y_recv, c_send, c_recv, turn_send, turn_recv, swap_sem) = sems
+    (line_send, line_recv, y_send, y_recv, c_send, c_recv, turn_send, turn_recv, swap_sem, pool_send, pool_recv) = sems
     weights = (wq_ref, wk_ref, wv_ref)
     arrays = range(len(weights))
     rows, columns = wq_ref.shape
@@ -600,6 +604,41 @@
                 acc[a] = part
             else:
                 acc[a] += part
+
+    def pool_line(zz, up, own):
+        there = pool_out.at[zz]
+        side = 1 if up else 0
+        return remote(
+            wp_ref if own else there,
+            there,
+            pool_send.at[zz, side],
+            pool_recv.at[zz],
+            {"sp": sp + (members if up else -members)},
+        )
+
+    def pool_start():
+        @pl.when(z < planes - 1)
+        def _():
+            pool_line(z, True, True).start()
+
+        @pl.when(z > 0)
+        def _():
+            pool_line(z, False, True).start()
+
+        pool_out[z] = wp_ref[...]
+
+    def pool_from(i):
+        zz = order[i]
+        there = pool_out.at[zz]
+        remote(there, there, pool_send.at[zz, 0], pool_recv.at[zz], c_peer).wait_recv()
+
+        @pl.when((zz < z) & (z < planes - 1))
+        def _():
+            pool_line(zz, True, False).start()
+
+        @pl.when((zz > z) & (z > 0))
+        def _():
+            pool_line(zz, False, False).start()
 
     from_line(1)
     from_pair(0)
@@ -620,6 +659,7 @@
     multiply(order[0], y, True)
     multiply(order[0], 1 - y)
     from_line(3)
+    pool_start()
     from_pair(1)
     multiply(order[1], y)
     from_pair(2)
@@ -627,10 +667,12 @@
     for j in range(2 * per_half):
         scaled_out[:, j * 2 * rows : (j + 1) * 2 * rows] = pieces[j]
     multiply(order[2], y)
+    pool_from(1)
     multiply(order[2], 1 - y)
     from_pair(3)
     multiply(order[3], y)
     multiply(order[3], 1 - y)
+    pool_from(2)
     width = columns // planes
     scale = 1.0 / math.sqrt(hdim)
     for p in range(planes):
@@ -639,6 +681,18 @@
         k_out[p] = (acc[1, :, part] * inverse).astype(jnp.bfloat16)
         v_out[p] = (acc[2, :, part] * inverse).T.astype(jnp.bfloat16)
 
+    pool_from(3)
+    for i in range(planes):
+        zz = order[i]
+
+        @pl.when((zz <= z) & (z < planes - 1))
+        def _():
+            pool_line(zz, True, i == 0).wait_send()
+
+        @pl.when((zz >= z) & (z > 0))
+        def _():
+            pool_line(zz, False, i == 0).wait_send()
+
     for a in arrays:
         for i in range(planes):
             zz = order[i]
@@ -657,7 +711,7 @@
         turn(a).wait_send()
 
 
-def gather_and_project(tokens, pre_gain, w_query, w_key, w_value, heads):
+def gather_and_project(tokens, pre_gain, w_query, w_key, w_value, w_pool, heads):
     tok_rows, half_width = tokens.shape
     n_sp = lax.axis_size("sp")
     rows, columns = w_query.shape
@@ -674,9 +728,10 @@
             jax.ShapeDtypeStruct((heads, width, tok_rows), jnp.bfloat16),
             jax.ShapeDtypeStruct((tok_rows, full_width), jnp.bfloat16),
             jax.ShapeDtypeStruct((tok_rows, 128), jnp.float32),
+            jax.ShapeDtypeStruct((heads,) + w_pool.shape, jnp.bfloat16),
         ],
-        in_specs=[vmem] * 5,
-        out_specs=[vmem] * 5,
+        in_specs=[vmem] * 6,
+        out_specs=[vmem] * 6,
         scratch_shapes=[
             pltpu.VMEM((3, full_width, columns), jnp.bfloat16),
             pltpu.VMEM((tok_rows, half_width), jnp.bfloat16),
@@ -692,6 +747,8 @@
             dma((3,)),
             dma((3,)),
             dma((4,)),
+            dma((heads, 2)),
+            dma((heads,)),
         ],
         compiler_params=pltpu.CompilerParams(
             vmem_limit_bytes=56 * 2**20, collective_id=3, has_side_effects=True
@@ -699,39 +756,88 @@
         cost_estimate=pl.CostEstimate(
             flops=6 * tok_rows * full_width * columns, bytes_accessed=2**23, transcendentals=0
         ),
-    )(tokens, pre_gain.reshape(1, -1), w_query, w_key, w_value)
-
-
-def mix(hdim, lam_ref, q_ref, k_ref, v_ref, gain_ref, out_ref, q_in, k_all, v_all, acc, top, total, done, *sems):
-    (z_send, z_recv, in_send, in_recv, back_send, back_recv) = sems
+    )(tokens, pre_gain.reshape(1, -1), w_query, w_key, w_value, w_pool)
+
+
+def mix(
+    hdim,
+    lam_ref,
+    q_ref,
+    k_ref,
+    v_ref,
+    gain_ref,
+    scaled_ref,
+    inverse_ref,
+    pool_ref,
+    group_ref,
+    pscale_ref,
+    wo_ref,
+    out_ref,
+    q_in,
+    k_all,
+    v_all,
+    acc,
+    top,
+    total,
+    done,
+    w_pool,
+    w_full,
+    branch,
+    pool_sc,
+    halo,
+    pooled_sc,
+    *sems,
+):
+    (z_send, z_recv, in_send, in_recv, back_send, back_recv) = sems[:6]
+    (py_send, py_recv, pc_send, pc_recv, edge_sem, half_sem) = sems[6:12]
+    (wl_send, wl_recv, wy_send, wy_recv, wx_send, wx_recv, wc_send, wc_recv) = sems[12:]
     planes, rows, _ = q_ref.shape
     vdim = v_ref.shape[1]
     members = k_all.shape[1]
+    groups = group_ref.shape[0]
+    half_rows = rows // 2
     sp = lax.axis_index("sp")
+    tp = lax.axis_index("tp")
+    n_sp = lax.axis_size("sp")
     z = sp // members
     m = sp % members
+    y = m // 2
+    c = m % 2
     y_member = (m + 2) % members
-    c_member = m + 1 - 2 * (m % 2)
+    c_member = m + 1 - 2 * c
     turned = members - 1 - m
-
-    def at(plane, member):
-        return {"sp": plane * members + member}
+    upper = z // 2
+
+    def at(plane, member, half=None):
+        device = {"sp": plane * members + member}
+        if half is not None:
+            device["tp"] = half
+        return device
+
+    y_peer = at(z, y_member)
+    c_peer = at(z, c_member)
+    x_peer = {"tp": 1 - tp}
 
     def holder(block, member):
         return member + (block % 2) * (members - 1 - 2 * member)
 
+    def order(i):
+        return arrival(z, i)
+
     barrier = pltpu.get_barrier_semaphore()
 
     def greet(device):
         pl.semaphore_signal(barrier, 1, device_id=device, device_id_type=pl.DeviceIdType.MESH)
 
-    order = [arrival(z, i) for i in range(planes)]
-    for plane in order[1:]:
-        greet(at(plane, m))
-        greet(at(plane, turned))
+    for i in range(1, planes):
+        greet(at(order(i), m))
+        greet(at(order(i), turned))
     for member in (turned, y_member, c_member):
         greet(at(z, member))
-    pl.semaphore_wait(barrier, 2 * planes + 1)
+    for plane in range(planes):
+        greet(at(plane, m, 1 - tp))
+        greet(at(plane, turned, 1 - tp))
+    pl.semaphore_wait(barrier, 4 * planes + 1)
 
     def remote(src, dst, send, recv, device):
         return pltpu.make_async_remote_copy(
@@ -743,6 +849,9 @@
             device_id_type=pl.DeviceIdType.MESH,
         )
 
+    def arrived(ref, recv):
+        remote(ref, ref, recv, recv, c_peer).wait_recv()
+
     def k_out(plane):
         return remote(k_ref.at[plane], k_all.at[z, m], z_send.at[0, plane], z_recv.at[0, z], at(plane, m))
 
@@ -753,9 +862,6 @@
         return remote(
             q_ref.at[plane], q_in.at[z], z_send.at[2, plane], z_recv.at[2, z], at(plane, holder(z, m))
         )
-
-    def came(kind, plane, dst):
-        remote(dst, dst, z_send.at[kind, plane], z_recv.at[kind, plane], at(z, c_member)).wait_recv()
 
     def in_plane(plane, own):
         copies = []
@@ -765,9 +871,9 @@
             passed = everyone.at[plane, y_member]
             copies.append(
                 [
-                    remote(src, there, in_send.at[plane, 0, t], in_recv.at[plane, 0, t], at(z, y_member)),
-                    remote(src, there, in_send.at[plane, 1, t], in_recv.at[plane, 1, t], at(z, c_member)),
-                    remote(passed, passed, in_send.at[plane, 2, t], in_recv.at[plane, 2, t], at(z, c_member)),
+                    remote(src, there, in_send.at[plane, 0, t], in_recv.at[plane, 0, t], y_peer),
+                    remote(src, there, in_send.at[plane, 1, t], in_recv.at[plane, 1, t], c_peer),
+                    remote(passed, passed, in_send.at[plane, 2, t], in_recv.at[plane, 2, t], c_peer),
                 ]
             )
         return copies
@@ -787,18 +893,123 @@
             copies[1].wait_recv()
             copies[2].wait_recv()
 
+    def landed(i):
+        plane = order(i)
+        arrived(k_all.at[plane, m], z_recv.at[0, plane])
+        arrived(v_all.at[plane, m], z_recv.at[1, plane])
+        share(plane, False)
+
+    pool_rows = pool_ref.shape[1]
+
+    def pool_slot(plane, member):
+        start = pl.multiple_of((plane * members + member) * pool_rows, pool_rows)
+        return w_pool.at[pl.ds(start, pool_rows), :]
+
+    def pool_across(plane):
+        return remote(pool_ref.at[plane], pool_slot(plane, m), py_send.at[plane], py_recv.at[plane], y_peer)
+
+    def pool_beside(plane):
+        return remote(pool_ref.at[plane], pool_slot(plane, m), pc_send.at[plane, 0], pc_recv.at[plane, 0], c_peer)
+
+    def pool_onward(plane):
+        passed = pool_slot(plane, y_member)
+        return remote(passed, passed, pc_send.at[plane, 1], pc_recv.at[plane, 1], c_peer)
+
+    out_rows, out_columns = wo_ref.shape
+
+    def out_slot(half, plane, yy, cc):
+        first = pl.multiple_of(half * out_rows, out_rows)
+        column = pl.multiple_of((plane * members + yy * 2 + cc) * out_columns, out_columns)
+        return w_full.at[pl.ds(first, out_rows), pl.ds(column, out_columns)]
+
+    def w_line(plane, up, own):
+        there = out_slot(tp, plane, y, c)
+        side = 1 if up else 0
+        return remote(
+            wo_ref if own else there,
+            there,
+            wl_send.at[plane, side],
+            wl_recv.at[plane],
+            {"sp": sp + (members if up else -members)},
+        )
+
+    def w_across(plane, own):
+        there = out_slot(tp, plane, y, c)
+        return remote(wo_ref if own else there, there, wy_send.at[plane], wy_recv.at[plane], y_peer)
+
+    def w_swap(plane, yy, own):
+        there = out_slot(tp, plane, yy, c)
+        return remote(wo_ref if own else there, there, wx_send.at[plane, yy], wx_recv.at[plane, yy], x_peer)
+
+    def w_beside(half, plane, yy, own):
+        there = out_slot(half, plane, yy, c)
+        return remote(
+            wo_ref if own else there, there, wc_send.at[half, plane, yy], wc_recv.at[half, plane, yy], c_peer
+        )
+
+    def w_spread(plane, own):
+        w_across(plane, own).start()
+        w_swap(plane, y, own).start()
+        w_beside(tp, plane, y, own).start()
+
+    def w_line_start():
+        @pl.when(z < planes - 1)
+        def _():
+            w_line(z, True, True).start()
+
+        @pl.when(z > 0)
+        def _():
+            w_line(z, False, True).start()
+
+    def w_from_line(i):
+        plane = order(i)
+        arrived(out_slot(tp, plane, y, c), wl_recv.at[plane])
+
+        @pl.when((plane < z) & (z < planes - 1))
+        def _():
+            w_line(plane, True, False).start()
+
+        @pl.when((plane > z) & (z > 0))
+        def _():
+            w_line(plane, False, False).start()
+
+        w_spread(plane, False)
+
+    def w_from_pair(i):
+        plane = order(i)
+        arrived(out_slot(tp, plane, 1 - y, c), wy_recv.at[plane])
+        w_swap(plane, 1 - y, False).start()
+        w_beside(tp, plane, 1 - y, False).start()
+
+    def w_from_swap(i):
+        plane = order(i)
+        for yy in (y, 1 - y):
+            arrived(out_slot(1 - tp, plane, yy, c), wx_recv.at[plane, yy])
+            w_beside(1 - tp, plane, yy, False).start()
+
     share(z, True)
 
     @pl.when(z % 2 == 1)
     def _():
         q_out(z).start()
 
-    for plane in order[1:]:
-        k_out(plane).start()
-        v_out(plane).start()
-        q_out(plane).start()
+    for i in range(1, planes):
+        k_out(order(i)).start()
+        v_out(order(i)).start()
+        q_out(order(i)).start()
+    for plane in range(planes):
+        pool_across(plane).start()
+        pool_beside(plane).start()
+    w_spread(z, True)
     k_all[z, m] = k_ref[z]
     v_all[z, m] = v_ref[z]
+    for plane in range(planes):
+        start = pl.multiple_of((plane * members + m) * pool_rows, pool_rows)
+        w_pool[pl.ds(start, pool_rows), :] = pool_ref[plane]
+    w_full[
+        pl.ds(pl.multiple_of(tp * out_rows, out_rows), out_rows),
+        pl.ds(pl.multiple_of(sp * out_columns, out_columns), out_columns),
+    ] = wo_ref[...]
 
     @pl.when(z % 2 == 0)
     def _():
@@ -846,12 +1057,13 @@
 
         visit(block, block, pair * (members // 2), members // 2, True)
 
-    def across(a, b):
-        visit(jnp.maximum(a, b), jnp.minimum(a, b), 0, members, False)
-
-    def result_copy(block):
+    def result_copy(block, half):
         return remote(
-            done.at[block], out_ref.at[z], back_send.at[block], back_recv.at[z], at(block, holder(block, m))
+            done.at[block, pl.ds(pl.multiple_of(half * half_rows, half_rows), half_rows)],
+            branch.at[tp * planes + z, :, pl.ds(0, vdim)],
+            back_send.at[block, half],
+            back_recv.at[tp * planes + z],
+            at(block, holder(block, m), half),
         )
 
     def at_home(block):
@@ -866,78 +1078,230 @@
 
         @pl.when(at_home(block))
         def _():
-            out_ref[z] = done[block]
+            kept = pl.ds(pl.multiple_of(tp * half_rows, half_rows), half_rows)
+            branch[tp * planes + z, :, :vdim] = done[block, kept]
 
         @pl.when(jnp.logical_not(at_home(block)))
         def _():
-            result_copy(block).start()
-
-    def landed(i):
-        plane = order[i]
-        came(0, plane, k_all.at[plane, m])
-        came(1, plane, v_all.at[plane, m])
-        share(plane, False)
+            result_copy(block, tp).start()
+
+        result_copy(block, 1 - tp).start()
+
+    edge_rows = halo.shape[0]
+
+    def edge_out():
+        return remote(
+            pool_sc.at[pl.ds(rows - edge_rows, edge_rows)], halo, edge_sem.at[0], edge_sem.at[1], {"sp": sp + 1}
+        )
+
+    def half_out():
+        mine = pl.ds(pl.multiple_of(tp * groups, groups), groups)
+        return remote(
+            pooled_sc, branch.at[mine, :, pl.ds(vdim, vdim)], half_sem.at[0], half_sem.at[1], x_peer
+        )
+
+    def pool_project():
+        for plane in range(planes):
+            arrived(pool_slot(plane, c_member), pc_recv.at[plane, 0])
+            arrived(pool_slot(plane, members - 1 - m), pc_recv.at[plane, 1])
+        product = jnp.dot(scaled_ref[...], w_pool[...], preferred_element_type=jnp.float32)
+        pool_sc[...] = (product * inverse_ref[:, :1]).astype(jnp.bfloat16)
+
+        @pl.when(sp < n_sp - 1)
+        def _():
+            edge_out().start()
+
+        @pl.when(sp == 0)
+        def _():
+            halo[...] = jnp.zeros_like(halo)
+
+    def pool_mix():
+        @pl.when(sp > 0)
+        def _():
+            arrived(halo, edge_sem.at[1])
+
+        for g in range(groups):
+            part = slice(g * vdim, (g + 1) * vdim)
+            own = pool_sc[:, part].astype(jnp.float32)
+            running = jnp.concatenate([halo[:, part].astype(jnp.float32), own], axis=0)
+            span = WINDOWS[g % len(WINDOWS)]
+            step = 1
+            while step < span:
+                running = running + pltpu.roll(running, step, 0)
+                step *= 2
+            position = sp * rows + lax.broadcasted_iota(jnp.int32, own.shape, 0)
+            count = jnp.minimum(position + 1, span).astype(jnp.float32)
+            differ = (running[edge_rows:] / count - own).astype(jnp.bfloat16)
+            pooled = jnp.dot(differ, group_ref[g], preferred_element_type=jnp.float32)
+            pooled = (pooled * pscale_ref[:, part]).astype(jnp.bfloat16)
+            low, high = pooled[:half_rows], pooled[half_rows:]
+            branch[tp * groups + g, :, vdim:] = jnp.where(tp == 0, low, high)
+            pooled_sc[g] = jnp.where(tp == 0, high, low)
+        half_out().start()
 
     hand_on(z, True)
     shared(z, True)
 
     @pl.when(z % 2 == 1)
     def _():
-        came(2, z, q_in.at[z])
-
-    for i in range(planes - 1):
-        landed(i + 1)
-        diagonal(order[i])
-        hand_on(order[i + 1], False)
-        for j in range(i):
-            across(order[i], order[j])
-        came(2, order[i + 1], q_in.at[order[i + 1]])
-        shared(order[i + 1], False)
-    late = order[planes - 1]
-    diagonal(late)
-    finish(0)
-    half = z // 2
-
-    def last(s, carry):
-        across(late, s - 1 + half)
-        finish(s)
+        arrived(q_in.at[z], z_recv.at[2, z])
+
+    for plane in range(planes):
+        arrived(pool_slot(plane, y_member), py_recv.at[plane])
+        pool_onward(plane).start()
+
+    def stage(i, carry):
+        block = order(i)
+
+        @pl.when(i < planes - 1)
+        def _():
+            landed(i + 1)
+
+        @pl.when(i == LINE_STAGE)
+        def _():
+            w_line_start()
+
+        diagonal(block)
+
+        @pl.when(i < planes - 1)
+        def _():
+            hand_on(order(i + 1), False)
+
+        @pl.when(i == 0)
+        def _():
+            pool_project()
+            w_from_pair(0)
+
+        @pl.when(i == 1)
+        def _():
+            pool_mix()
+            w_from_swap(0)
+
+        @pl.when(i == planes - 1)
+        def _():
+            w_from_line(1)
+            finish(0)
+
+        def pair(j, carry):
+            other = jnp.where(i < planes - 1, order(j), j + upper)
+            visit(jnp.maximum(block, other), jnp.minimum(block, other), 0, members, False)
+
+            @pl.when(i == planes - 1)
+            def _():
+                finish(j + 1)
+
+                @pl.when(j == 0)
+                def _():
+                    w_from_pair(1)
+                    w_from_line(2)
+
+                @pl.when(j == 1)
+                def _():
+                    w_from_pair(2)
+                    w_from_line(3)
+
+            return carry
+
+        lax.fori_loop(0, i, pair, 0)
+
+        @pl.when(i < planes - 1)
+        def _():
+            arrived(q_in.at[order(i + 1)], z_recv.at[2, order(i + 1)])
+            shared(order(i + 1), False)
+
         return carry
 
-    lax.fori_loop(1, planes, last, 0)
-
-    for plane in order[1:]:
-        k_out(plane).wait_send()
-        v_out(plane).wait_send()
-        q_out(plane).wait_send()
+    lax.fori_loop(0, planes, stage, 0)
+    w_from_pair(3)
+    for i in range(1, planes):
+        w_from_swap(i)
+
+    for head in range(2 * planes):
+        own_head = tp * planes + z == head
+
+        @pl.when(jnp.logical_not(own_head & at_home(z)))
+        def _():
+            arrived(branch.at[head, :, pl.ds(0, vdim)], back_recv.at[head])
+
+    theirs = pl.ds(pl.multiple_of((1 - tp) * groups, groups), groups)
+    arrived(branch.at[theirs, :, pl.ds(vdim, vdim)], half_sem.at[1])
+    for half in range(2):
+        for plane in range(planes):
+            for yy in range(2):
+                arrived(out_slot(half, plane, yy, 1 - c), wc_recv.at[half, plane, yy])
+    left = jnp.concatenate([branch[head] for head in range(2 * planes)], axis=1)
+    width = out_ref.shape[1] // planes
+
+    def column(n, carry):
+        part = pl.ds(pl.multiple_of(n * width, width), width)
+        out_ref[:, part] = jnp.dot(
+            left, w_full[:, part], preferred_element_type=jnp.float32
+        ).astype(jnp.bfloat16)
+        return carry
+
+    lax.fori_loop(0, planes, column, 0)
+
+    for i in range(1, planes):
+        k_out(order(i)).wait_send()
+        v_out(order(i)).wait_send()
+        q_out(order(i)).wait_send()
 
     @pl.when(z % 2 == 1)
     def _():
         q_out(z).wait_send()
 
     for i in range(planes):
-        for copies in in_plane(order[i], i == 0):
+        plane = order(i)
+        for copies in in_plane(plane, i == 0):
             for copy in copies:
                 copy.wait_send()
-    for block in range(planes):
-
-        @pl.when(jnp.logical_not(at_home(block)))
-        def _():
-            result_copy(block).wait_send()
-            here = out_ref.at[block]
-            remote(here, here, back_send.at[block], back_recv.at[block], at(z, c_member)).wait_recv()
-
-
-def attend_and_return(queries, keys, values, lambdas, sub_gain):
+        w_across(plane, i == 0).wait_send()
+        for yy in (y, 1 - y):
+            w_swap(plane, yy, False).wait_send()
+            w_beside(0, plane, yy, False).wait_send()
+            w_beside(1, plane, yy, False).wait_send()
+
+        @pl.when((plane <= z) & (z < planes - 1))
+        def _():
+            w_line(plane, True, False).wait_send()
+
+        @pl.when((plane >= z) & (z > 0))
+        def _():
+            w_line(plane, False, False).wait_send()
+
+    for plane in range(planes):
+        pool_across(plane).wait_send()
+        pool_beside(plane).wait_send()
+        pool_onward(plane).wait_send()
+        result_copy(plane, 1 - tp).wait_send()
+
+        @pl.when(jnp.logical_not(at_home(plane)))
+        def _():
+            result_copy(plane, tp).wait_send()
+
+    half_out().wait_send()
+
+    @pl.when(sp < n_sp - 1)
+    def _():
+        edge_out().wait_send()
+
+
+def attend_and_project(
+    queries, keys, values, lambdas, sub_gain, scaled, inverse, pool_lines, group_weight, pool_scale, w_out
+):
     planes, rows, width = queries.shape
     vdim = values.shape[1]
-    members = lax.axis_size("sp") // planes
+    n_sp = lax.axis_size("sp")
+    members = n_sp // planes
+    groups, group_dim, _ = group_weight.shape
+    out_rows, out_columns = w_out.shape
     vmem = pl.BlockSpec(memory_space=pltpu.VMEM)
     dma = pltpu.SemaphoreType.DMA
     work = planes * rows * members * planes * rows
     return pl.pallas_call(
         functools.partial(mix, width // 2),
-        out_shape=jax.ShapeDtypeStruct((planes, rows, vdim), jnp.bfloat16),
-        in_specs=[pl.BlockSpec(memory_space=pltpu.SMEM), vmem, vmem, vmem, vmem],
+        out_shape=jax.ShapeDtypeStruct((rows // 2, n_sp * out_columns), jnp.bfloat16),
+        in_specs=[pl.BlockSpec(memory_space=pltpu.SMEM)] + [vmem] * 10,
         out_specs=vmem,
         scratch_shapes=[
             pltpu.VMEM((planes, rows, width), jnp.bfloat16),
@@ -947,20 +1311,52 @@
             pltpu.VMEM((planes, 1, 2 * rows), jnp.float32),
             pltpu.VMEM((planes, 8, 2 * rows), jnp.float32),
             pltpu.VMEM((planes, rows, vdim), jnp.bfloat16),
+            pltpu.VMEM((scaled.shape[1], groups * group_dim), jnp.bfloat16),
+            pltpu.VMEM((2 * out_rows, n_sp * out_columns), jnp.bfloat16),
+            pltpu.VMEM((2 * planes, rows // 2, 2 * vdim), jnp.bfloat16),
+            pltpu.VMEM((rows, groups * group_dim), jnp.bfloat16),
+            pltpu.VMEM((RIM_ROWS + 1, groups * group_dim), jnp.bfloat16),
+            pltpu.VMEM((groups, rows // 2, group_dim), jnp.bfloat16),
             dma((3, planes)),
             dma((3, planes)),
             dma((planes, 3, 2)),
             dma((planes, 3, 2)),
+            dma((planes, 2)),
+            dma((2 * planes,)),
             dma((planes,)),
             dma((planes,)),
+            dma((planes, 2)),
+            dma((planes, 2)),
+            dma((2,)),
+            dma((2,)),
+            dma((planes, 2)),
+            dma((planes,)),
+            dma((planes,)),
+            dma((planes,)),
+            dma((planes, 2)),
+            dma((planes, 2)),
+            dma((2, planes, 2)),
+            dma((2, planes, 2)),
         ],
         compiler_params=pltpu.CompilerParams(
-            vmem_limit_bytes=56 * 2**20, collective_id=2, has_side_effects=True
+            vmem_limit_bytes=60 * 2**20, collective_id=2, has_side_effects=True
         ),
         cost_estimate=pl.CostEstimate(
             flops=4 * work * vdim, bytes_accessed=keys.size * 8, transcendentals=work
         ),
-    )(lambdas, queries, keys, values, sub_gain.reshape(1, -1))
+    )(
+        lambdas,
+        queries,
+        keys,
+        values,
+        sub_gain.reshape(1, -1),
+        scaled,
+        inverse,
+        pool_lines,
+        group_weight,
+        pool_scale.reshape(1, -1),
+        w_out,
+    )
 
 
 def trailing(x, window_ids, group_dim):
@@ -1041,44 +1437,51 @@
     groups = group_weight.shape[0]
     group_dim = group_weight.shape[1]
 
+    shaped_for_mix = n_tp == 2 and heads == 4 and n_sp == 4 * heads and tok_rows % 32 == 0
+    if shaped_for_mix and qdim == vdim == group_dim and groups == heads:
+        queries, key_rows, values, scaled, inverse, pool_lines = gather_and_project(
+            tokens, pre_gain, w_query, w_key, w_value, w_pool, heads
+        )
+        return attend_and_project(
+            queries,
+            key_rows,
+            values,
+            lambdas,
+            sub_gain,
+            scaled,
+            inverse,
+            pool_lines,
+            group_weight,
+            pool_scale,
+            w_out,
+        )
     swap = [(0, 1), (1, 0)]
-    shaped_for_mix = n_tp == 2 and heads == 4 and n_sp == 4 * heads and qdim == vdim
     w_sorted = w_out.reshape(heads, 2, vdim, -1).swapaxes(0, 1).reshape(w_out.shape)
-    if shaped_for_mix:
-        w_pool_rows = lax.all_gather(w_pool, "sp", axis=0, tiled=True)
-        w_out_rows = lax.all_gather(w_sorted, "sp", axis=1, tiled=True)
-        queries, key_rows, values, scaled, inverse = gather_and_project(
-            tokens, pre_gain, w_query, w_key, w_value, heads
-        )
-        attended = attend_and_return(queries, key_rows, values, lambdas, sub_gain)
-        pool_in = jnp.dot(scaled, w_pool_rows, preferred_element_type=jnp.float32)
-        pool_in = (pool_in * inverse[:, :1]).astype(jnp.bfloat16)
+    features = tokens.astype(jnp.float32)
+    mine = (features * pre_gain.astype(jnp.float32)[None, :]).astype(jnp.bfloat16)
+    squares = jnp.sum(features * features, axis=1, keepdims=True)
+    weights = [w_query, w_key, w_value, w_pool]
+    if n_sp % 4 == 0:
+        *weights, theirs = gather_weights(weights, mine, n_tp == 2)
     else:
-        features = tokens.astype(jnp.float32)
-        mine = (features * pre_gain.astype(jnp.float32)[None, :]).astype(jnp.bfloat16)
-        squares = jnp.sum(features * features, axis=1, keepdims=True)
-        weights = [w_query, w_key, w_value, w_pool]
-        if n_sp % 4 == 0:
-            *weights, theirs = gather_weights(weights, mine, n_tp == 2)
-        else:
-            weights = [lax.all_gather(w, "sp", axis=0, tiled=True) for w in weights]
-            theirs = lax.ppermute(mine, "tp", swap) if n_tp == 2 else mine
-        w_sorted, weights = lax.optimization_barrier((w_sorted, weights))
-        w_out_rows = lax.all_gather(w_sorted, "sp", axis=1, tiled=True)
-        if n_tp == 2:
-            squares = squares + lax.ppermute(squares, "tp", swap)
-            scaled = jnp.concatenate(
-                [jnp.where(tp == 0, mine, theirs), jnp.where(tp == 0, theirs, mine)], axis=1
-            )
-        else:
-            scaled = lax.all_gather(mine, "tp", axis=1, tiled=True)
-            squares = lax.psum(squares, "tp")
-        inverse = lax.rsqrt(squares / model_width + EPSILON)
-        queries, key_rows, values, pool_in = [
-            (jnp.dot(scaled, w, preferred_element_type=jnp.float32) * inverse).astype(jnp.bfloat16)
-            for w in weights
-        ]
-        attended = general_attention(queries, key_rows, values, lambdas, sub_gain)
+        weights = [lax.all_gather(w, "sp", axis=0, tiled=True) for w in weights]
+        theirs = lax.ppermute(mine, "tp", swap) if n_tp == 2 else mine
+    w_sorted, weights = lax.optimization_barrier((w_sorted, weights))
+    w_out_rows = lax.all_gather(w_sorted, "sp", axis=1, tiled=True)
+    if n_tp == 2:
+        squares = squares + lax.ppermute(squares, "tp", swap)
+        scaled = jnp.concatenate(
+            [jnp.where(tp == 0, mine, theirs), jnp.where(tp == 0, theirs, mine)], axis=1
+        )
+    else:
+        scaled = lax.all_gather(mine, "tp", axis=1, tiled=True)
+        squares = lax.psum(squares, "tp")
+    inverse = lax.rsqrt(squares / model_width + EPSILON)
+    queries, key_rows, values, pool_in = [
+        (jnp.dot(scaled, w, preferred_element_type=jnp.float32) * inverse).astype(jnp.bfloat16)
+        for w in weights
+    ]
+    attended = general_attention(queries, key_rows, values, lambdas, sub_gain)
 
     halo = passed_along(pool_in[tok_rows - RIM_ROWS - 1 :], "sp", 1)
     extended = jnp.concatenate([halo, pool_in], axis=0).astype(jnp.float32)

time: 189 us -> 164 us (0.87)
  Pallas kernels: 134 us -> 159 us
  waiting for transfers between devices: 19.9 us -> 0 us
  between operations: 13.6 us -> 0.02 us
  matrix products: 11.4 us -> 0 us
  starting transfers between devices: 3.1 us -> 0 us
    pallas_call x1, Pallas kernels: 76.8 us -> 105 us  [attend_and_project(): pl.pallas_call(functools.partial(mix, width // 2), out_shape=jax.ShapeDty...]
    ppermute x2 -> x0, waiting for transfers between devices: 19.1 us -> none  [the longest x1 18.8 us: local(): got = lax.ppermute(send, 'tp', swap)]
    dot_general x4 -> x0, matrix products: 11.4 us -> none  [the longest x1 4.51 us: local(): keep = jnp.dot(keep, w_out_rows, preferred_element_type=jnp.float32)]
    ppermute x2 -> x0, starting transfers between devices: 3.05 us -> none  [the longest x1 1.54 us: local(): got = lax.ppermute(send, 'tp', swap)]
    pallas_call x1, Pallas kernels: 57 us -> 54 us  [gather_and_project(): pl.pallas_call(functools.partial(project, width // 2, full_width), out_sh...]
    transpose x2 -> x0, local copies, waits for them, and re-layouts: 1.9 us -> none  [the longest x1 1.67 us: local(): w_out.reshape(heads, 2, vdim, -1).swapaxes(0, 1).reshape(w_out.shape)]
  transfers between devices with their start and end apart: 4 -> 0, of which waited for: 2 -> 0; matrix products, arithmetic and copies ran while one was open for 5% -> 0% of each run, Pallas kernels for 71% -> 0%
where the time goes in v3:
time: 164 us; the launch traced here: 162 us
  Pallas kernels  159 us (97%)
  local copies, waits for them, and re-layouts  3.37 us (2%)
    pallas_call x1, Pallas kernels, attend_and_project(): pl.pallas_call(functools.partial(mix, width // 2), out_shape=jax.ShapeDty...  105 us
    pallas_call x1, Pallas kernels, gather_and_project(): pl.pallas_call(functools.partial(project, width // 2, full_width), out_sh...  54 us

profile of v3, /device:TPU:0, one launch (start us, length us, event | category | flops | bytes accessed | tf_op | source)
XLA Modules:
  0.0 162.2 jit_solution(6474995646840172407)
XLA Ops:
  0.0 1.3 reshape.9.gain_ref
  1.3 54.0 %shard_map.109 = (bf16[4,384,128]{2,1,0:T(8,128)(2,1)}, bf16[4,384,128]{2,1,0:T(8,128)(2,1)}, bf16[4,128,384]{2,1,0:T(8,128)(2,1)}, bf16[384,2048]{1,0:T(8,128)(...) custom-call(bf16[384,1024]{1,0:T(8,128)(2,1)} %tok_ref.1, bf16[1,1024]{1,0:T(2,128)(2,1)} %reshape.9.gain_ref, ...), custom_call_target="tpu_custom_call" | custom-call | flops 2415919104 | bytes 8388608 | tf_op jit(solution)/shard_map/pallas_call | solution.py:723
  55.3 104.8 %shard_map.110 = bf16[192,2048]{1,0:T(8,128)(2,1)} custom-call(f32[4]{0:T(128)} %lam_ref.1, bf16[4,384,128]{2,1,0:T(8,128)(2,1)} %get-tuple-element.11.q_ref, bf16[4,384,128]{2,1,0:T(8,128)(2,1)} %get-tuple-element.12.k_ref, bf16[4,128,384]{2,1,0:T(8,128)(2,1)} %get-tuple-element.13.v_ref, f32[1,128]{1,0:T(1,128)} %bitcast.3, ...), custom_call_target="tpu_custom_call" | custom-call | flops 4831838208 | bytes 1572864 | tf_op jit(solution)/shard_map/pallas_call | solution.py:1301
  160.1 2.1 %copy.13 = bf16[192,2048]{1,0:T(8,128)(2,1)} copy(bf16[192,2048]{1,0:T(8,128)(2,1)} %shard_map.110) | data formatting | bytes 1572864

commit v4 on v3

--- a/solution.py
+++ b/solution.py
@@ -12,7 +12,6 @@
 NEG_LARGE = -1e30
 WINDOWS = (2, 4, 8, 16)
 RIM_ROWS = 15
-LINE_STAGE = 2
 
 
 def passed_along(block, axis, distance):
@@ -429,350 +428,30 @@
     return jnp.where(i == 0, z, jnp.where(i == 1, 1 + 4 * half - z, later))
 
 
-def project(
+def layer(
     hdim,
     model_width,
+    lam_ref,
     tok_ref,
-    gain_ref,
-    wq_ref,
+    gain_in,
     wk_ref,
     wv_ref,
+    wq_ref,
     wp_ref,
-    q_out,
-    k_out,
-    v_out,
-    scaled_out,
-    inverse_out,
-    pool_out,
+    gain_ref,
+    group_ref,
+    pscale_ref,
+    wo_ref,
+    out_ref,
     full,
     theirs,
     their_gain,
     pieces,
-    acc,
-    *sems,
-):
-    (line_send, line_recv, y_send, y_recv, c_send, c_recv, turn_send, turn_recv, swap_sem, pool_send, pool_recv) = sems
-    weights = (wq_ref, wk_ref, wv_ref)
-    arrays = range(len(weights))
-    rows, columns = wq_ref.shape
-    tok_rows, half_width = tok_ref.shape
-    planes = q_out.shape[0]
-    members = lax.axis_size("sp") // planes
-    sp = lax.axis_index("sp")
-    tp = lax.axis_index("tp")
-    z = sp // members
-    y = (sp % members) // 2
-    c = sp % 2
-    y_peer = {"sp": sp + 2 - 4 * y}
-    c_peer = {"sp": sp + 1 - 2 * c}
-    x_peer = {"tp": 1 - tp}
-    order = [arrival(z, i) for i in range(planes)]
-    partner = {"sp": order[1] * members + sp % members}
-
-    barrier = pltpu.get_barrier_semaphore()
-
-    def greet(device):
-        pl.semaphore_signal(barrier, 1, device_id=device, device_id_type=pl.DeviceIdType.MESH)
-
-    for device in (y_peer, c_peer, x_peer):
-        greet(device)
-
-    @pl.when(z > 0)
-    def _():
-        greet({"sp": sp - members})
-
-    @pl.when(z < planes - 1)
-    def _():
-        greet({"sp": sp + members})
-
-    pl.semaphore_wait(barrier, 3 + jnp.where(z > 0, 1, 0) + jnp.where(z < planes - 1, 1, 0))
-
-    def remote(src, dst, send, recv, device):
-        return pltpu.make_async_remote_copy(
-            src_ref=src,
-            dst_ref=dst,
-            send_sem=send,
-            recv_sem=recv,
-            device_id=device,
-            device_id_type=pl.DeviceIdType.MESH,
-        )
-
-    def slot(a, zz, yy, cc, first=0, count=rows):
-        start = pl.multiple_of((zz * members + yy * 2 + cc) * rows + first, count)
-        return full.at[a, pl.ds(start, count), :]
-
-    def line(a, zz, up, own):
-        there = slot(a, zz, y, c)
-        side = 1 if up else 0
-        return remote(
-            weights[a] if own else there,
-            there,
-            line_send.at[zz, side, a],
-            line_recv.at[zz, a],
-            {"sp": sp + (members if up else -members)},
-        )
-
-    def y_copy(a, i, own):
-        if i == 1:
-            there = slot(a, order[i], y, c, rows // 2, rows // 2)
-            src = there
-        else:
-            there = slot(a, order[i], y, c)
-            src = weights[a] if own else there
-        return remote(src, there, y_send.at[order[i], a], y_recv.at[order[i], a], y_peer)
-
-    def y_came(a, i):
-        there = slot(a, order[i], 1 - y, c, *((rows // 2, rows // 2) if i == 1 else ()))
-        return remote(there, there, y_send.at[order[i], a], y_recv.at[order[i], a], y_peer)
-
-    def turn(a):
-        there = slot(a, z, 1 - y, c, 0, rows // 2)
-        return remote(there, there, turn_send.at[a], turn_recv.at[a], partner)
-
-    def turned(a):
-        there = slot(a, order[1], 1 - y, c, 0, rows // 2)
-        return remote(there, there, turn_send.at[a], turn_recv.at[a], partner)
-
-    def c_copy(a, zz, yy, own):
-        there = slot(a, zz, yy, c)
-        src = weights[a] if own else there
-        return remote(src, there, c_send.at[zz, yy, a], c_recv.at[zz, yy, a], c_peer)
-
-    def c_came(a, zz, yy):
-        there = slot(a, zz, yy, 1 - c)
-        return remote(there, there, c_send.at[zz, yy, a], c_recv.at[zz, yy, a], c_peer)
-
-    swaps = (
-        remote(tok_ref, theirs, swap_sem.at[0], swap_sem.at[1], x_peer),
-        remote(gain_ref, their_gain, swap_sem.at[2], swap_sem.at[3], x_peer),
-    )
-    for a in arrays:
-
-        @pl.when(z < planes - 1)
-        def _():
-            line(a, z, True, True).start()
-
-        @pl.when(z > 0)
-        def _():
-            line(a, z, False, True).start()
-
-        y_copy(a, 0, True).start()
-        if a == 0:
-            for swap in swaps:
-                swap.start()
-    for a in arrays:
-        c_copy(a, z, y, True).start()
-        full[a, pl.ds(pl.multiple_of(sp * rows, rows), rows), :] = weights[a][...]
-
-    def from_line(i):
-        zz = order[i]
-        for a in arrays:
-            there = slot(a, zz, y, c)
-            remote(there, there, line_send.at[zz, 0, a], line_recv.at[zz, a], c_peer).wait_recv()
-
-            @pl.when((zz < z) & (z < planes - 1))
-            def _():
-                line(a, zz, True, False).start()
-
-            @pl.when((zz > z) & (z > 0))
-            def _():
-                line(a, zz, False, False).start()
-
-            y_copy(a, i, False).start()
-            c_copy(a, zz, y, False).start()
-
-    def from_pair(i):
-        zz = order[i]
-        for a in arrays:
-            y_came(a, i).wait_recv()
-            if i == 0:
-                turn(a).start()
-            if i == 1:
-                turned(a).wait_recv()
-            c_copy(a, zz, 1 - y, False).start()
-
-    def multiply(zz, yy, first=False):
-        for a in arrays:
-            c_came(a, zz, yy).wait_recv()
-        piece = zz * 2 + yy
-        start = pl.multiple_of(piece * 2 * rows, 2 * rows)
-        for a in arrays:
-            part = jnp.dot(
-                pieces[piece], full[a, pl.ds(start, 2 * rows), :], preferred_element_type=jnp.float32
-            )
-            if first:
-                acc[a] = part
-            else:
-                acc[a] += part
-
-    def pool_line(zz, up, own):
-        there = pool_out.at[zz]
-        side = 1 if up else 0
-        return remote(
-            wp_ref if own else there,
-            there,
-            pool_send.at[zz, side],
-            pool_recv.at[zz],
-            {"sp": sp + (members if up else -members)},
-        )
-
-    def pool_start():
-        @pl.when(z < planes - 1)
-        def _():
-            pool_line(z, True, True).start()
-
-        @pl.when(z > 0)
-        def _():
-            pool_line(z, False, True).start()
-
-        pool_out[z] = wp_ref[...]
-
-    def pool_from(i):
-        zz = order[i]
-        there = pool_out.at[zz]
-        remote(there, there, pool_send.at[zz, 0], pool_recv.at[zz], c_peer).wait_recv()
-
-        @pl.when((zz < z) & (z < planes - 1))
-        def _():
-            pool_line(zz, True, False).start()
-
-        @pl.when((zz > z) & (z > 0))
-        def _():
-            pool_line(zz, False, False).start()
-
-    from_line(1)
-    from_pair(0)
-    from_line(2)
-    for swap in swaps:
-        swap.wait()
-    squares = jnp.zeros((tok_rows, 1), jnp.float32)
-    per_half = half_width // (2 * rows)
-    for ref, gains, owner in ((tok_ref, gain_ref, tp), (theirs, their_gain, 1 - tp)):
-        for j in range(per_half):
-            chunk = pl.ds(j * 2 * rows, 2 * rows)
-            features = ref[:, chunk].astype(jnp.float32)
-            squares += jnp.sum(features * features, axis=1, keepdims=True)
-            scaled = (features * gains[:, chunk].astype(jnp.float32)).astype(jnp.bfloat16)
-            pieces[owner * per_half + j] = scaled
-    inverse = lax.rsqrt(squares / model_width + EPSILON)
-    inverse_out[...] = jnp.broadcast_to(inverse, inverse_out.shape)
-    multiply(order[0], y, True)
-    multiply(order[0], 1 - y)
-    from_line(3)
-    pool_start()
-    from_pair(1)
-    multiply(order[1], y)
-    from_pair(2)
-    multiply(order[1], 1 - y)
-    for j in range(2 * per_half):
-        scaled_out[:, j * 2 * rows : (j + 1) * 2 * rows] = pieces[j]
-    multiply(order[2], y)
-    pool_from(1)
-    multiply(order[2], 1 - y)
-    from_pair(3)
-    multiply(order[3], y)
-    multiply(order[3], 1 - y)
-    pool_from(2)
-    width = columns // planes
-    scale = 1.0 / math.sqrt(hdim)
-    for p in range(planes):
-        part = slice(p * width, (p + 1) * width)
-        q_out[p] = (acc[0, :, part] * inverse).astype(jnp.bfloat16) * scale
-        k_out[p] = (acc[1, :, part] * inverse).astype(jnp.bfloat16)
-        v_out[p] = (acc[2, :, part] * inverse).T.astype(jnp.bfloat16)
-
-    pool_from(3)
-    for i in range(planes):
-        zz = order[i]
-
-        @pl.when((zz <= z) & (z < planes - 1))
-        def _():
-            pool_line(zz, True, i == 0).wait_send()
-
-        @pl.when((zz >= z) & (z > 0))
-        def _():
-            pool_line(zz, False, i == 0).wait_send()
-
-    for a in arrays:
-        for i in range(planes):
-            zz = order[i]
-            y_copy(a, i, i == 0).wait_send()
-            c_copy(a, zz, y, i == 0).wait_send()
-            c_copy(a, zz, 1 - y, False).wait_send()
-
-            @pl.when((zz <= z) & (z < planes - 1))
-            def _():
-                line(a, zz, True, i == 0).wait_send()
-
-            @pl.when((zz >= z) & (z > 0))
-            def _():
-                line(a, zz, False, i == 0).wait_send()
-
-        turn(a).wait_send()
-
-
-def gather_and_project(tokens, pre_gain, w_query, w_key, w_value, w_pool, heads):
-    tok_rows, half_width = tokens.shape
-    n_sp = lax.axis_size("sp")
-    rows, columns = w_query.shape
-    width = columns // heads
-    full_width = n_sp * rows
-    vmem = pl.BlockSpec(memory_space=pltpu.VMEM)
-    dma = pltpu.SemaphoreType.DMA
-    by_head = jax.ShapeDtypeStruct((heads, tok_rows, width), jnp.bfloat16)
-    return pl.pallas_call(
-        functools.partial(project, width // 2, full_width),
-        out_shape=[
-            by_head,
-            by_head,
-            jax.ShapeDtypeStruct((heads, width, tok_rows), jnp.bfloat16),
-            jax.ShapeDtypeStruct((tok_rows, full_width), jnp.bfloat16),
-            jax.ShapeDtypeStruct((tok_rows, 128), jnp.float32),
-            jax.ShapeDtypeStruct((heads,) + w_pool.shape, jnp.bfloat16),
-        ],
-        in_specs=[vmem] * 6,
-        out_specs=[vmem] * 6,
-        scratch_shapes=[
-            pltpu.VMEM((3, full_width, columns), jnp.bfloat16),
-            pltpu.VMEM((tok_rows, half_width), jnp.bfloat16),
-            pltpu.VMEM((1, half_width), jnp.bfloat16),
-            pltpu.VMEM((full_width // (2 * rows), tok_rows, 2 * rows), jnp.bfloat16),
-            pltpu.VMEM((3, tok_rows, columns), jnp.float32),
-            dma((heads, 2, 3)),
-            dma((heads, 3)),
-            dma((heads, 3)),
-            dma((heads, 3)),
-            dma((heads, 2, 3)),
-            dma((heads, 2, 3)),
-            dma((3,)),
-            dma((3,)),
-            dma((4,)),
-            dma((heads, 2)),
-            dma((heads,)),
-        ],
-        compiler_params=pltpu.CompilerParams(
-            vmem_limit_bytes=56 * 2**20, collective_id=3, has_side_effects=True
-        ),
-        cost_estimate=pl.CostEstimate(
-            flops=6 * tok_rows * full_width * columns, bytes_accessed=2**23, transcendentals=0
-        ),
-    )(tokens, pre_gain.reshape(1, -1), w_query, w_key, w_value, w_pool)
-
-
-def mix(
-    hdim,
-    lam_ref,
-    q_ref,
-    k_ref,
-    v_ref,
-    gain_ref,
-    scaled_ref,
-    inverse_ref,
-    pool_ref,
-    group_ref,
-    pscale_ref,
-    wo_ref,
-    out_ref,
+    product,
+    inverse_sc,
+    k_src,
+    v_src,
+    q_src,
     q_in,
     k_all,
     v_all,
@@ -788,12 +467,17 @@
     pooled_sc,
     *sems,
 ):
-    (z_send, z_recv, in_send, in_recv, back_send, back_recv) = sems[:6]
-    (py_send, py_recv, pc_send, pc_recv, edge_sem, half_sem) = sems[6:12]
-    (wl_send, wl_recv, wy_send, wy_recv, wx_send, wx_recv, wc_send, wc_recv) = sems[12:]
-    planes, rows, _ = q_ref.shape
-    vdim = v_ref.shape[1]
+    (line_send, line_recv, y_send, y_recv, c_send, c_recv, turn_send, turn_recv, swap_sem) = sems[:9]
+    (z_send, z_recv, in_send, in_recv, back_send, back_recv) = sems[9:15]
+    (py_send, py_recv, pc_send, pc_recv, edge_sem, half_sem, pool_send, pool_recv) = sems[15:23]
+    (wl_send, wl_recv, wy_send, wy_recv, wx_send, wx_recv, wc_send, wc_recv) = sems[23:]
+    weights = (wk_ref, wv_ref, wq_ref)
+    first_pair, last_one = (0, 1), (2,)
+    planes, rows, _ = q_src.shape
+    vdim = v_src.shape[1]
     members = k_all.shape[1]
+    w_rows, columns = wq_ref.shape
+    half_width = tok_ref.shape[1]
     groups = group_ref.shape[0]
     half_rows = rows // 2
     sp = lax.axis_index("sp")
@@ -853,19 +537,19 @@
         remote(ref, ref, recv, recv, c_peer).wait_recv()
 
     def k_out(plane):
-        return remote(k_ref.at[plane], k_all.at[z, m], z_send.at[0, plane], z_recv.at[0, z], at(plane, m))
+        return remote(k_src.at[plane], k_all.at[z, m], z_send.at[0, plane], z_recv.at[0, z], at(plane, m))
 
     def v_out(plane):
-        return remote(v_ref.at[plane], v_all.at[z, m], z_send.at[1, plane], z_recv.at[1, z], at(plane, m))
+        return remote(v_src.at[plane], v_all.at[z, m], z_send.at[1, plane], z_recv.at[1, z], at(plane, m))
 
     def q_out(plane):
         return remote(
-            q_ref.at[plane], q_in.at[z], z_send.at[2, plane], z_recv.at[2, z], at(plane, holder(z, m))
+            q_src.at[plane], q_in.at[z], z_send.at[2, plane], z_recv.at[2, z], at(plane, holder(z, m))
         )
 
     def in_plane(plane, own):
         copies = []
-        for t, (mine, everyone) in enumerate(((k_ref, k_all), (v_ref, v_all))):
+        for t, (mine, everyone) in enumerate(((k_src, k_all), (v_src, v_all))):
             src = mine.at[plane] if own else everyone.at[plane, m]
             there = everyone.at[plane, m]
             passed = everyone.at[plane, y_member]
@@ -899,21 +583,65 @@
         arrived(v_all.at[plane, m], z_recv.at[1, plane])
         share(plane, False)
 
-    pool_rows = pool_ref.shape[1]
+    pool_rows = wp_ref.shape[0]
 
     def pool_slot(plane, member):
         start = pl.multiple_of((plane * members + member) * pool_rows, pool_rows)
         return w_pool.at[pl.ds(start, pool_rows), :]
 
-    def pool_across(plane):
-        return remote(pool_ref.at[plane], pool_slot(plane, m), py_send.at[plane], py_recv.at[plane], y_peer)
-
-    def pool_beside(plane):
-        return remote(pool_ref.at[plane], pool_slot(plane, m), pc_send.at[plane, 0], pc_recv.at[plane, 0], c_peer)
+    def pool_line(plane, up, own):
+        there = pool_slot(plane, m)
+        side = 1 if up else 0
+        return remote(
+            wp_ref if own else there,
+            there,
+            pool_send.at[plane, side],
+            pool_recv.at[plane],
+            {"sp": sp + (members if up else -members)},
+        )
+
+    def pool_across(plane, own):
+        there = pool_slot(plane, m)
+        return remote(wp_ref if own else there, there, py_send.at[plane], py_recv.at[plane], y_peer)
+
+    def pool_beside(plane, own):
+        there = pool_slot(plane, m)
+        return remote(wp_ref if own else there, there, pc_send.at[plane, 0], pc_recv.at[plane, 0], c_peer)
 
     def pool_onward(plane):
         passed = pool_slot(plane, y_member)
         return remote(passed, passed, pc_send.at[plane, 1], pc_recv.at[plane, 1], c_peer)
+
+    def pool_start():
+        @pl.when(z < planes - 1)
+        def _():
+            pool_line(z, True, True).start()
+
+        @pl.when(z > 0)
+        def _():
+            pool_line(z, False, True).start()
+
+        pool_across(z, True).start()
+        pool_beside(z, True).start()
+
+    def pool_from_line(i):
+        plane = order(i)
+        arrived(pool_slot(plane, m), pool_recv.at[plane])
+
+        @pl.when((plane < z) & (z < planes - 1))
+        def _():
+            pool_line(plane, True, False).start()
+
+        @pl.when((plane > z) & (z > 0))
+        def _():
+            pool_line(plane, False, False).start()
+
+        pool_across(plane, False).start()
+        pool_beside(plane, False).start()
+
+    def pool_from_pair(i):
+        arrived(pool_slot(order(i), y_member), py_recv.at[order(i)])
+        pool_onward(order(i)).start()
 
     out_rows, out_columns = wo_ref.shape
 
@@ -947,10 +675,10 @@
             wo_ref if own else there, there, wc_send.at[half, plane, yy], wc_recv.at[half, plane, yy], c_peer
         )
 
-    def w_spread(plane, own):
-        w_across(plane, own).start()
-        w_swap(plane, y, own).start()
-        w_beside(tp, plane, y, own).start()
+    def w_spread(plane):
+        w_across(plane, False).start()
+        w_swap(plane, y, False).start()
+        w_beside(tp, plane, y, False).start()
 
     def w_line_start():
         @pl.when(z < planes - 1)
@@ -973,7 +701,7 @@
         def _():
             w_line(plane, False, False).start()
 
-        w_spread(plane, False)
+        w_spread(plane)
 
     def w_from_pair(i):
         plane = order(i)
@@ -987,37 +715,202 @@
             arrived(out_slot(1 - tp, plane, yy, c), wx_recv.at[plane, yy])
             w_beside(1 - tp, plane, yy, False).start()
 
-    share(z, True)
-
-    @pl.when(z % 2 == 1)
-    def _():
-        q_out(z).start()
-
-    for i in range(1, planes):
-        k_out(order(i)).start()
-        v_out(order(i)).start()
-        q_out(order(i)).start()
-    for plane in range(planes):
-        pool_across(plane).start()
-        pool_beside(plane).start()
-    w_spread(z, True)
-    k_all[z, m] = k_ref[z]
-    v_all[z, m] = v_ref[z]
-    for plane in range(planes):
-        start = pl.multiple_of((plane * members + m) * pool_rows, pool_rows)
-        w_pool[pl.ds(start, pool_rows), :] = pool_ref[plane]
+    def slot(a, zz, yy, cc, first=0, count=w_rows):
+        start = pl.multiple_of((zz * members + yy * 2 + cc) * w_rows + first, count)
+        return full.at[a, pl.ds(start, count), :]
+
+    def line(a, zz, up, own):
+        there = slot(a, zz, y, c)
+        side = 1 if up else 0
+        return remote(
+            weights[a] if own else there,
+            there,
+            line_send.at[zz, side, a],
+            line_recv.at[zz, a],
+            {"sp": sp + (members if up else -members)},
+        )
+
+    def y_copy(a, i, own):
+        if i == 1:
+            there = slot(a, order(i), y, c, w_rows // 2, w_rows // 2)
+            src = there
+        else:
+            there = slot(a, order(i), y, c)
+            src = weights[a] if own else there
+        return remote(src, there, y_send.at[order(i), a], y_recv.at[order(i), a], y_peer)
+
+    def y_came(a, i):
+        there = slot(a, order(i), 1 - y, c, *((w_rows // 2, w_rows // 2) if i == 1 else ()))
+        return remote(there, there, y_send.at[order(i), a], y_recv.at[order(i), a], y_peer)
+
+    def turn(a):
+        there = slot(a, z, 1 - y, c, 0, w_rows // 2)
+        return remote(there, there, turn_send.at[a], turn_recv.at[a], at(order(1), m))
+
+    def turn_came(a):
+        there = slot(a, order(1), 1 - y, c, 0, w_rows // 2)
+        return remote(there, there, turn_send.at[a], turn_recv.at[a], at(order(1), m))
+
+    def c_copy(a, zz, yy, own):
+        there = slot(a, zz, yy, c)
+        src = weights[a] if own else there
+        return remote(src, there, c_send.at[zz, yy, a], c_recv.at[zz, yy, a], c_peer)
+
+    def c_came(a, zz, yy):
+        there = slot(a, zz, yy, 1 - c)
+        return remote(there, there, c_send.at[zz, yy, a], c_recv.at[zz, yy, a], c_peer)
+
+    def from_line(i, arrays):
+        zz = order(i)
+        for a in arrays:
+            there = slot(a, zz, y, c)
+            remote(there, there, line_send.at[zz, 0, a], line_recv.at[zz, a], c_peer).wait_recv()
+
+            @pl.when((zz < z) & (z < planes - 1))
+            def _():
+                line(a, zz, True, False).start()
+
+            @pl.when((zz > z) & (z > 0))
+            def _():
+                line(a, zz, False, False).start()
+
+            y_copy(a, i, False).start()
+            c_copy(a, zz, y, False).start()
+
+    def from_pair(i, arrays):
+        zz = order(i)
+        for a in arrays:
+            y_came(a, i).wait_recv()
+            if i == 0:
+                turn(a).start()
+            if i == 1:
+                turn_came(a).wait_recv()
+            c_copy(a, zz, 1 - y, False).start()
+
+    def multiply(i, yy, arrays):
+        zz = order(i)
+        for a in arrays:
+            c_came(a, zz, yy).wait_recv()
+        piece = zz * 2 + yy
+        start = pl.multiple_of(piece * 2 * w_rows, 2 * w_rows)
+        for a in arrays:
+            part = jnp.dot(
+                pieces[piece], full[a, pl.ds(start, 2 * w_rows), :], preferred_element_type=jnp.float32
+            )
+            product[a] += part
+
+    def own_weights(arrays):
+        for a in arrays:
+
+            @pl.when(z < planes - 1)
+            def _():
+                line(a, z, True, True).start()
+
+            @pl.when(z > 0)
+            def _():
+                line(a, z, False, True).start()
+
+            y_copy(a, 0, True).start()
+            c_copy(a, z, y, True).start()
+            full[a, pl.ds(pl.multiple_of(sp * w_rows, w_rows), w_rows), :] = weights[a][...]
+
+    swaps = (
+        remote(tok_ref, theirs, swap_sem.at[0], swap_sem.at[1], x_peer),
+        remote(gain_in, their_gain, swap_sem.at[2], swap_sem.at[3], x_peer),
+    )
+    own_weights(first_pair)
+    for swap in swaps:
+        swap.start()
+    w_swap(z, y, True).start()
+    w_beside(tp, z, y, True).start()
+    product[...] = jnp.zeros_like(product)
+    acc[...] = jnp.zeros_like(acc)
+    total[...] = jnp.zeros_like(total)
+    top[...] = jnp.full_like(top, NEG_LARGE)
+    own_pool = pl.ds(pl.multiple_of(sp * pool_rows, pool_rows), pool_rows)
+    w_pool[own_pool, :] = wp_ref[...]
     w_full[
         pl.ds(pl.multiple_of(tp * out_rows, out_rows), out_rows),
         pl.ds(pl.multiple_of(sp * out_columns, out_columns), out_columns),
     ] = wo_ref[...]
 
+    from_line(1, first_pair)
+    from_pair(0, first_pair)
+    from_line(2, first_pair)
+    for swap in swaps:
+        swap.wait()
+    squares = jnp.zeros((rows, 1), jnp.float32)
+    per_half = half_width // (2 * w_rows)
+    for ref, gains, owner in ((tok_ref, gain_in, tp), (theirs, their_gain, 1 - tp)):
+        for j in range(per_half):
+            chunk = pl.ds(j * 2 * w_rows, 2 * w_rows)
+            features = ref[:, chunk].astype(jnp.float32)
+            squares += jnp.sum(features * features, axis=1, keepdims=True)
+            scaled = (features * gains[:, chunk].astype(jnp.float32)).astype(jnp.bfloat16)
+            pieces[owner * per_half + j] = scaled
+    inverse = lax.rsqrt(squares / model_width + EPSILON)
+    inverse_sc[...] = jnp.broadcast_to(inverse, inverse_sc.shape)
+    multiply(0, y, first_pair)
+    multiply(0, 1 - y, first_pair)
+    from_line(3, first_pair)
+    own_weights(last_one)
+    from_pair(1, first_pair)
+    multiply(1, y, first_pair)
+    from_pair(2, first_pair)
+    multiply(1, 1 - y, first_pair)
+    multiply(2, y, first_pair)
+    from_line(1, last_one)
+    from_pair(0, last_one)
+    multiply(2, 1 - y, first_pair)
+    from_pair(3, first_pair)
+    multiply(3, y, first_pair)
+    multiply(3, 1 - y, first_pair)
+    width = columns // planes
+    for p in range(planes):
+        part = slice(p * width, (p + 1) * width)
+        k_src[p] = (product[0, :, part] * inverse_sc[:, :1]).astype(jnp.bfloat16)
+        v_src[p] = (product[1, :, part] * inverse_sc[:, :1]).T.astype(jnp.bfloat16)
+    k_all[z, m] = k_src[z]
+    v_all[z, m] = v_src[z]
+    share(z, True)
+    k_out(order(1)).start()
+    v_out(order(1)).start()
+    from_line(2, last_one)
+    k_out(order(2)).start()
+    v_out(order(2)).start()
+    from_pair(1, last_one)
+    multiply(0, y, last_one)
+    multiply(0, 1 - y, last_one)
+    from_line(3, last_one)
+    k_out(order(3)).start()
+    v_out(order(3)).start()
+    from_pair(2, last_one)
+    hand_on(z, True)
+    multiply(1, y, last_one)
+    multiply(1, 1 - y, last_one)
+    multiply(2, y, last_one)
+    multiply(2, 1 - y, last_one)
+    from_pair(3, last_one)
+    multiply(3, y, last_one)
+    multiply(3, 1 - y, last_one)
+    for p in range(planes):
+        part = slice(p * width, (p + 1) * width)
+        query = (product[2, :, part] * inverse_sc[:, :1]).astype(jnp.bfloat16)
+        q_src[p] = query * (1.0 / math.sqrt(hdim))
+
     @pl.when(z % 2 == 0)
     def _():
-        q_in[z] = q_ref[z]
-
-    acc[...] = jnp.zeros_like(acc)
-    total[...] = jnp.zeros_like(total)
-    top[...] = jnp.full_like(top, NEG_LARGE)
+        q_in[z] = q_src[z]
+
+    @pl.when(z % 2 == 1)
+    def _():
+        q_out(z).start()
+
+    for i in range(1, planes):
+        q_out(order(i)).start()
+    w_across(z, True).start()
+    w_line_start()
+    pool_start()
 
     def visit(block, plane, first, count, masked):
         query = q_in[block]
@@ -1103,9 +996,10 @@
     def pool_project():
         for plane in range(planes):
             arrived(pool_slot(plane, c_member), pc_recv.at[plane, 0])
-            arrived(pool_slot(plane, members - 1 - m), pc_recv.at[plane, 1])
-        product = jnp.dot(scaled_ref[...], w_pool[...], preferred_element_type=jnp.float32)
-        pool_sc[...] = (product * inverse_ref[:, :1]).astype(jnp.bfloat16)
+            arrived(pool_slot(plane, turned), pc_recv.at[plane, 1])
+        scaled = jnp.concatenate([pieces[j] for j in range(pieces.shape[0])], axis=1)
+        pool_in = jnp.dot(scaled, w_pool[...], preferred_element_type=jnp.float32)
+        pool_sc[...] = (pool_in * inverse_sc[:, :1]).astype(jnp.bfloat16)
 
         @pl.when(sp < n_sp - 1)
         def _():
@@ -1139,17 +1033,12 @@
             pooled_sc[g] = jnp.where(tp == 0, high, low)
         half_out().start()
 
-    hand_on(z, True)
     shared(z, True)
 
     @pl.when(z % 2 == 1)
     def _():
         arrived(q_in.at[z], z_recv.at[2, z])
 
-    for plane in range(planes):
-        arrived(pool_slot(plane, y_member), py_recv.at[plane])
-        pool_onward(plane).start()
-
     def stage(i, carry):
         block = order(i)
 
@@ -1157,10 +1046,6 @@
         def _():
             landed(i + 1)
 
-        @pl.when(i == LINE_STAGE)
-        def _():
-            w_line_start()
-
         diagonal(block)
 
         @pl.when(i < planes - 1)
@@ -1169,22 +1054,24 @@
 
         @pl.when(i == 0)
         def _():
-            pool_project()
             w_from_pair(0)
 
         @pl.when(i == 1)
         def _():
-            pool_mix()
-            w_from_swap(0)
+            pool_from_pair(0)
 
         @pl.when(i == planes - 1)
         def _():
-            w_from_line(1)
             finish(0)
 
         def pair(j, carry):
             other = jnp.where(i < planes - 1, order(j), j + upper)
             visit(jnp.maximum(block, other), jnp.minimum(block, other), 0, members, False)
+
+            @pl.when((i == planes - 2) & (j == i - 1))
+            def _():
+                w_from_line(1)
+                pool_from_line(1)
 
             @pl.when(i == planes - 1)
             def _():
@@ -1194,11 +1081,13 @@
                 def _():
                     w_from_pair(1)
                     w_from_line(2)
+                    pool_from_line(2)
 
                 @pl.when(j == 1)
                 def _():
                     w_from_pair(2)
                     w_from_line(3)
+                    pool_from_line(3)
 
             return carry
 
@@ -1212,9 +1101,16 @@
         return carry
 
     lax.fori_loop(0, planes, stage, 0)
+    w_from_swap(0)
+    pool_from_pair(1)
+    pool_from_pair(2)
     w_from_pair(3)
-    for i in range(1, planes):
-        w_from_swap(i)
+    pool_from_pair(3)
+    pool_project()
+    w_from_swap(1)
+    pool_mix()
+    w_from_swap(2)
+    w_from_swap(3)
 
     for head in range(2 * planes):
         own_head = tp * planes + z == head
@@ -1230,10 +1126,10 @@
             for yy in range(2):
                 arrived(out_slot(half, plane, yy, 1 - c), wc_recv.at[half, plane, yy])
     left = jnp.concatenate([branch[head] for head in range(2 * planes)], axis=1)
-    width = out_ref.shape[1] // planes
+    out_width = out_ref.shape[1] // planes
 
     def column(n, carry):
-        part = pl.ds(pl.multiple_of(n * width, width), width)
+        part = pl.ds(pl.multiple_of(n * out_width, out_width), out_width)
         out_ref[:, part] = jnp.dot(
             left, w_full[:, part], preferred_element_type=jnp.float32
         ).astype(jnp.bfloat16)
@@ -1255,7 +1151,13 @@
         for copies in in_plane(plane, i == 0):
             for copy in copies:
                 copy.wait_send()
-        w_across(plane, i == 0).wait_send()
+        w_across(plane, False).wait_send()
+        for a in first_pair + last_one:
+            y_copy(a, i, False).wait_send()
+            c_copy(a, plane, y, False).wait_send()
+            c_copy(a, plane, 1 - y, False).wait_send()
+            if i == 0:
+                turn(a).wait_send()
         for yy in (y, 1 - y):
             w_swap(plane, yy, False).wait_send()
             w_beside(0, plane, yy, False).wait_send()
@@ -1264,14 +1166,20 @@
         @pl.when((plane <= z) & (z < planes - 1))
         def _():
             w_line(plane, True, False).wait_send()
+            pool_line(plane, True, False).wait_send()
+            for a in first_pair + last_one:
+                line(a, plane, True, False).wait_send()
 
         @pl.when((plane >= z) & (z > 0))
         def _():
             w_line(plane, False, False).wait_send()
+            pool_line(plane, False, False).wait_send()
+            for a in first_pair + last_one:
+                line(a, plane, False, False).wait_send()
 
     for plane in range(planes):
-        pool_across(plane).wait_send()
-        pool_beside(plane).wait_send()
+        pool_across(plane, False).wait_send()
+        pool_beside(plane, False).wait_send()
         pool_onward(plane).wait_send()
         result_copy(plane, 1 - tp).wait_send()
 
@@ -1286,37 +1194,69 @@
         edge_out().wait_send()
 
 
-def attend_and_project(
-    queries, keys, values, lambdas, sub_gain, scaled, inverse, pool_lines, group_weight, pool_scale, w_out
+def whole_layer(
+    tokens,
+    pre_gain,
+    w_query,
+    w_key,
+    w_value,
+    w_pool,
+    lambdas,
+    sub_gain,
+    group_weight,
+    pool_scale,
+    w_out,
 ):
-    planes, rows, width = queries.shape
-    vdim = values.shape[1]
+    planes = lambdas.shape[0]
+    rows, half_width = tokens.shape
     n_sp = lax.axis_size("sp")
     members = n_sp // planes
-    groups, group_dim, _ = group_weight.shape
+    w_rows, columns = w_query.shape
+    model_width = n_sp * w_rows
+    width = columns // planes
+    groups, vdim, _ = group_weight.shape
     out_rows, out_columns = w_out.shape
     vmem = pl.BlockSpec(memory_space=pltpu.VMEM)
     dma = pltpu.SemaphoreType.DMA
+    bf16, f32 = jnp.bfloat16, jnp.float32
     work = planes * rows * members * planes * rows
     return pl.pallas_call(
-        functools.partial(mix, width // 2),
-        out_shape=jax.ShapeDtypeStruct((rows // 2, n_sp * out_columns), jnp.bfloat16),
+        functools.partial(layer, width // 2, model_width),
+        out_shape=jax.ShapeDtypeStruct((rows // 2, n_sp * out_columns), bf16),
         in_specs=[pl.BlockSpec(memory_space=pltpu.SMEM)] + [vmem] * 10,
         out_specs=vmem,
         scratch_shapes=[
-            pltpu.VMEM((planes, rows, width), jnp.bfloat16),
-            pltpu.VMEM((planes, members, rows, width), jnp.bfloat16),
-            pltpu.VMEM((planes, members, vdim, rows), jnp.bfloat16),
-            pltpu.VMEM((planes, vdim, 2 * rows), jnp.float32),
-            pltpu.VMEM((planes, 1, 2 * rows), jnp.float32),
-            pltpu.VMEM((planes, 8, 2 * rows), jnp.float32),
-            pltpu.VMEM((planes, rows, vdim), jnp.bfloat16),
-            pltpu.VMEM((scaled.shape[1], groups * group_dim), jnp.bfloat16),
-            pltpu.VMEM((2 * out_rows, n_sp * out_columns), jnp.bfloat16),
-            pltpu.VMEM((2 * planes, rows // 2, 2 * vdim), jnp.bfloat16),
-            pltpu.VMEM((rows, groups * group_dim), jnp.bfloat16),
-            pltpu.VMEM((RIM_ROWS + 1, groups * group_dim), jnp.bfloat16),
-            pltpu.VMEM((groups, rows // 2, group_dim), jnp.bfloat16),
+            pltpu.VMEM((3, model_width, columns), bf16),
+            pltpu.VMEM((rows, half_width), bf16),
+            pltpu.VMEM((1, half_width), bf16),
+            pltpu.VMEM((model_width // (2 * w_rows), rows, 2 * w_rows), bf16),
+            pltpu.VMEM((3, rows, columns), f32),
+            pltpu.VMEM((rows, 128), f32),
+            pltpu.VMEM((planes, rows, width), bf16),
+            pltpu.VMEM((planes, vdim, rows), bf16),
+            pltpu.VMEM((planes, rows, width), bf16),
+            pltpu.VMEM((planes, rows, width), bf16),
+            pltpu.VMEM((planes, members, rows, width), bf16),
+            pltpu.VMEM((planes, members, vdim, rows), bf16),
+            pltpu.VMEM((planes, vdim, 2 * rows), f32),
+            pltpu.VMEM((planes, 1, 2 * rows), f32),
+            pltpu.VMEM((planes, 8, 2 * rows), f32),
+            pltpu.VMEM((planes, rows, vdim), bf16),
+            pltpu.VMEM((model_width, groups * vdim), bf16),
+            pltpu.VMEM((2 * out_rows, n_sp * out_columns), bf16),
+            pltpu.VMEM((2 * planes, rows // 2, 2 * vdim), bf16),
+            pltpu.VMEM((rows, groups * vdim), bf16),
+            pltpu.VMEM((RIM_ROWS + 1, groups * vdim), bf16),
+            pltpu.VMEM((groups, rows // 2, vdim), bf16),
+            dma((planes, 2, 3)),
+            dma((planes, 3)),
+            dma((planes, 3)),
+            dma((planes, 3)),
+            dma((planes, 2, 3)),
+            dma((planes, 2, 3)),
+            dma((3,)),
+            dma((3,)),
+            dma((4,)),
             dma((3, planes)),
             dma((3, planes)),
             dma((planes, 3, 2)),
@@ -1331,6 +1271,8 @@
             dma((2,)),
             dma((planes, 2)),
             dma((planes,)),
+            dma((planes, 2)),
+            dma((planes,)),
             dma((planes,)),
             dma((planes,)),
             dma((planes, 2)),
@@ -1342,17 +1284,17 @@
             vmem_limit_bytes=60 * 2**20, collective_id=2, has_side_effects=True
         ),
         cost_estimate=pl.CostEstimate(
-            flops=4 * work * vdim, bytes_accessed=keys.size * 8, transcendentals=work
+            flops=4 * work * vdim, bytes_accessed=2**24, transcendentals=work
         ),
     )(
         lambdas,
-        queries,
-        keys,
-        values,
+        tokens,
+        pre_gain.reshape(1, -1),
+        w_key,
+        w_value,
+        w_query,
+        w_pool,
         sub_gain.reshape(1, -1),
-        scaled,
-        inverse,
-        pool_lines,
         group_weight,
         pool_scale.reshape(1, -1),
         w_out,
@@ -1439,18 +1381,15 @@
 
     shaped_for_mix = n_tp == 2 and heads == 4 and n_sp == 4 * heads and tok_rows % 32 == 0
     if shaped_for_mix and qdim == vdim == group_dim and groups == heads:
-        queries, key_rows, values, scaled, inverse, pool_lines = gather_and_project(
-            tokens, pre_gain, w_query, w_key, w_value, w_pool, heads
-        )
-        return attend_and_project(
-            queries,
-            key_rows,
-            values,
+        return whole_layer(
+            tokens,
+            pre_gain,
+            w_query,
+            w_key,
+            w_value,
+            w_pool,
             lambdas,
             sub_gain,
-            scaled,
-            inverse,
-            pool_lines,
             group_weight,
             pool_scale,
             w_out,

time: 164 us -> 155 us (0.945)
  Pallas kernels: 159 us -> 151 us
    pallas_call x2 -> x1, Pallas kernels: 159 us -> 151 us  [whole_layer(): pl.pallas_call(functools.partial(layer, width // 2, model_width), out_sha...]
where the time goes in v4:
time: 155 us
  Pallas kernels  151 us (97%)
  local copies, waits for them, and re-layouts  3.37 us (2%)
    pallas_call x1, Pallas kernels, whole_layer(): pl.pallas_call(functools.partial(layer, width // 2, model_width), out_sha...  151 us

profile of v4, /device:TPU:0, one launch (start us, length us, event | category | flops | bytes accessed | tf_op | source)
XLA Modules:
  0.0 154.6 jit_solution(3579544674037268941)
XLA Ops:
  0.0 0.0 copy-start
  0.0 0.7 copy-done
  0.7 0.6 reshape.9.gain_in
  1.3 151.3 %shard_map.109 = bf16[192,2048]{1,0:T(8,128)(2,1)} custom-call(f32[4]{0:T(128)} %lam_ref.1, bf16[384,1024]{1,0:T(8,128)(2,1)} %tok_ref.1, bf16[1,1024]{1,0:T(2,128)(2,1)} %reshape.9.gain_in, bf16[128,512]{1,0:T(8,128)(2,1)} %wk_ref.1, bf16[128,512]{1,0:T(8,128)(2,1)} %wv_ref.1, bf16[128,512]{1,0:T(8,128)(2,1)} %wq_ref.1, bf16[128,512]{1,0:T(8,128)(2,1)} %wp_ref.1, ...), custom_call_target="tpu_custom_call" | custom-call | flops 4831838208 | bytes 16777216 | tf_op jit(solution)/shard_map/pallas_call | solution.py:1223
  152.6 2.1 %copy.13 = bf16[192,2048]{1,0:T(8,128)(2,1)} copy(bf16[192,2048]{1,0:T(8,128)(2,1)} %shard_map.109) | data formatting | bytes 1572864
Async XLA Ops:
  0.0 0.7 copy-start

commit v5 on v4

--- a/solution.py
+++ b/solution.py
@@ -467,10 +467,10 @@
     pooled_sc,
     *sems,
 ):
-    (line_send, line_recv, y_send, y_recv, c_send, c_recv, turn_send, turn_recv, swap_sem) = sems[:9]
-    (z_send, z_recv, in_send, in_recv, back_send, back_recv) = sems[9:15]
-    (py_send, py_recv, pc_send, pc_recv, edge_sem, half_sem, pool_send, pool_recv) = sems[15:23]
-    (wl_send, wl_recv, wy_send, wy_recv, wx_send, wx_recv, wc_send, wc_recv) = sems[23:]
+    (line_send, line_recv, y_send, y_recv, c_send, c_recv, swap_sem) = sems[:7]
+    (z_send, z_recv, in_send, in_recv, back_send, back_recv) = sems[7:13]
+    (py_send, py_recv, pc_send, pc_recv, edge_sem, half_sem, pool_send, pool_recv) = sems[13:21]
+    (wl_send, wl_recv, wy_send, wy_recv, wx_send, wx_recv, wc_send, wc_recv) = sems[21:]
     weights = (wk_ref, wv_ref, wq_ref)
     first_pair, last_one = (0, 1), (2,)
     planes, rows, _ = q_src.shape
@@ -491,6 +491,9 @@
     c_member = m + 1 - 2 * c
     turned = members - 1 - m
     upper = z // 2
+    between = (z > 0) & (z < planes - 1)
+    turn = [jnp.where(between, 1 + i % 3, i) for i in range(planes)]
+    turn[0] = 0
 
     def at(plane, member, half=None):
         device = {"sp": plane * members + member}
@@ -589,16 +592,12 @@
         start = pl.multiple_of((plane * members + member) * pool_rows, pool_rows)
         return w_pool.at[pl.ds(start, pool_rows), :]
 
-    def pool_line(plane, up, own):
-        there = pool_slot(plane, m)
-        side = 1 if up else 0
-        return remote(
-            wp_ref if own else there,
-            there,
-            pool_send.at[plane, side],
-            pool_recv.at[plane],
-            {"sp": sp + (members if up else -members)},
-        )
+    def pool_line(i):
+        return remote(wp_ref, pool_slot(z, m), pool_send.at[i - 1], pool_recv.at[z], at(order(i), m))
+
+    def pool_line_on(i):
+        there = pool_slot(order(i), m)
+        return remote(there, there, pool_send.at[i], pool_recv.at[order(i)], at(order(1), m))
 
     def pool_across(plane, own):
         there = pool_slot(plane, m)
@@ -613,28 +612,17 @@
         return remote(passed, passed, pc_send.at[plane, 1], pc_recv.at[plane, 1], c_peer)
 
     def pool_start():
-        @pl.when(z < planes - 1)
-        def _():
-            pool_line(z, True, True).start()
-
-        @pl.when(z > 0)
-        def _():
-            pool_line(z, False, True).start()
-
-        pool_across(z, True).start()
-        pool_beside(z, True).start()
+        pool_line(1).start()
+        pool_line(2).start()
 
     def pool_from_line(i):
         plane = order(i)
         arrived(pool_slot(plane, m), pool_recv.at[plane])
-
-        @pl.when((plane < z) & (z < planes - 1))
-        def _():
-            pool_line(plane, True, False).start()
-
-        @pl.when((plane > z) & (z > 0))
-        def _():
-            pool_line(plane, False, False).start()
+        if i > 1:
+
+            @pl.when(between)
+            def _():
+                pool_line_on(i).start()
 
         pool_across(plane, False).start()
         pool_beside(plane, False).start()
@@ -650,16 +638,12 @@
         column = pl.multiple_of((plane * members + yy * 2 + cc) * out_columns, out_columns)
         return w_full.at[pl.ds(first, out_rows), pl.ds(column, out_columns)]
 
-    def w_line(plane, up, own):
-        there = out_slot(tp, plane, y, c)
-        side = 1 if up else 0
-        return remote(
-            wo_ref if own else there,
-            there,
-            wl_send.at[plane, side],
-            wl_recv.at[plane],
-            {"sp": sp + (members if up else -members)},
-        )
+    def w_line(i):
+        return remote(wo_ref, out_slot(tp, z, y, c), wl_send.at[i - 1], wl_recv.at[z], at(order(i), m))
+
+    def w_line_on(i):
+        there = out_slot(tp, order(i), y, c)
+        return remote(there, there, wl_send.at[i], wl_recv.at[order(i)], at(order(1), m))
 
     def w_across(plane, own):
         there = out_slot(tp, plane, y, c)
@@ -675,33 +659,21 @@
             wo_ref if own else there, there, wc_send.at[half, plane, yy], wc_recv.at[half, plane, yy], c_peer
         )
 
-    def w_spread(plane):
-        w_across(plane, False).start()
-        w_swap(plane, y, False).start()
-        w_beside(tp, plane, y, False).start()
-
     def w_line_start():
-        @pl.when(z < planes - 1)
-        def _():
-            w_line(z, True, True).start()
-
-        @pl.when(z > 0)
-        def _():
-            w_line(z, False, True).start()
+        w_line(1).start()
+        w_line(2).start()
 
     def w_from_line(i):
         plane = order(i)
         arrived(out_slot(tp, plane, y, c), wl_recv.at[plane])
-
-        @pl.when((plane < z) & (z < planes - 1))
-        def _():
-            w_line(plane, True, False).start()
-
-        @pl.when((plane > z) & (z > 0))
-        def _():
-            w_line(plane, False, False).start()
-
-        w_spread(plane)
+        if i > 1:
+
+            @pl.when(between)
+            def _():
+                w_line_on(i).start()
+
+        w_swap(plane, y, False).start()
+        w_beside(tp, plane, y, False).start()
 
     def w_from_pair(i):
         plane = order(i)
@@ -715,41 +687,22 @@
             arrived(out_slot(1 - tp, plane, yy, c), wx_recv.at[plane, yy])
             w_beside(1 - tp, plane, yy, False).start()
 
-    def slot(a, zz, yy, cc, first=0, count=w_rows):
-        start = pl.multiple_of((zz * members + yy * 2 + cc) * w_rows + first, count)
-        return full.at[a, pl.ds(start, count), :]
-
-    def line(a, zz, up, own):
-        there = slot(a, zz, y, c)
-        side = 1 if up else 0
-        return remote(
-            weights[a] if own else there,
-            there,
-            line_send.at[zz, side, a],
-            line_recv.at[zz, a],
-            {"sp": sp + (members if up else -members)},
-        )
+    def slot(a, zz, yy, cc):
+        start = pl.multiple_of((zz * members + yy * 2 + cc) * w_rows, w_rows)
+        return full.at[a, pl.ds(start, w_rows), :]
+
+    def line(a, i):
+        there = slot(a, z, y, c)
+        return remote(weights[a], there, line_send.at[i - 1, a], line_recv.at[z, a], at(order(i), m))
+
+    def line_on(a, i):
+        there = slot(a, order(i), y, c)
+        return remote(there, there, line_send.at[i, a], line_recv.at[order(i), a], at(order(1), m))
 
     def y_copy(a, i, own):
-        if i == 1:
-            there = slot(a, order(i), y, c, w_rows // 2, w_rows // 2)
-            src = there
-        else:
-            there = slot(a, order(i), y, c)
-            src = weights[a] if own else there
+        there = slot(a, order(i), y, c)
+        src = weights[a] if own else there
         return remote(src, there, y_send.at[order(i), a], y_recv.at[order(i), a], y_peer)
-
-    def y_came(a, i):
-        there = slot(a, order(i), 1 - y, c, *((w_rows // 2, w_rows // 2) if i == 1 else ()))
-        return remote(there, there, y_send.at[order(i), a], y_recv.at[order(i), a], y_peer)
-
-    def turn(a):
-        there = slot(a, z, 1 - y, c, 0, w_rows // 2)
-        return remote(there, there, turn_send.at[a], turn_recv.at[a], at(order(1), m))
-
-    def turn_came(a):
-        there = slot(a, order(1), 1 - y, c, 0, w_rows // 2)
-        return remote(there, there, turn_send.at[a], turn_recv.at[a], at(order(1), m))
 
     def c_copy(a, zz, yy, own):
         there = slot(a, zz, yy, c)
@@ -763,16 +716,11 @@
     def from_line(i, arrays):
         zz = order(i)
         for a in arrays:
-            there = slot(a, zz, y, c)
-            remote(there, there, line_send.at[zz, 0, a], line_recv.at[zz, a], c_peer).wait_recv()
-
-            @pl.when((zz < z) & (z < planes - 1))
+            arrived(slot(a, zz, y, c), line_recv.at[zz, a])
+
+            @pl.when(between & (i > 1))
             def _():
-                line(a, zz, True, False).start()
-
-            @pl.when((zz > z) & (z > 0))
-            def _():
-                line(a, zz, False, False).start()
+                line_on(a, i).start()
 
             y_copy(a, i, False).start()
             c_copy(a, zz, y, False).start()
@@ -780,11 +728,7 @@
     def from_pair(i, arrays):
         zz = order(i)
         for a in arrays:
-            y_came(a, i).wait_recv()
-            if i == 0:
-                turn(a).start()
-            if i == 1:
-                turn_came(a).wait_recv()
+            arrived(slot(a, zz, 1 - y, c), y_recv.at[zz, a])
             c_copy(a, zz, 1 - y, False).start()
 
     def multiply(i, yy, arrays):
@@ -801,15 +745,8 @@
 
     def own_weights(arrays):
         for a in arrays:
-
-            @pl.when(z < planes - 1)
-            def _():
-                line(a, z, True, True).start()
-
-            @pl.when(z > 0)
-            def _():
-                line(a, z, False, True).start()
-
+            line(a, 2).start()
+            line(a, 1).start()
             y_copy(a, 0, True).start()
             c_copy(a, z, y, True).start()
             full[a, pl.ds(pl.multiple_of(sp * w_rows, w_rows), w_rows), :] = weights[a][...]
@@ -821,6 +758,7 @@
     own_weights(first_pair)
     for swap in swaps:
         swap.start()
+    own_weights(last_one)
     w_swap(z, y, True).start()
     w_beside(tp, z, y, True).start()
     product[...] = jnp.zeros_like(product)
@@ -834,9 +772,14 @@
         pl.ds(pl.multiple_of(sp * out_columns, out_columns), out_columns),
     ] = wo_ref[...]
 
-    from_line(1, first_pair)
+    from_line(turn[1], first_pair)
+    from_line(turn[2], first_pair)
     from_pair(0, first_pair)
-    from_line(2, first_pair)
+    from_line(turn[1], last_one)
+    from_line(turn[2], last_one)
+    from_pair(0, last_one)
+    from_line(turn[3], first_pair)
+    from_pair(turn[1], first_pair)
     for swap in swaps:
         swap.wait()
     squares = jnp.zeros((rows, 1), jnp.float32)
@@ -850,21 +793,21 @@
             pieces[owner * per_half + j] = scaled
     inverse = lax.rsqrt(squares / model_width + EPSILON)
     inverse_sc[...] = jnp.broadcast_to(inverse, inverse_sc.shape)
-    multiply(0, y, first_pair)
-    multiply(0, 1 - y, first_pair)
-    from_line(3, first_pair)
-    own_weights(last_one)
-    from_pair(1, first_pair)
-    multiply(1, y, first_pair)
-    from_pair(2, first_pair)
-    multiply(1, 1 - y, first_pair)
-    multiply(2, y, first_pair)
-    from_line(1, last_one)
-    from_pair(0, last_one)
-    multiply(2, 1 - y, first_pair)
-    from_pair(3, first_pair)
-    multiply(3, y, first_pair)
-    multiply(3, 1 - y, first_pair)
+    every = first_pair + last_one
+    multiply(0, y, every)
+    multiply(0, 1 - y, every)
+    from_line(turn[3], last_one)
+    w_line_start()
+    from_pair(turn[1], last_one)
+    multiply(turn[1], y, every)
+    from_pair(turn[2], first_pair)
+    multiply(turn[1], 1 - y, every)
+    from_pair(turn[2], last_one)
+    multiply(turn[2], y, every)
+    multiply(turn[2], 1 - y, every)
+    multiply(turn[3], y, first_pair)
+    from_pair(turn[3], first_pair)
+    multiply(turn[3], 1 - y, first_pair)
     width = columns // planes
     for p in range(planes):
         part = slice(p * width, (p + 1) * width)
@@ -873,26 +816,13 @@
     k_all[z, m] = k_src[z]
     v_all[z, m] = v_src[z]
     share(z, True)
-    k_out(order(1)).start()
-    v_out(order(1)).start()
-    from_line(2, last_one)
-    k_out(order(2)).start()
-    v_out(order(2)).start()
-    from_pair(1, last_one)
-    multiply(0, y, last_one)
-    multiply(0, 1 - y, last_one)
-    from_line(3, last_one)
-    k_out(order(3)).start()
-    v_out(order(3)).start()
-    from_pair(2, last_one)
-    hand_on(z, True)
-    multiply(1, y, last_one)
-    multiply(1, 1 - y, last_one)
-    multiply(2, y, last_one)
-    multiply(2, 1 - y, last_one)
-    from_pair(3, last_one)
-    multiply(3, y, last_one)
-    multiply(3, 1 - y, last_one)
+    w_across(z, True).start()
+    for i in range(1, planes):
+        k_out(order(i)).start()
+        v_out(order(i)).start()
+    from_pair(turn[3], last_one)
+    multiply(turn[3], y, last_one)
+    multiply(turn[3], 1 - y, last_one)
     for p in range(planes):
         part = slice(p * width, (p + 1) * width)
         query = (product[2, :, part] * inverse_sc[:, :1]).astype(jnp.bfloat16)
@@ -908,9 +838,13 @@
 
     for i in range(1, planes):
         q_out(order(i)).start()
-    w_across(z, True).start()
-    w_line_start()
     pool_start()
+    w_from_line(1)
+
+    @pl.when(between)
+    def _():
+        w_from_line(2)
+        w_from_line(3)
 
     def visit(block, plane, first, count, masked):
         query = q_in[block]
@@ -1033,6 +967,8 @@
             pooled_sc[g] = jnp.where(tp == 0, high, low)
         half_out().start()
 
+    hand_on(z, True)
+    landed(1)
     shared(z, True)
 
     @pl.when(z % 2 == 1)
@@ -1042,23 +978,36 @@
     def stage(i, carry):
         block = order(i)
 
+        @pl.when(i < planes - 2)
+        def _():
+            landed(i + 2)
+
+        @pl.when(i == planes - 3)
+        def _():
+            w_across(order(1), False).start()
+
+            @pl.when(between)
+            def _():
+                w_across(order(2), False).start()
+                w_across(order(3), False).start()
+
+            pool_across(z, True).start()
+            pool_beside(z, True).start()
+
+        @pl.when(i == planes - 2)
+        def _():
+            w_from_pair(0)
+
+            @pl.when(jnp.logical_not(between))
+            def _():
+                w_from_line(2)
+                w_across(order(2), False).start()
+
+        diagonal(block)
+
         @pl.when(i < planes - 1)
         def _():
-            landed(i + 1)
-
-        diagonal(block)
-
-        @pl.when(i < planes - 1)
-        def _():
             hand_on(order(i + 1), False)
-
-        @pl.when(i == 0)
-        def _():
-            w_from_pair(0)
-
-        @pl.when(i == 1)
-        def _():
-            pool_from_pair(0)
 
         @pl.when(i == planes - 1)
         def _():
@@ -1068,26 +1017,23 @@
             other = jnp.where(i < planes - 1, order(j), j + upper)
             visit(jnp.maximum(block, other), jnp.minimum(block, other), 0, members, False)
 
-            @pl.when((i == planes - 2) & (j == i - 1))
-            def _():
-                w_from_line(1)
-                pool_from_line(1)
-
             @pl.when(i == planes - 1)
             def _():
                 finish(j + 1)
 
                 @pl.when(j == 0)
                 def _():
-                    w_from_pair(1)
-                    w_from_line(2)
-                    pool_from_line(2)
+                    @pl.when(jnp.logical_not(between))
+                    def _():
+                        w_from_line(3)
+                        w_across(order(3), False).start()
+
+                    pool_from_line(1)
 
                 @pl.when(j == 1)
                 def _():
-                    w_from_pair(2)
-                    w_from_line(3)
-                    pool_from_line(3)
+                    w_from_pair(1)
+                    pool_from_line(2)
 
             return carry
 
@@ -1101,15 +1047,17 @@
         return carry
 
     lax.fori_loop(0, planes, stage, 0)
+
+    w_from_pair(2)
+    pool_from_line(3)
     w_from_swap(0)
-    pool_from_pair(1)
-    pool_from_pair(2)
     w_from_pair(3)
-    pool_from_pair(3)
+    w_from_swap(1)
+    for i in range(planes):
+        pool_from_pair(i)
     pool_project()
-    w_from_swap(1)
+    w_from_swap(2)
     pool_mix()
-    w_from_swap(2)
     w_from_swap(3)
 
     for head in range(2 * planes):
@@ -1156,26 +1104,24 @@
             y_copy(a, i, False).wait_send()
             c_copy(a, plane, y, False).wait_send()
             c_copy(a, plane, 1 - y, False).wait_send()
-            if i == 0:
-                turn(a).wait_send()
         for yy in (y, 1 - y):
             w_swap(plane, yy, False).wait_send()
             w_beside(0, plane, yy, False).wait_send()
             w_beside(1, plane, yy, False).wait_send()
 
-        @pl.when((plane <= z) & (z < planes - 1))
-        def _():
-            w_line(plane, True, False).wait_send()
-            pool_line(plane, True, False).wait_send()
+    for i in (1, 2):
+        w_line(i).wait_send()
+        pool_line(i).wait_send()
+        for a in first_pair + last_one:
+            line(a, i).wait_send()
+
+    @pl.when(between)
+    def _():
+        for i in (2, 3):
+            w_line_on(i).wait_send()
+            pool_line_on(i).wait_send()
             for a in first_pair + last_one:
-                line(a, plane, True, False).wait_send()
-
-        @pl.when((plane >= z) & (z > 0))
-        def _():
-            w_line(plane, False, False).wait_send()
-            pool_line(plane, False, False).wait_send()
-            for a in first_pair + last_one:
-                line(a, plane, False, False).wait_send()
+                line_on(a, i).wait_send()
 
     for plane in range(planes):
         pool_across(plane, False).wait_send()
@@ -1248,14 +1194,12 @@
             pltpu.VMEM((rows, groups * vdim), bf16),
             pltpu.VMEM((RIM_ROWS + 1, groups * vdim), bf16),
             pltpu.VMEM((groups, rows // 2, vdim), bf16),
-            dma((planes, 2, 3)),
+            dma((planes, 3)),
             dma((planes, 3)),
             dma((planes, 3)),
             dma((planes, 3)),
             dma((planes, 2, 3)),
             dma((planes, 2, 3)),
-            dma((3,)),
-            dma((3,)),
             dma((4,)),
             dma((3, planes)),
             dma((3, planes)),
@@ -1269,9 +1213,9 @@
             dma((planes, 2)),
             dma((2,)),
             dma((2,)),
-            dma((planes, 2)),
             dma((planes,)),
-            dma((planes, 2)),
+            dma((planes,)),
+            dma((planes,)),
             dma((planes,)),
             dma((planes,)),
             dma((planes,)),

time: 155 us -> 137 us (0.88); the launches traced: 155 us -> 134 us
  Pallas kernels: 151 us -> 131 us
    pallas_call x1, Pallas kernels: 151 us -> 131 us  [whole_layer(): pl.pallas_call(functools.partial(layer, width // 2, model_width), out_sha...]
where the time goes in v5:
time: 137 us; the launch traced here: 134 us
  Pallas kernels  131 us (96%)
  local copies, waits for them, and re-layouts  3.37 us (2%)
    pallas_call x1, Pallas kernels, whole_layer(): pl.pallas_call(functools.partial(layer, width // 2, model_width), out_sha...  131 us
    unnamed x3, local copies, waits for them, and re-layouts  2.77 us

profile of v5, /device:TPU:0, one launch (start us, length us, event | category | flops | bytes accessed | tf_op | source)
XLA Modules:
  0.0 134.1 jit_solution(9579731998865106370)
XLA Ops:
  0.0 0.0 copy-start
  0.0 0.7 copy-done
  0.7 0.6 reshape.9.gain_in
  1.3 130.7 %shard_map.109 = bf16[192,2048]{1,0:T(8,128)(2,1)} custom-call(f32[4]{0:T(128)} %lam_ref.1, bf16[384,1024]{1,0:T(8,128)(2,1)} %tok_ref.1, bf16[1,1024]{1,0:T(2,128)(2,1)} %reshape.9.gain_in, bf16[128,512]{1,0:T(8,128)(2,1)} %wk_ref.1, bf16[128,512]{1,0:T(8,128)(2,1)} %wv_ref.1, bf16[128,512]{1,0:T(8,128)(2,1)} %wq_ref.1, bf16[128,512]{1,0:T(8,128)(2,1)} %wp_ref.1, ...), custom_call_target="tpu_custom_call" | custom-call | flops 4831838208 | bytes 16777216 | tf_op jit(solution)/shard_map/pallas_call | solution.py:1169
  132.0 2.1 %copy.13 = bf16[192,2048]{1,0:T(8,128)(2,1)} copy(bf16[192,2048]{1,0:T(8,128)(2,1)} %shard_map.109) | data formatting | bytes 1572864
Async XLA Ops:
  0.0 0.7 copy-start

commit v6 on v5

--- a/solution.py
+++ b/solution.py
@@ -505,9 +505,6 @@
     c_peer = at(z, c_member)
     x_peer = {"tp": 1 - tp}
 
-    def holder(block, member):
-        return member + (block % 2) * (members - 1 - 2 * member)
-
     def order(i):
         return arrival(z, i)
 
@@ -518,13 +515,22 @@
 
     for i in range(1, planes):
         greet(at(order(i), m))
-        greet(at(order(i), turned))
-    for member in (turned, y_member, c_member):
-        greet(at(z, member))
+    for member in range(1, members):
+        greet(at(z, (m + member) % members))
     for plane in range(planes):
         greet(at(plane, m, 1 - tp))
-        greet(at(plane, turned, 1 - tp))
-    pl.semaphore_wait(barrier, 4 * planes + 1)
+
+    @pl.when((m == 0) & (z > 0))
+    def _():
+        greet({"sp": sp - 1})
+
+    @pl.when((m == members - 1) & (z < planes - 1))
+    def _():
+        greet({"sp": sp + 1})
+
+    beyond = jnp.where((m == 0) & (z > 0), 1, 0)
+    beyond += jnp.where((m == members - 1) & (z < planes - 1), 1, 0)
+    pl.semaphore_wait(barrier, 2 * planes + members - 2 + beyond)
 
     def remote(src, dst, send, recv, device):
         return pltpu.make_async_remote_copy(
@@ -547,7 +553,7 @@
 
     def q_out(plane):
         return remote(
-            q_src.at[plane], q_in.at[z], z_send.at[2, plane], z_recv.at[2, z], at(plane, holder(z, m))
+            q_src.at[plane], q_in.at[z], z_send.at[2, plane], z_recv.at[2, z], at(plane, m)
         )
 
     def in_plane(plane, own):
@@ -611,20 +617,9 @@
         passed = pool_slot(plane, y_member)
         return remote(passed, passed, pc_send.at[plane, 1], pc_recv.at[plane, 1], c_peer)
 
-    def pool_start():
-        pool_line(1).start()
-        pool_line(2).start()
-
     def pool_from_line(i):
         plane = order(i)
         arrived(pool_slot(plane, m), pool_recv.at[plane])
-        if i > 1:
-
-            @pl.when(between)
-            def _():
-                pool_line_on(i).start()
-
-        pool_across(plane, False).start()
         pool_beside(plane, False).start()
 
     def pool_from_pair(i):
@@ -659,19 +654,9 @@
             wo_ref if own else there, there, wc_send.at[half, plane, yy], wc_recv.at[half, plane, yy], c_peer
         )
 
-    def w_line_start():
-        w_line(1).start()
-        w_line(2).start()
-
     def w_from_line(i):
         plane = order(i)
         arrived(out_slot(tp, plane, y, c), wl_recv.at[plane])
-        if i > 1:
-
-            @pl.when(between)
-            def _():
-                w_line_on(i).start()
-
         w_swap(plane, y, False).start()
         w_beside(tp, plane, y, False).start()
 
@@ -761,6 +746,15 @@
     own_weights(last_one)
     w_swap(z, y, True).start()
     w_beside(tp, z, y, True).start()
+    pool_beside(z, True).start()
+    w_line(2).start()
+    pool_line(2).start()
+
+    @pl.when(jnp.logical_not(between))
+    def _():
+        w_line(1).start()
+        pool_line(1).start()
+
     product[...] = jnp.zeros_like(product)
     acc[...] = jnp.zeros_like(acc)
     total[...] = jnp.zeros_like(total)
@@ -797,7 +791,12 @@
     multiply(0, y, every)
     multiply(0, 1 - y, every)
     from_line(turn[3], last_one)
-    w_line_start()
+
+    @pl.when(between)
+    def _():
+        w_line(1).start()
+        pool_line(1).start()
+
     from_pair(turn[1], last_one)
     multiply(turn[1], y, every)
     from_pair(turn[2], first_pair)
@@ -828,23 +827,17 @@
         query = (product[2, :, part] * inverse_sc[:, :1]).astype(jnp.bfloat16)
         q_src[p] = query * (1.0 / math.sqrt(hdim))
 
-    @pl.when(z % 2 == 0)
-    def _():
-        q_in[z] = q_src[z]
-
-    @pl.when(z % 2 == 1)
-    def _():
-        q_out(z).start()
-
+    q_in[z] = q_src[z]
     for i in range(1, planes):
         q_out(order(i)).start()
-    pool_start()
     w_from_line(1)
+    pool_from_line(1)
 
     @pl.when(between)
     def _():
-        w_from_line(2)
-        w_from_line(3)
+        for i in (2, 3):
+            w_from_line(i)
+            pool_from_line(i)
 
     def visit(block, plane, first, count, masked):
         query = q_in[block]
@@ -859,7 +852,7 @@
             keys, both, (((1,), (1,)), ((), ())), preferred_element_type=jnp.float32
         )
         if masked:
-            shift = (first - holder(block, m)) * rows
+            shift = (first - m) * rows
             key = lax.broadcasted_iota(jnp.int32, scores.shape, 0)
             col = lax.broadcasted_iota(jnp.int32, scores.shape, 1)
             col = jnp.where(col < rows, col, col - rows)
@@ -876,7 +869,7 @@
         top[block] = new
 
     def diagonal(block):
-        pair = holder(block, m) // 2
+        pair = m // 2
 
         @pl.when(pair > 0)
         def _():
@@ -890,11 +883,11 @@
             branch.at[tp * planes + z, :, pl.ds(0, vdim)],
             back_send.at[block, half],
             back_recv.at[tp * planes + z],
-            at(block, holder(block, m), half),
+            at(block, m, half),
         )
 
     def at_home(block):
-        return (block == z) & (z % 2 == 0)
+        return block == z
 
     def finish(block):
         both = acc[block] / jnp.sum(total[block], axis=0, keepdims=True)
@@ -971,39 +964,53 @@
     landed(1)
     shared(z, True)
 
-    @pl.when(z % 2 == 1)
-    def _():
-        arrived(q_in.at[z], z_recv.at[2, z])
-
     def stage(i, carry):
         block = order(i)
 
+        diagonal(block)
+
         @pl.when(i < planes - 2)
         def _():
             landed(i + 2)
 
-        @pl.when(i == planes - 3)
+        @pl.when(i == 0)
+        def _():
+            w_from_pair(0)
+
+        @pl.when(i == 1)
         def _():
             w_across(order(1), False).start()
 
             @pl.when(between)
             def _():
-                w_across(order(2), False).start()
-                w_across(order(3), False).start()
+                for j in (2, 3):
+                    w_line_on(j).start()
+                    w_across(order(j), False).start()
+                for j in (2, 3):
+                    pool_line_on(j).start()
 
             pool_across(z, True).start()
-            pool_beside(z, True).start()
-
-        @pl.when(i == planes - 2)
-        def _():
-            w_from_pair(0)
-
-            @pl.when(jnp.logical_not(between))
+            pool_across(order(1), False).start()
+
+            @pl.when(between)
             def _():
-                w_from_line(2)
-                w_across(order(2), False).start()
-
-        diagonal(block)
+                for j in (2, 3):
+                    pool_across(order(j), False).start()
+
+        for j in (2, 3):
+
+            @pl.when((i == j) & jnp.logical_not(between))
+            def _():
+                w_from_line(j)
+                w_across(order(j), False).start()
+
+        @pl.when(i == 2)
+        def _():
+            w_from_pair(1)
+
+        @pl.when((i == 3) & between)
+        def _():
+            w_from_pair(2)
 
         @pl.when(i < planes - 1)
         def _():
@@ -1021,19 +1028,13 @@
             def _():
                 finish(j + 1)
 
-                @pl.when(j == 0)
+                @pl.when((j == 1) & between)
                 def _():
-                    @pl.when(jnp.logical_not(between))
-                    def _():
-                        w_from_line(3)
-                        w_across(order(3), False).start()
-
-                    pool_from_line(1)
-
-                @pl.when(j == 1)
+                    w_from_pair(3)
+
+                @pl.when((j == 1) & jnp.logical_not(between))
                 def _():
-                    w_from_pair(1)
-                    pool_from_line(2)
+                    w_from_pair(2)
 
             return carry
 
@@ -1048,17 +1049,19 @@
 
     lax.fori_loop(0, planes, stage, 0)
 
-    w_from_pair(2)
-    pool_from_line(3)
-    w_from_swap(0)
-    w_from_pair(3)
-    w_from_swap(1)
+
+    @pl.when(jnp.logical_not(between))
+    def _():
+        for i in (2, 3):
+            pool_from_line(i)
+            pool_across(order(i), False).start()
+        w_from_pair(3)
+
     for i in range(planes):
         pool_from_pair(i)
     pool_project()
-    w_from_swap(2)
+    w_from_swap(0)
     pool_mix()
-    w_from_swap(3)
 
     for head in range(2 * planes):
         own_head = tp * planes + z == head
@@ -1069,15 +1072,20 @@
 
     theirs = pl.ds(pl.multiple_of((1 - tp) * groups, groups), groups)
     arrived(branch.at[theirs, :, pl.ds(vdim, vdim)], half_sem.at[1])
-    for half in range(2):
-        for plane in range(planes):
+    left = jnp.concatenate([branch[head] for head in range(2 * planes)], axis=1)
+    out_width = members * out_columns
+
+    def column(i, carry):
+        plane = order(i)
+
+        @pl.when(i > 0)
+        def _():
+            w_from_swap(i)
+
+        for half in range(2):
             for yy in range(2):
                 arrived(out_slot(half, plane, yy, 1 - c), wc_recv.at[half, plane, yy])
-    left = jnp.concatenate([branch[head] for head in range(2 * planes)], axis=1)
-    out_width = out_ref.shape[1] // planes
-
-    def column(n, carry):
-        part = pl.ds(pl.multiple_of(n * out_width, out_width), out_width)
+        part = pl.ds(pl.multiple_of(plane * out_width, out_width), out_width)
         out_ref[:, part] = jnp.dot(
             left, w_full[:, part], preferred_element_type=jnp.float32
         ).astype(jnp.bfloat16)
@@ -1089,10 +1097,6 @@
         k_out(order(i)).wait_send()
         v_out(order(i)).wait_send()
         q_out(order(i)).wait_send()
-
-    @pl.when(z % 2 == 1)
-    def _():
-        q_out(z).wait_send()
 
     for i in range(planes):
         plane = order(i)

time: 137 us -> 128 us (0.934); the launches traced: 134 us -> 127 us
  Pallas kernels: 131 us -> 124 us
    pallas_call x1, Pallas kernels: 131 us -> 124 us  [whole_layer(): pl.pallas_call(functools.partial(layer, width // 2, model_width), out_sha...]
where the time goes in v6:
time: 128 us; the launch traced here: 127 us
  Pallas kernels  124 us (97%)
  local copies, waits for them, and re-layouts  3.37 us (3%)
    pallas_call x1, Pallas kernels, whole_layer(): pl.pallas_call(functools.partial(layer, width // 2, model_width), out_sha...  124 us
    unnamed x3, local copies, waits for them, and re-layouts  2.77 us

profile of v6, /device:TPU:0, one launch (start us, length us, event | category | flops | bytes accessed | tf_op | source)
XLA Modules:
  0.0 127.1 jit_solution(17461069723667646325)
XLA Ops:
  0.0 0.0 copy-start
  0.0 0.7 copy-done
  0.7 0.6 reshape.9.gain_in
  1.3 123.7 %shard_map.109 = bf16[192,2048]{1,0:T(8,128)(2,1)} custom-call(f32[4]{0:T(128)} %lam_ref.1, bf16[384,1024]{1,0:T(8,128)(2,1)} %tok_ref.1, bf16[1,1024]{1,0:T(2,128)(2,1)} %reshape.9.gain_in, bf16[128,512]{1,0:T(8,128)(2,1)} %wk_ref.1, bf16[128,512]{1,0:T(8,128)(2,1)} %wv_ref.1, bf16[128,512]{1,0:T(8,128)(2,1)} %wq_ref.1, bf16[128,512]{1,0:T(8,128)(2,1)} %wp_ref.1, ...), custom_call_target="tpu_custom_call" | custom-call | flops 4831838208 | bytes 16777216 | tf_op jit(solution)/shard_map/pallas_call | solution.py:1173
  125.0 2.1 %copy.13 = bf16[192,2048]{1,0:T(8,128)(2,1)} copy(bf16[192,2048]{1,0:T(8,128)(2,1)} %shard_map.109) | data formatting | bytes 1572864
Async XLA Ops:
  0.0 0.7 copy-start

commit v7 on v6

--- a/solution.py
+++ b/solution.py
@@ -969,6 +969,10 @@
 
         diagonal(block)
 
+        @pl.when(i == 1)
+        def _():
+            w_across(order(1), False).start()
+
         @pl.when(i < planes - 2)
         def _():
             landed(i + 2)
@@ -977,33 +981,24 @@
         def _():
             w_from_pair(0)
 
-        @pl.when(i == 1)
-        def _():
-            w_across(order(1), False).start()
-
-            @pl.when(between)
-            def _():
-                for j in (2, 3):
-                    w_line_on(j).start()
-                    w_across(order(j), False).start()
-                for j in (2, 3):
-                    pool_line_on(j).start()
-
+        @pl.when((i == 1) & between)
+        def _():
+            for j in (2, 3):
+                w_line_on(j).start()
+                w_across(order(j), False).start()
+            for j in (2, 3):
+                pool_line_on(j).start()
+            pool_across(z, True).start()
+            for j in (1, 2, 3):
+                pool_across(order(j), False).start()
+
+        @pl.when((i == 2) & jnp.logical_not(between))
+        def _():
+            w_from_line(2)
+            w_across(order(2), False).start()
             pool_across(z, True).start()
             pool_across(order(1), False).start()
 
-            @pl.when(between)
-            def _():
-                for j in (2, 3):
-                    pool_across(order(j), False).start()
-
-        for j in (2, 3):
-
-            @pl.when((i == j) & jnp.logical_not(between))
-            def _():
-                w_from_line(j)
-                w_across(order(j), False).start()
-
         @pl.when(i == 2)
         def _():
             w_from_pair(1)
@@ -1012,7 +1007,7 @@
         def _():
             w_from_pair(2)
 
-        @pl.when(i < planes - 1)
+        @pl.when(i < planes - 2)
         def _():
             hand_on(order(i + 1), False)
 
@@ -1028,13 +1023,22 @@
             def _():
                 finish(j + 1)
 
-                @pl.when((j == 1) & between)
-                def _():
-                    w_from_pair(3)
-
-                @pl.when((j == 1) & jnp.logical_not(between))
-                def _():
-                    w_from_pair(2)
+            @pl.when((i == 3) & (j == 1) & between)
+            def _():
+                w_from_pair(3)
+
+            @pl.when((i == planes - 2) & (j == 0))
+            def _():
+                hand_on(order(i + 1), False)
+
+            @pl.when((i == 2) & (j == 1) & jnp.logical_not(between))
+            def _():
+                w_from_line(3)
+                w_across(order(3), False).start()
+
+            @pl.when((i == 3) & (j == 0) & jnp.logical_not(between))
+            def _():
+                w_from_pair(2)
 
             return carry
 
@@ -1070,17 +1074,16 @@
         def _():
             arrived(branch.at[head, :, pl.ds(0, vdim)], back_recv.at[head])
 
+    w_from_swap(1)
+    w_from_swap(2)
     theirs = pl.ds(pl.multiple_of((1 - tp) * groups, groups), groups)
     arrived(branch.at[theirs, :, pl.ds(vdim, vdim)], half_sem.at[1])
+    w_from_swap(3)
     left = jnp.concatenate([branch[head] for head in range(2 * planes)], axis=1)
     out_width = members * out_columns
 
     def column(i, carry):
         plane = order(i)
-
-        @pl.when(i > 0)
-        def _():
-            w_from_swap(i)
 
         for half in range(2):
             for yy in range(2):

time: 128 us -> 123 us (0.961)
  Pallas kernels: 124 us -> 119 us
    pallas_call x1, Pallas kernels: 124 us -> 119 us  [whole_layer(): pl.pallas_call(functools.partial(layer, width // 2, model_width), out_sha...]
where the time goes in v7:
time: 123 us
  Pallas kernels  119 us (97%)
  local copies, waits for them, and re-layouts  3.37 us (3%)
    pallas_call x1, Pallas kernels, whole_layer(): pl.pallas_call(functools.partial(layer, width // 2, model_width), out_sha...  119 us
    unnamed x3, local copies, waits for them, and re-layouts  2.77 us

profile of v7, /device:TPU:0, one launch (start us, length us, event | category | flops | bytes accessed | tf_op | source)
XLA Modules:
  0.0 122.6 jit_solution(5814813532760447878)
XLA Ops:
  0.0 0.0 copy-start
  0.0 0.7 copy-done
  0.7 0.6 reshape.9.gain_in
  1.3 119.2 %shard_map.109 = bf16[192,2048]{1,0:T(8,128)(2,1)} custom-call(f32[4]{0:T(128)} %lam_ref.1, bf16[384,1024]{1,0:T(8,128)(2,1)} %tok_ref.1, bf16[1,1024]{1,0:T(2,128)(2,1)} %reshape.9.gain_in, bf16[128,512]{1,0:T(8,128)(2,1)} %wk_ref.1, bf16[128,512]{1,0:T(8,128)(2,1)} %wv_ref.1, bf16[128,512]{1,0:T(8,128)(2,1)} %wq_ref.1, bf16[128,512]{1,0:T(8,128)(2,1)} %wp_ref.1, ...), custom_call_target="tpu_custom_call" | custom-call | flops 4831838208 | bytes 16777216 | tf_op jit(solution)/shard_map/pallas_call | solution.py:1176
  120.5 2.1 %copy.13 = bf16[192,2048]{1,0:T(8,128)(2,1)} copy(bf16[192,2048]{1,0:T(8,128)(2,1)} %shard_map.109) | data formatting | bytes 1572864
Async XLA Ops:
  0.0 0.7 copy-start

commit v8 on v7

--- a/solution.py
+++ b/solution.py
@@ -969,17 +969,17 @@
 
         diagonal(block)
 
-        @pl.when(i == 1)
+        @pl.when(i < planes - 2)
+        def _():
+            landed(i + 2)
+
+        @pl.when(i == 0)
+        def _():
+            w_from_pair(0)
+
+        @pl.when(i == 0)
         def _():
             w_across(order(1), False).start()
-
-        @pl.when(i < planes - 2)
-        def _():
-            landed(i + 2)
-
-        @pl.when(i == 0)
-        def _():
-            w_from_pair(0)
 
         @pl.when((i == 1) & between)
         def _():
@@ -996,8 +996,6 @@
         def _():
             w_from_line(2)
             w_across(order(2), False).start()
-            pool_across(z, True).start()
-            pool_across(order(1), False).start()
 
         @pl.when(i == 2)
         def _():
@@ -1035,6 +1033,8 @@
             def _():
                 w_from_line(3)
                 w_across(order(3), False).start()
+                pool_across(z, True).start()
+                pool_across(order(1), False).start()
 
             @pl.when((i == 3) & (j == 0) & jnp.logical_not(between))
             def _():

time: 123 us -> 123 us (level)
  no operation moved by 1% of the time
where the time goes in v8:
time: 123 us; the launch traced here: 122 us
  Pallas kernels  119 us (97%)
  local copies, waits for them, and re-layouts  3.37 us (3%)
    pallas_call x1, Pallas kernels, whole_layer(): pl.pallas_call(functools.partial(layer, width // 2, model_width), out_sha...  119 us
    unnamed x3, local copies, waits for them, and re-layouts  2.77 us

profile of v8, /device:TPU:0, one launch (start us, length us, event | category | flops | bytes accessed | tf_op | source)
XLA Modules:
  0.0 122.4 jit_solution(13632781380579651353)
XLA Ops:
  0.0 0.0 copy-start
  0.0 0.7 copy-done
  0.7 0.6 reshape.9.gain_in
  1.3 119.0 %shard_map.109 = bf16[192,2048]{1,0:T(8,128)(2,1)} custom-call(f32[4]{0:T(128)} %lam_ref.1, bf16[384,1024]{1,0:T(8,128)(2,1)} %tok_ref.1, bf16[1,1024]{1,0:T(2,128)(2,1)} %reshape.9.gain_in, bf16[128,512]{1,0:T(8,128)(2,1)} %wk_ref.1, bf16[128,512]{1,0:T(8,128)(2,1)} %wv_ref.1, bf16[128,512]{1,0:T(8,128)(2,1)} %wq_ref.1, bf16[128,512]{1,0:T(8,128)(2,1)} %wp_ref.1, ...), custom_call_target="tpu_custom_call" | custom-call | flops 4831838208 | bytes 16777216 | tf_op jit(solution)/shard_map/pallas_call | solution.py:1176
  120.3 2.1 %copy.13 = bf16[192,2048]{1,0:T(8,128)(2,1)} copy(bf16[192,2048]{1,0:T(8,128)(2,1)} %shard_map.109) | data formatting | bytes 1572864
Async XLA Ops:
  0.0 0.7 copy-start
